TPU v7x, 32 devices: a whole 2x2x4 slice. The times are simulated.
32 devices in a mesh: sp: 8 (over z, y), dp: 4 (over x, core).
Axes of the slice: x: 2, y: 2, z: 4, core: 2. Of those that a mesh axis runs over, the one named last changes fastest.
Arguments:
- residual: bfloat16 [4, 1024, 2048], P('dp', 'sp'), may hold values from -6 to 6
- head_input: bfloat16 [4, 1024, 2048], P('dp', 'sp'), may hold values from -6 to 6
- gate_input: bfloat16 [4, 1024, 2048], P('dp', 'sp'), may hold values from -6 to 6
- b_input: bfloat16 [4, 1024, 1024], P('dp', 'sp'), may hold values from -6 to 6
- c_input: bfloat16 [4, 1024, 1024], P('dp', 'sp'), may hold values from -6 to 6
- step_input: bfloat16 [4, 1024, 32], P('dp', 'sp'), may hold values from -4.8 to 4.8
- conv_weight: bfloat16 [4, 2048], replicated, may hold values from -3 to 3
- conv_b_weight: bfloat16 [4, 1024], replicated, may hold values from -3 to 3
- conv_c_weight: bfloat16 [4, 1024], replicated, may hold values from -3 to 3
- step_bias: float32 [32], replicated, may hold values from -1 to 1
- decay_log: float32 [32], replicated, may hold values from -9.92 to -2.99
- skip: float32 [32], replicated, may hold values from 0.5 to 1.5
- norm_gain: float32 [2048], replicated, may hold values from 0.1 to 1.9
- out_weight: bfloat16 [2048, 2048], P('dp'), may hold values from -0.125 to 0.125
- ffn_gain: float32 [2048], replicated, may hold values from 0.1 to 1.9
- shared_gate: bfloat16 [2048, 512], replicated, may hold values from -0.125 to 0.125
- shared_up: bfloat16 [2048, 512], replicated, may hold values from -0.125 to 0.125
- shared_down: bfloat16 [512, 2048], replicated, may hold values from -0.25 to 0.25
- expert_gate: bfloat16 [32, 2048, 512], P(('sp', 'dp')), may hold values from -0.125 to 0.125
- expert_up: bfloat16 [32, 2048, 512], P(('sp', 'dp')), may hold values from -0.125 to 0.125
- expert_down: bfloat16 [32, 512, 2048], P(('sp', 'dp')), may hold values from -0.25 to 0.25
- routes: int32 [4, 1024, 2], P('dp', 'sp'), may hold values from 0 to 31, all different within a row; in each aligned block of 128 rows (0 to 127, 128 to 255, ..., all dimensions but the last counted through in order) at most 16 rows name the same one
- route_weights: float32 [4, 1024, 2], P('dp', 'sp'), may hold values from 0.25 to 1.25
Outputs:
- layer_out: bfloat16 [4, 1024, 2048], P('dp', 'sp')
Inputs may be any that keep to these rules, and one draw needn't show every extreme that they name: `routes`: each token names 2 different experts; among the rows of one device no expert is named more than 16 times, a bound that some block reaches.
All inputs are finite; a program needn't handle non-finite values.
Results may differ from a plain program's by a relative error of at most 0.015.
Values may be sent and summed in bfloat16 or wider, within the bound.
No kernel may reach another device: no remote copies, remote signals or barrier semaphores. Data moves between devices by JAX's collectives and lax.ppermute only.
A program may use at most 128 MiB of HBM per device.

v0:
```python
import jax
import jax.numpy as jnp
import numpy as np
from jax import lax
from jax.sharding import PartitionSpec as P

D = 2048
HEADS = 32
HEAD_DIM = 64
GROUPS = 8
STATE = 128
CONV_K = 4
BLOCK = 128
TOP_K = 2
INNER = 2048


EPS = 1e-06
HIGH = lax.Precision.HIGHEST


def conv_silu(padded, weight, length):
    total = jnp.zeros((length, padded.shape[1]), jnp.float32)
    for tap in range(weight.shape[0]):
        total = total + padded[tap : tap + length].astype(jnp.float32) * weight[tap].astype(
            jnp.float32
        )
    return jax.nn.silu(total)


def block_scan(xs, step, rate, bmat, cmat, block, init):
    length, heads, width = xs.shape
    count = length // block
    logs = (step * rate[None, :]).reshape(count, block, heads)
    weighted = (xs * step[:, :, None]).reshape(count, block, heads, width)
    bb = bmat.reshape(count, block, heads, -1)
    cc = cmat.reshape(count, block, heads, -1)
    cum = jnp.cumsum(logs, axis=1)
    lower = jnp.tril(jnp.ones((block, block), dtype=bool))[None, :, :, None]
    diff = cum[:, :, None, :] - cum[:, None, :, :]
    decay = jnp.where(lower, jnp.exp(jnp.where(lower, diff, 0.0)), 0.0)
    scores = jnp.einsum("clhn,cshn->clsh", cc, bb, precision=HIGH) * decay
    inner = jnp.einsum("clsh,cshp->clhp", scores, weighted, precision=HIGH)
    to_end = jnp.exp(cum[:, -1:, :] - cum)
    states = jnp.einsum("cshn,cshp->chpn", bb * to_end[..., None], weighted, precision=HIGH)
    totals = jnp.exp(cum[:, -1, :])

    def advance(carry, item):
        fresh, factor = item
        return (carry * factor[:, None, None] + fresh, carry)

    last, before = lax.scan(advance, init, (states, totals))
    outer = jnp.einsum("clhn,chpn->clhp", cc * jnp.exp(cum)[..., None], before, precision=HIGH)
    return ((inner + outer).reshape(length, heads, width), last)


def serve_experts(arrived, gate_w, up_w, down_w):
    local = gate_w.shape[0]
    shaped = arrived.reshape(-1, local, arrived.shape[1], arrived.shape[2])
    gate = jnp.einsum("aenc,ecf->aenf", shaped, gate_w, preferred_element_type=jnp.float32)
    up = jnp.einsum("aenc,ecf->aenf", shaped, up_w, preferred_element_type=jnp.float32)
    hidden = (jax.nn.silu(gate) * up).astype(jnp.bfloat16)
    done = jnp.einsum("aenf,efc->aenc", hidden, down_w, preferred_element_type=jnp.float32).astype(
        jnp.bfloat16
    )
    return done.reshape(arrived.shape)


def body(
    residual,
    head_input,
    gate_input,
    b_input,
    c_input,
    step_input,
    conv_weight,
    conv_b_weight,
    conv_c_weight,
    step_bias,
    decay_log,
    skip,
    norm_gain,
    out_weight,
    ffn_gain,
    shared_gate,
    shared_up,
    shared_down,
    expert_gate,
    expert_up,
    expert_down,
    routes,
    route_weights,
):
    tokens = head_input.shape[1]
    x_rows = head_input[0]
    b_rows = b_input[0]
    c_rows = c_input[0]
    step_rows = step_input[0]
    per_group = HEADS // GROUPS
    ways = lax.axis_size("sp")
    place = lax.axis_index("sp")
    local = HEADS // ways
    width = local * HEAD_DIM
    targets = np.arange(ways) * local // per_group
    paired = jnp.concatenate(
        [b_rows.reshape(tokens, GROUPS, STATE), c_rows.reshape(tokens, GROUPS, STATE)], axis=2
    )
    outgoing = (
        x_rows.reshape(tokens, ways, width),
        paired[:, targets],
        step_rows.reshape(tokens, ways, local),
    )
    got_x, got_pair, got_step = (
        lax.all_to_all(outgoing[0], "sp", split_axis=1, concat_axis=0, tiled=True),
        lax.all_to_all(outgoing[1], "sp", split_axis=1, concat_axis=0, tiled=True),
        lax.all_to_all(outgoing[2], "sp", split_axis=1, concat_axis=0, tiled=True),
    )
    length = got_x.shape[0]
    group = place * local // per_group
    taps = jnp.concatenate(
        [
            lax.dynamic_slice_in_dim(conv_weight, place * width, width, 1),
            lax.dynamic_slice_in_dim(conv_b_weight, group * STATE, STATE, 1),
            lax.dynamic_slice_in_dim(conv_c_weight, group * STATE, STATE, 1),
        ],
        axis=1,
    )
    rows = jnp.concatenate(
        [got_x.reshape(length, width), got_pair.reshape(length, 2 * STATE)], axis=1
    )
    act = conv_silu(jnp.pad(rows, ((CONV_K - 1, 0), (0, 0))), taps, length)
    xs = act[:, :width].reshape(length, local, HEAD_DIM)
    bm = jnp.broadcast_to(act[:, width : width + STATE][:, None, :], (length, local, STATE))
    cm = jnp.broadcast_to(act[:, width + STATE :][:, None, :], (length, local, STATE))
    step = jax.nn.softplus(
        got_step.reshape(length, local).astype(jnp.float32)
        + lax.dynamic_slice_in_dim(step_bias, place * local, local, 0)[None, :]
    )
    rate = -jnp.exp(lax.dynamic_slice_in_dim(decay_log, place * local, local, 0))
    skip_local = lax.dynamic_slice_in_dim(skip, place * local, local, 0)
    y, _ = block_scan(
        xs, step, rate, bm, cm, BLOCK, jnp.zeros((local, HEAD_DIM, STATE), jnp.float32)
    )
    y = (y + skip_local[None, :, None] * xs).astype(jnp.bfloat16).reshape(ways, tokens, width)
    scanned = lax.all_to_all(y, "sp", split_axis=0, concat_axis=2, tiled=True).reshape(
        tokens, INNER
    )
    gated = (scanned.astype(jnp.float32) * jax.nn.silu(gate_input[0].astype(jnp.float32))).reshape(
        tokens, GROUPS, INNER // GROUPS
    )
    gated = gated * lax.rsqrt(jnp.mean(gated * gated, axis=2, keepdims=True) + EPS)
    normed = (gated.reshape(tokens, INNER) * norm_gain[None, :]).astype(jnp.bfloat16)
    projected = jnp.dot(
        normed,
        lax.all_gather(out_weight, "dp", axis=0, tiled=True),
        preferred_element_type=jnp.float32,
    )
    mixed = (residual[0].astype(jnp.float32) + projected).astype(jnp.bfloat16)
    mixed_f = mixed.astype(jnp.float32)
    expert_in = (
        mixed_f
        * lax.rsqrt(jnp.mean(mixed_f * mixed_f, axis=1, keepdims=True) + EPS)
        * ffn_gain[None, :]
    ).astype(jnp.bfloat16)
    shared_hidden = (
        jax.nn.silu(jnp.dot(expert_in, shared_gate, preferred_element_type=jnp.float32))
        * jnp.dot(expert_in, shared_up, preferred_element_type=jnp.float32)
    ).astype(jnp.bfloat16)
    shared = jnp.dot(shared_hidden, shared_down, preferred_element_type=jnp.float32)
    ways_sp = lax.axis_size("sp")
    ways_dp = lax.axis_size("dp")
    experts = ways_sp * ways_dp * expert_gate.shape[0]
    slots = 2 * tokens * TOP_K // experts
    chosen = routes[0].reshape(-1)
    pairs = chosen.shape[0]
    onehot = (chosen[:, None] == jnp.arange(experts, dtype=jnp.int32)[None, :]).astype(jnp.int32)
    position = jnp.sum((jnp.cumsum(onehot, axis=0) - onehot) * onehot, axis=1)
    target = chosen * slots + position
    owner = jnp.arange(pairs, dtype=jnp.int32) // TOP_K
    outgoing = jnp.zeros((experts * slots, D), jnp.bfloat16).at[target].set(expert_in[owner])
    outgoing = outgoing.reshape(experts, slots, D)
    done = serve_experts(
        lax.all_to_all(outgoing, ("sp", "dp"), split_axis=0, concat_axis=0, tiled=True),
        expert_gate,
        expert_up,
        expert_down,
    )
    returned = lax.all_to_all(done, ("sp", "dp"), split_axis=0, concat_axis=0, tiled=True)
    pair_out = returned.reshape(experts * slots, D)[target]
    routed = jnp.sum(
        pair_out.reshape(tokens, TOP_K, D).astype(jnp.float32) * route_weights[0][:, :, None],
        axis=1,
    )
    return (mixed_f + shared + routed).astype(jnp.bfloat16)[None]


def solution(mesh):
    return jax.shard_map(
        body,
        mesh=mesh,
        in_specs=(
            P("dp", "sp", None),
            P("dp", "sp", None),
            P("dp", "sp", None),
            P("dp", "sp", None),
            P("dp", "sp", None),
            P("dp", "sp", None),
            P(),
            P(),
            P(),
            P(),
            P(),
            P(),
            P(),
            P("dp", None),
            P(),
            P(),
            P(),
            P(),
            P(("sp", "dp"), None, None),
            P(("sp", "dp"), None, None),
            P(("sp", "dp"), None, None),
            P("dp", "sp", None),
            P("dp", "sp", None),
        ),
        out_specs=P("dp", "sp", None),
        check_vma=False,
    )
```

profile of v0, /device:TPU:0, one launch (start us, length us, event | category | flops | bytes accessed | tf_op | source)
XLA Modules:
  0.0 292.4 jit_solution(8568359432632893805)
XLA Ops:
  6.5 0.7 all-gather.2.cloned.1.call-update
  7.3 7.5 %all-to-all-start.2 = ((bf16[128,8,4]{0,2,1:T(4,128)(2,1)}), bf16[128,8,4]{0,2,1:T(4,128)(2,1)S(1)}, u32[]{:S(2)}, u32[]{:S(2)}) async-start(bf16[128,8,4]{0,2,1:T(4,128)(2,1)} %bitcast.15), calls=%async_computation.2 | async-start | bytes 16384 | tf_op jit(solution)/shard_map/all_to_all | solution.py:116
  14.7 1.0 copy.114
  15.8 5.5 %all-to-all-done.2 = bf16[128,8,4]{0,2,1:T(4,128)(2,1)S(1)} async-done(((bf16[128,8,4]{0,2,1:T(4,128)(2,1)}), bf16[128,8,4]{0,2,1:T(4,128)(2,1)S(1)}, u32[]{:S(2)}, u32[]{:S(2)}) %all-to-all-start.2) | async-done | bytes 8224 | tf_op jit(solution)/shard_map/all_to_all | solution.py:116
  21.2 3.5 %all-to-all-start = ((bf16[128,8,256]{0,2,1:T(8,128)(2,1)}), bf16[128,8,256]{0,2,1:T(8,128)(2,1)S(1)}, u32[]{:S(2)}, u32[]{:S(2)}) async-start(bf16[128,8,256]{0,2,1:T(8,128)(2,1)} %bitcast.1), calls=%async_computation | async-start | bytes 1048576 | tf_op jit(solution)/shard_map/all_to_all | solution.py:114
  25.2 1.1 copy.117
  26.3 0.9 copy.119
  27.2 1.3 dynamic_slice.29
  28.5 0.7 dynamic_slice.31
  29.3 0.7 mul.258
  30.7 1.0 pad_maximum_fusion.1
  31.7 1.4 gather_fusion
  33.1 0.7 exponential_negate_fusion
  33.8 0.7 constant_dynamic-slice_fusion.3
  34.5 0.7 constant_dynamic-slice_fusion.1
  35.2 2.8 all-to-all-done
  38.0 4.1 %all-to-all-start.1 = ((bf16[128,8,256]{2,0,1:T(8,128)(2,1)}), bf16[128,8,256]{2,0,1:T(8,128)(2,1)}, u32[]{:S(2)}, u32[]{:S(2)}) async-start(bf16[128,8,256]{2,0,1:T(8,128)(2,1)} %bitcast.7), calls=%async_computation.1 | async-start | bytes 1048576 | tf_op jit(solution)/shard_map/all_to_all | solution.py:115
  42.5 23.3 %fusion.88 = f32[8,128,4]{2,0,1:T(8,128)S(1)} fusion(f32[8,128,4]{2,0,1:T(8,128)S(1)} %copy.122), kind=kOutput, calls=%fused_computation.132 | output fusion | flops 520192 | bytes 32768 | tf_op jit(solution)/shard_map/jit(cumsum)/reduce_window_sum | solution.py:38
  66.2 1.0 fusion.87
  67.2 1.2 copy.129
  68.8 1.3 copy.115
  70.1 1.1 pad_maximum_fusion
  71.2 1.3 divide_multiply_fusion
  72.5 1.4 copy-done.1
  74.0 1.3 copy.120
  75.3 1.6 copy.145
  77.4 3.2 %fusion.14 = f32[8,4,64,128]{3,2,1,0:T(8,128)} fusion(f32[8,128,4]{1,2,0:T(4,128)S(1)} %copy.129, f32[8,128,128]{2,1,0:T(8,128)S(1)} %bitcast.211, f32[8,128,4,64]{1,0,3,2:T(8,128)S(1)} %broadcast_multiply_fusion), kind=kOutput, calls=%fused_computation.26 | convolution fusion | flops 403177472 | bytes 2637824 | tf_op jit(solution)/shard_map/cshn,cshp->chpn/dot_general | solution.py:45
  80.5 4.4 %fusion.57 = f32[8,4,128,128]{3,2,1,0:T(8,128)S(1)} fusion(f32[8,128,128]{2,1,0:T(8,128)S(1)} %bitcast.209, f32[8,128,128]{2,1,0:T(8,128)S(1)} %bitcast.212), kind=kOutput, calls=%fused_computation.68 | convolution fusion | flops 805306368 | bytes 3145728 | tf_op jit(solution)/shard_map/clhn,cshn->clsh/dot_general | solution.py:42
  85.0 3.5 %fusion.11 = f32[8,4,64,128]{3,2,1,0:T(8,128)} fusion(f32[8,4,128,128]{3,2,1,0:T(8,128)S(1)} %fusion.57, f32[8,128,4]{1,2,0:T(4,128)S(1)} %copy.123, pred[128,128]{0,1:T(8,128)(4,1)S(1)} %iota_compare_fusion, f32[8,128,4,64]{1,0,3,2:T(8,128)S(1)} %broadcast_multiply_fusion), kind=kOutput, calls=%fused_computation.22 | convolution fusion | flops 404750336 | bytes 4227072 | tf_op jit(solution)/shard_map/clsh,cshp->clhp/dot_general | solution.py:43
  88.5 13.5 %while.13 = (s32[]{:T(128)}, f32[4,64,128]{2,1,0:T(8,128)S(1)}, f32[8,4,64,128]{3,2,1,0:T(8,128)}, f32[8,4]{1,0:T(8,128)S(1)}, f32[8,4,64,128]{3,2,1,0:T(8,128)}, /*index=5*/s32[]{:T(128)}, s32[]{:T(128)}) while((s32[]{:T(128)}, f32[4,64,128]{2,1,0:T(8,128)S(1)}, f32[8,4,64,128]{3,2,1,0:T(8,128)}, f32[8,4]{1,0:T(8,128)S(1)}, ...), condition=%wide.region_2.3_spmd.clone, body=%wide.region_1.2_spmd.clone.sunk | while | flops 131075 | bytes 656016 | solution.py:52
  89.2 1.0 bitcast_add_fusion.3
  90.8 1.0 bitcast_add_fusion.3
  92.5 1.0 bitcast_add_fusion.3
  93.5 0.7 bitcast_dynamic-update-slice_fusion.2
  94.2 1.0 bitcast_add_fusion.3
  95.8 1.0 bitcast_add_fusion.3
  97.5 1.0 bitcast_add_fusion.3
  99.2 1.0 bitcast_add_fusion.3
  100.8 1.0 bitcast_add_fusion.3
  102.0 7.0 %fusion.20 = f32[8,4,64,128]{3,2,1,0:T(8,128)} fusion(f32[8,4,64,128]{3,2,1,0:T(8,128)} %fusion.11, f32[8,4,64,128]{3,2,1,0:T(8,128)} %get-tuple-element.32, f32[8,128,4]{1,2,0:T(4,128)S(1)} %copy.132, f32[8,128,128]{2,1,0:T(8,128)} %bitcast.210), kind=kOutput, calls=%fused_computation.33 | convolution fusion | flops 403439616 | bytes 3686400 | tf_op jit(solution)/shard_map/clhn,chpn->clhp/dot_general | solution.py:53
  109.0 2.5 copy.133
  111.5 2.2 add_convert_fusion
  113.7 6.0 %all-to-all-start.3 = ((bf16[8,128,256]{2,1,0:T(8,128)(2,1)}), bf16[8,128,256]{2,1,0:T(8,128)(2,1)S(1)}, u32[]{:S(2)}, u32[]{:S(2)}) async-start(bf16[8,128,256]{2,1,0:T(8,128)(2,1)} %add_convert_fusion), calls=%async_computation.3 | async-start | bytes 1048576 | tf_op jit(solution)/shard_map/all_to_all | solution.py:145
  119.9 1.3 copy.135
  121.2 1.3 copy.137
  123.7 8.8 %all-to-all-done.3 = bf16[8,128,256]{2,1,0:T(8,128)(2,1)S(1)} async-done(((bf16[8,128,256]{2,1,0:T(8,128)(2,1)}), bf16[8,128,256]{2,1,0:T(8,128)(2,1)S(1)}, u32[]{:S(2)}, u32[]{:S(2)}) %all-to-all-start.3) | async-done | bytes 524320 | tf_op jit(solution)/shard_map/all_to_all | solution.py:145
  132.6 1.1 convert_bitcast_fusion.1
  133.7 2.5 copy.134
  136.2 1.8 fusion.41
  138.0 1.2 fusion.43
  139.2 4.9 %multiply_reduce_fusion.1 = (f32[128]{0:T(128)S(1)}, f32[128,2048]{1,0:T(8,128)S(1)}) fusion(bf16[128,2048]{0,1:T(8,128)(2,1)} %fusion.43, bf16[2048,2048]{1,0:T(8,128)(2,1)} %all-gather.2.cloned.1.call-done, bf16[1,128,2048]{2,1,0:T(8,128)(2,1)} %param.27), kind=kOutput, calls=%fused_computation.60 | convolution fusion | flops 1075314560 | bytes 10486272 | tf_op jit(solution)/shard_map/dot_general | solution.py:153
  144.1 1.0 multiply_convert_fusion
  145.1 7.2 %scatter_custom_fusion = bf16[512,2048]{1,0:T(8,128)(2,1)} fusion(s32[256]{0:T(256)S(1)} %bitcast.225, bf16[128,2048]{1,0:T(8,128)(2,1)} %multiply_convert_fusion, s32[1024]{0:T(1024)S(1)} %pad_clamp_fusion.1, bf16[]{:T(256)} %constant.86.clone.1), kind=kCustom, calls=%fused_computation.56 | custom fusion | bytes 2097664 | tf_op jit(solution)/shard_map/scatter | solution.py:180
  152.3 52.4 %all_to_all.58 = bf16[32,16,2048]{2,1,0:T(8,128)(2,1)S(1)} all-to-all(bf16[32,16,2048]{2,1,0:T(8,128)(2,1)} %bitcast.207), channel_id=1, replica_groups=mesh['sp'=8,'dp'=4] {'sp','dp'}, dimensions={0} | all-to-all | bytes 4194304 | tf_op jit(solution)/shard_map/all_to_all | solution.py:183
  204.7 1.3 copy-done.5
  206.0 2.2 fusion.23
  208.2 6.2 %convolution_convert_fusion = bf16[32,16,2048]{2,1,0:T(8,128)(2,1)} fusion(bf16[1,512,2048]{2,1,0:T(8,128)(2,1)S(1)} %copy-done, bf16[32,16,2048]{2,1,0:T(8,128)(2,1)} %copy-done.5, bf16[1,2048,512]{2,1,0:T(8,128)(2,1)} %param.46, f32[32,1,16,512]{3,2,0,1:T(8,128)} %fusion.23), kind=kOutput, calls=%fused_computation.8 | convolution fusion | flops 2150105088 | bytes 9437184 | tf_op jit(solution)/shard_map/aenf,efc->aenc/dot_general | solution.py:63
  214.5 3.8 %all-to-all-start.5 = ((bf16[32,16,2048]{2,1,0:T(8,128)(2,1)}), bf16[32,16,2048]{2,1,0:T(8,128)(2,1)}, u32[]{:S(2)}, u32[]{:S(2)}) async-start(bf16[32,16,2048]{2,1,0:T(8,128)(2,1)} %convolution_convert_fusion), calls=%async_computation.5 | async-start | bytes 4194304 | tf_op jit(solution)/shard_map/all_to_all | solution.py:188
  218.4 2.2 fusion.89
  220.6 46.4 %all-to-all-done.5 = bf16[32,16,2048]{2,1,0:T(8,128)(2,1)} async-done(((bf16[32,16,2048]{2,1,0:T(8,128)(2,1)}), bf16[32,16,2048]{2,1,0:T(8,128)(2,1)}, u32[]{:S(2)}, u32[]{:S(2)}) %all-to-all-start.5) | async-done | bytes 2097184 | tf_op jit(solution)/shard_map/all_to_all | solution.py:188
  267.0 5.2 %gather_fusion.1 = bf16[256,2048]{1,0:T(8,128)(2,1)} fusion(bf16[512,2048]{1,0:T(8,128)(2,1)} %bitcast.54, s32[1024]{0:T(1024)S(1)} %pad_clamp_fusion), kind=kCustom, calls=%fused_computation.2 | custom fusion | bytes 2098176 | tf_op jit(solution)/shard_map/gather | solution.py:189
  272.2 3.4 %reshape.277 = f32[128,2,2048]{2,1,0:T(2,128)} reshape(bf16[256,2048]{1,0:T(8,128)(2,1)} %gather_fusion.1) | data formatting | bytes 3145728 | tf_op jit(solution)/shard_map/convert_element_type | solution.py:191
  275.5 5.7 %multiply_reduce_fusion = f32[128,2048]{1,0:T(8,128)} fusion(f32[128,2,2048]{2,1,0:T(2,128)} %reshape.277, f32[128,2]{1,0:T(8,128)S(1)} %copy.142), kind=kLoop, calls=%fused_computation.23 | loop fusion | flops 786432 | bytes 3146752 | tf_op jit(solution)/shard_map/reduce_sum | solution.py:190
  281.3 4.3 %fusion.5 = bf16[1,128,2048]{2,1,0:T(8,128)(2,1)} fusion(f32[128,2048]{1,0:T(8,128)} %multiply_reduce_fusion, f32[128,2048]{1,0:T(8,128)S(1)} %get-tuple-element.97, bf16[512,2048]{1,0:T(8,128)(2,1)} %param.44, bf16[128,2048]{1,0:T(8,128)(2,1)} %multiply_convert_fusion, bf16[2048,512]{1,0:T(8,128)(2,1)} %param.43, f32[128,512]{1,0:T(8,128)S(1)} %fusion.89), kind=kOutput, calls=%fused_computation.15 | convolution fusion | flops 538050560 | bytes 7602176 | tf_op jit(solution)/shard_map/dot_general | solution.py:169
  (95 shorter events, 9.0 us)
Async XLA Ops:
  6.5 201.7 %copy-start = (bf16[1,512,2048]{2,1,0:T(8,128)(2,1)S(1)}, bf16[1,512,2048]{2,1,0:T(8,128)(2,1)}, u32[]{:S(2)}) copy-start(bf16[1,512,2048]{2,1,0:T(8,128)(2,1)} %param.47) | copy-start | bytes 6291460
  6.5 8.2 %copy-start.9 = (bf16[1,128,2048]{2,1,0:T(8,128)(2,1)S(1)}, bf16[1,128,2048]{2,1,0:T(8,128)(2,1)}, u32[]{:S(2)}) copy-start(bf16[1,128,2048]{2,1,0:T(8,128)(2,1)} %param.28) | copy-start | bytes 1572868
  6.5 18.3 %copy-start.10 = (bf16[1,128,1024]{2,1,0:T(8,128)(2,1)S(1)}, bf16[1,128,1024]{2,1,0:T(8,128)(2,1)}, u32[]{:S(2)}) copy-start(bf16[1,128,1024]{2,1,0:T(8,128)(2,1)} %param.30) | copy-start | bytes 786436
  6.5 132.6 %all-gather.2.cloned.1.call-start = ((), (), s32[]{:S(2)}) async-start(), calls=%async_computation.6 | async-start | bytes 10485760 | tf_op jit(solution)/shard_map/all_gather | solution.py:155
  7.3 14.0 %all-to-all-start.2 = ((bf16[128,8,4]{0,2,1:T(4,128)(2,1)}), bf16[128,8,4]{0,2,1:T(4,128)(2,1)S(1)}, u32[]{:S(2)}, u32[]{:S(2)}) async-start(bf16[128,8,4]{0,2,1:T(4,128)(2,1)} %bitcast.15), calls=%async_computation.2 | async-start | bytes 16384 | tf_op jit(solution)/shard_map/all_to_all | solution.py:116
  14.7 15.2 %copy-start.14 = (s32[1,128,2]{1,2,0:T(2,128)S(1)}, s32[1,128,2]{1,2,0:T(2,128)}, u32[]{:S(2)}) copy-start(s32[1,128,2]{1,2,0:T(2,128)} %param.48) | copy-start | bytes 3076
  21.2 16.8 %all-to-all-start = ((bf16[128,8,256]{0,2,1:T(8,128)(2,1)}), bf16[128,8,256]{0,2,1:T(8,128)(2,1)S(1)}, u32[]{:S(2)}, u32[]{:S(2)}) async-start(bf16[128,8,256]{0,2,1:T(8,128)(2,1)} %bitcast.1), calls=%async_computation | async-start | bytes 1048576 | tf_op jit(solution)/shard_map/all_to_all | solution.py:114
  30.1 0.6 copy-start.7
  31.7 10.5 %copy-start.17 = (f32[4]{0:T(128)S(1)}, f32[4]{0:T(128)}, u32[]{:S(2)}) copy-start(f32[4]{0:T(128)} %dynamic_slice.29) | copy-start | bytes 52
  38.0 4.3 %copy-start.6 = (bf16[128,8,256]{0,2,1:T(8,128)(2,1)}, bf16[128,8,256]{0,2,1:T(8,128)(2,1)S(1)}, u32[]{:S(2)}) copy-start(bf16[128,8,256]{0,2,1:T(8,128)(2,1)S(1)} %all-to-all-done) | copy-start | bytes 1572868
  38.0 32.1 %all-to-all-start.1 = ((bf16[128,8,256]{2,0,1:T(8,128)(2,1)}), bf16[128,8,256]{2,0,1:T(8,128)(2,1)}, u32[]{:S(2)}, u32[]{:S(2)}) async-start(bf16[128,8,256]{2,0,1:T(8,128)(2,1)} %bitcast.7), calls=%async_computation.1 | async-start | bytes 1048576 | tf_op jit(solution)/shard_map/all_to_all | solution.py:115
  72.5 1.4 copy-start.1
  75.3 1.9 copy-start.2
  77.3 3.3 %copy-start.3 = (f32[1024,128]{1,0:T(8,128)}, f32[1024,128]{1,0:T(8,128)S(1)}, u32[]{:S(2)}) copy-start(f32[1024,128]{1,0:T(8,128)S(1)} %get-tuple-element.87) | copy-start | bytes 1572868
  102.0 9.5 %copy-start.13 = (f32[256]{0:T(256)S(1)}, f32[256]{0:T(256)}, u32[]{:S(2)}) copy-start(f32[256]{0:T(256)} %mul.258) | copy-start | bytes 3076
  111.5 8.2 %copy-start.8 = (s32[1,128,2]{2,1,0:T(8,128)S(1)}, s32[1,128,2]{2,1,0:T(8,128)}, u32[]{:S(2)}) copy-start(s32[1,128,2]{2,1,0:T(8,128)} %copy-done.7) | copy-start | bytes 3076
  113.7 9.6 %copy-start.15 = (s32[1,128,2]{1,2,0:T(2,128)S(1)}, s32[1,128,2]{1,2,0:T(2,128)}, u32[]{:S(2)}) copy-start(s32[1,128,2]{1,2,0:T(2,128)} %param.48) | copy-start | bytes 3076
  113.7 18.8 %all-to-all-start.3 = ((bf16[8,128,256]{2,1,0:T(8,128)(2,1)}), bf16[8,128,256]{2,1,0:T(8,128)(2,1)S(1)}, u32[]{:S(2)}, u32[]{:S(2)}) async-start(bf16[8,128,256]{2,1,0:T(8,128)(2,1)} %add_convert_fusion), calls=%async_computation.3 | async-start | bytes 1048576 | tf_op jit(solution)/shard_map/all_to_all | solution.py:145
  133.7 4.3 %copy-start.11 = (f32[2048]{0:T(1024)S(1)}, f32[2048]{0:T(1024)}, u32[]{:S(2)}) copy-start(f32[2048]{0:T(1024)} %param.39) | copy-start | bytes 24580
  136.2 1.8 copy-start.4
  139.2 5.0 %copy-start.12 = (f32[2048]{0:T(1024)S(1)}, f32[2048]{0:T(1024)}, u32[]{:S(2)}) copy-start(f32[2048]{0:T(1024)} %param.41) | copy-start | bytes 24580
  152.3 53.7 %copy-start.18 = (bf16[1,2048,512]{2,1,0:T(8,128)(2,1)S(1)}, bf16[1,2048,512]{2,1,0:T(8,128)(2,1)}, u32[]{:S(2)}) copy-start(bf16[1,2048,512]{2,1,0:T(8,128)(2,1)} %param.45) | copy-start | bytes 6291460
  204.7 1.3 copy-start.5
  214.5 3.8 %copy-start.16 = (f32[1,128,2]{1,2,0:T(2,128)S(1)}, f32[1,128,2]{1,2,0:T(2,128)}, u32[]{:S(2)}) copy-start(f32[1,128,2]{1,2,0:T(2,128)} %param.49) | copy-start | bytes 3076
  214.5 52.5 %all-to-all-start.5 = ((bf16[32,16,2048]{2,1,0:T(8,128)(2,1)}), bf16[32,16,2048]{2,1,0:T(8,128)(2,1)}, u32[]{:S(2)}, u32[]{:S(2)}) async-start(bf16[32,16,2048]{2,1,0:T(8,128)(2,1)} %convolution_convert_fusion), calls=%async_computation.5 | async-start | bytes 4194304 | tf_op jit(solution)/shard_map/all_to_all | solution.py:188
Sparse Core Ops, SparseCore 0:
  8.9 60.9 all-gather.1
where the time goes:
time: 294 us; the launch traced here: 292 us
  waiting for transfers between devices  64.1 us (22%)
  other arithmetic  55.4 us (19%)
  blocking collectives  52.4 us (18%)
  local copies, waits for them, and re-layouts  43.4 us (15%)
  matrix products  38 us (13%)
  starting transfers between devices  24.9 us (8%)
  between operations  13.8 us (5%)
    all_to_all x1, blocking collectives, body(): lax.all_to_all(outgoing, ('sp', 'dp'), split_axis=0, concat_axis=0, tiled...  52.4 us
    all_to_all x1, waiting for transfers between devices, body(): lax.all_to_all(done, ('sp', 'dp'), split_axis=0, concat_axis=0, tiled=True)  46.4 us
    another operation x1, other arithmetic, block_scan(): cum = jnp.cumsum(logs, axis=1)  23.3 us
    unnamed x45, local copies, waits for them, and re-layouts  8.94 us
    all_to_all x1, waiting for transfers between devices, body(): lax.all_to_all(y, 'sp', split_axis=0, concat_axis=2, tiled=True)  8.85 us
    add x8, other arithmetic, advance(): return (carry * factor[:, None, None] + fresh, carry)  7.87 us
    all_to_all x1, starting transfers between devices, body(): lax.all_to_all(outgoing[2], 'sp', split_axis=1, concat_axis=0, tiled=True)  7.45 us
    scatter x1, local copies, waits for them, and re-layouts, body(): jnp.zeros((experts * slots, D), jnp.bfloat16).at[target]  7.19 us
  transfers between devices with their start and end apart: 6, of which 4 were waited for; matrix products, arithmetic and copies ran while one was open for 32% of the time, Pallas kernels for 0%

commit v1 on v0

v1 whole, which is shorter than its diff:
```python
import functools

import jax
import jax.numpy as jnp
import numpy as np
from jax import lax
from jax.experimental import pallas as pl
from jax.experimental.pallas import tpu as pltpu
from jax.sharding import PartitionSpec as P

HEAD_DIM = 64
STATE = 128
EPS = 1e-06
HIGH = lax.Precision.HIGHEST
F32 = jnp.float32
BF16 = jnp.bfloat16
EXTRA = 8
MIB = 1 << 20


def dot(a, b, ca, cb, precision=None):
    return lax.dot_general(
        a, b, (((ca,), (cb,)), ((), ())), preferred_element_type=F32, precision=precision
    )


def iota(shape, axis):
    return lax.broadcasted_iota(jnp.int32, shape, axis)


def silu(v):
    return v / (1.0 + jnp.exp(-v))


def vmem(limit):
    return pltpu.CompilerParams(vmem_limit_bytes=limit * MIB)


def cost(flops, nbytes):
    return pl.CostEstimate(flops=flops, bytes_accessed=nbytes, transcendentals=0)


def pack_kernel(width, targets, x_ref, b_ref, c_ref, s_ref, out_ref):
    tokens = x_ref.shape[0]
    ways = out_ref.shape[0]
    local = width // HEAD_DIM
    lanes = out_ref.shape[2]
    eye = (iota((tokens, tokens), 0) == iota((tokens, tokens), 1)).astype(BF16)
    turned = dot(s_ref[...], eye, 0, 0)
    for d in range(ways):
        out_ref[d, 0:tokens, 0:width] = x_ref[:, d * width : (d + 1) * width]
        at = targets[d] * STATE
        out_ref[d, 0:tokens, width : width + STATE] = b_ref[:, at : at + STATE]
        out_ref[d, 0:tokens, width + STATE : width + 2 * STATE] = c_ref[:, at : at + STATE]
        rows = jnp.concatenate(
            [turned[d * local : (d + 1) * local], jnp.zeros((EXTRA - local, tokens), F32)], axis=0
        )
        if tokens < lanes:
            rows = jnp.concatenate([rows, jnp.zeros((EXTRA, lanes - tokens), F32)], axis=1)
        out_ref[d, tokens : tokens + EXTRA, :] = rows.astype(BF16)


def scan_kernel(
    heads, place_ref, got_ref, wx_ref, wb_ref, wc_ref, bias_ref, dlog_ref, skip_ref,
    y_ref, rows_ref, state_ref,
):
    chunks = got_ref.shape[0]
    tokens = got_ref.shape[1] - EXTRA
    width = y_ref.shape[2]
    local = width // HEAD_DIM
    place = place_ref[0]
    rows_ref[0:8] = jnp.zeros((8, rows_ref.shape[1]), F32)
    taps = jnp.concatenate([wx_ref[...], wb_ref[...], wc_ref[...]], axis=1).astype(F32)
    pick = iota((EXTRA, heads), 1) == place * local + iota((EXTRA, heads), 0)
    bias = jnp.sum(jnp.where(pick, bias_ref[...], 0.0), axis=1, keepdims=True)
    rate = -jnp.exp(jnp.sum(jnp.where(pick, dlog_ref[...], 0.0), axis=1, keepdims=True))
    own = iota((heads, width), 0) == place * local + iota((heads, width), 1) // HEAD_DIM
    skip = dot(skip_ref[...], own.astype(F32), 1, 0, HIGH)
    upper = (iota((tokens, tokens), 0) <= iota((tokens, tokens), 1)).astype(F32)
    lower = iota((tokens, tokens), 0) >= iota((tokens, tokens), 1)
    r = iota((2 * EXTRA, 2 * width), 0)
    q = iota((2 * EXTRA, 2 * width), 1)
    spread = (r == (q // width) * EXTRA + (q % width) // HEAD_DIM).astype(F32)
    state_ref[...] = jnp.zeros_like(state_ref)
    for c in range(chunks):
        base = 8 + c * tokens
        rows_ref[base : base + tokens] = got_ref[c, 0:tokens, :].astype(F32)
    for c in range(chunks):
        base = 8 + c * tokens
        act = rows_ref[base : base + tokens] * taps[3:4]
        for k in range(3):
            act = act + rows_ref[pl.ds(base - 3 + k, tokens), :] * taps[k : k + 1]
        act = silu(act)
        xs = act[:, :width]
        bm = act[:, width : width + STATE].astype(BF16)
        cm = act[:, width + STATE :].astype(BF16)
        pre = got_ref[c, tokens : tokens + EXTRA, 0:tokens].astype(F32) + bias
        step = jnp.maximum(pre, 0.0) + jnp.log1p(jnp.exp(-jnp.abs(pre)))
        cum = dot(step * rate, upper, 1, 0, HIGH)
        total = cum[:, tokens - 1 : tokens]
        both = jnp.concatenate([step * jnp.exp(total - cum), jnp.exp(cum - total)], axis=0)
        wide = dot(both, spread, 0, 0, HIGH)
        xw = (xs * wide[:, :width]).astype(BF16)
        scores = jnp.where(lower, dot(cm, bm, 1, 1), 0.0).astype(BF16)
        fade = jnp.exp(total)
        old = jnp.concatenate(
            [
                state_ref[h * HEAD_DIM : (h + 1) * HEAD_DIM, :] * fade[h : h + 1, :]
                for h in range(local)
            ],
            axis=0,
        )
        y = dot(scores, xw, 1, 0) + dot(cm, old.astype(BF16), 1, 1)
        y_ref[c] = (wide[:, width:] * y + skip * xs).astype(BF16)
        if c < chunks - 1:
            state_ref[...] = old + dot(xw, bm, 0, 0)


def slot_of(routes, experts, slots):
    tokens, top = routes.shape
    hot = [iota((tokens, experts), 1) == routes[:, k : k + 1] for k in range(top)]
    count = sum(h.astype(F32) for h in hot).astype(BF16)
    before = (iota((tokens, tokens), 0) > iota((tokens, tokens), 1)).astype(BF16)
    ahead = dot(before, count, 1, 0)
    out = []
    for k in range(top):
        rank = jnp.sum(jnp.where(hot[k], ahead, 0.0), axis=1, keepdims=True)
        out.append(routes[:, k : k + 1] * slots + rank.astype(jnp.int32))
    return out


def mix_kernel(
    blocks, experts, slots, order_ref, got_ref, gate_ref, gain_ref, res_ref, fgain_ref,
    routes_ref, *refs,
):
    count = len(blocks)
    w_refs, (mixed_ref, x_ref, send_ref), (wbuf, acc, sem) = refs[:-6], refs[-6:-3], refs[-3:]
    per = wbuf.shape[1]
    copies = []
    for i, (which, row) in enumerate(blocks):
        copies.append(
            pltpu.make_async_copy(w_refs[which].at[pl.ds(row, per), :], wbuf.at[i], sem.at[i])
        )
        copies[-1].start()
    for i in range(count):
        at = pl.multiple_of(order_ref[i] * per, per)
        sub = got_ref.shape[2]
        if sub == per:
            v = got_ref[order_ref[i]].astype(F32)
        else:
            n = per // sub
            v = jnp.concatenate([got_ref[order_ref[i] * n + k] for k in range(n)], axis=1)
            v = v.astype(F32)
        v = v * silu(gate_ref[:, pl.ds(at, per)].astype(F32))
        v = v * lax.rsqrt(jnp.mean(v * v, axis=1, keepdims=True) + EPS)
        v = (v * gain_ref[:, pl.ds(at, per)]).astype(BF16)
        copies[i].wait()
        part = dot(v, wbuf[i], 1, 0)
        if i == 0:
            acc[...] = part
        else:
            acc[...] += part
    mixed = (res_ref[...].astype(F32) + acc[...]).astype(BF16)
    mixed_ref[...] = mixed
    m = mixed.astype(F32)
    x = m * lax.rsqrt(jnp.mean(m * m, axis=1, keepdims=True) + EPS) * fgain_ref[...]
    x = x.astype(BF16)
    x_ref[...] = x
    tokens = x.shape[0]
    lane = iota((tokens, experts * slots), 1)
    hit = functools.reduce(
        jnp.logical_or, [lane == s for s in slot_of(routes_ref[...], experts, slots)]
    )
    send_ref[...] = dot(hit.astype(BF16), x, 0, 0).astype(BF16)


def shared_kernel(x_ref, mixed_ref, wg_ref, wu_ref, wd_ref, out_ref):
    x = x_ref[...]
    h = (silu(dot(x, wg_ref[...], 1, 0)) * dot(x, wu_ref[...], 1, 0)).astype(BF16)
    out_ref[...] = mixed_ref[...].astype(F32) + dot(h, wd_ref[...], 1, 0)


def expert_kernel(x_ref, wg_ref, wu_ref, wd_ref, out_ref, acc):
    j = pl.program_id(1)
    x = x_ref[...]
    h = (silu(dot(x, wg_ref[0], 1, 0)) * dot(x, wu_ref[0], 1, 0)).astype(BF16)
    part = dot(h, wd_ref[0], 1, 0)

    @pl.when(j == 0)
    def _():
        acc[...] = part

    @pl.when(j > 0)
    def _():
        acc[...] += part

    @pl.when(j == pl.num_programs(1) - 1)
    def _():
        out_ref[...] = acc[...].astype(BF16)


def combine_kernel(experts, slots, got_ref, base_ref, routes_ref, weights_ref, out_ref):
    tokens = base_ref.shape[0]
    lane = iota((tokens, experts * slots), 1)
    w = jnp.zeros((tokens, experts * slots), F32)
    for k, s in enumerate(slot_of(routes_ref[...], experts, slots)):
        w = w + jnp.where(lane == s, weights_ref[:, k : k + 1], 0.0)
    high = w.astype(BF16)
    low = (w - high.astype(F32)).astype(BF16)
    got = got_ref[...]
    out_ref[...] = (base_ref[...] + dot(high, got, 1, 0) + dot(low, got, 1, 0)).astype(BF16)


def gather_rows(w, ways):
    if ways == 4:
        me = lax.axis_index("dp")
        across = lax.ppermute(w, "dp", [(j, j ^ 2) for j in range(4)])
        beside = lax.ppermute(w, "dp", [(j, j ^ 1) for j in range(4)])
        far = lax.ppermute(across, "dp", [(j, j ^ 1) for j in range(4)])
        return [w, beside, across, far], [me, me ^ 1, me ^ 2, me ^ 3]
    return [lax.all_gather(w, "dp", axis=0, tiled=True)], None


def body(
    residual, head_input, gate_input, b_input, c_input, step_input, conv_weight, conv_b_weight,
    conv_c_weight, step_bias, decay_log, skip, norm_gain, out_weight, ffn_gain, shared_gate,
    shared_up, shared_down, expert_gate, expert_up, expert_down, routes, route_weights,
):
    _, tokens, inner = head_input.shape
    features = residual.shape[2]
    heads = step_input.shape[2]
    groups = b_input.shape[2] // STATE
    per_group = heads // groups
    top = routes.shape[2]
    ways = lax.axis_size("sp")
    ways_dp = lax.axis_size("dp")
    experts = ways * ways_dp * expert_gate.shape[0]
    slots = 2 * tokens * top // experts
    place = lax.axis_index("sp").astype(jnp.int32)
    local = heads // ways
    width = local * HEAD_DIM
    targets = [d * local // per_group for d in range(ways)]
    span = inner // groups

    ws, owners = gather_rows(out_weight, ways_dp)
    rows_of = out_weight.shape[0]
    if owners is None:
        blocks = [(0, g * span) for g in range(groups)]
        order = jnp.arange(groups, dtype=jnp.int32)
    else:
        each = rows_of // span
        blocks = [(i, k * span) for i in range(len(ws)) for k in range(each)]
        order = jnp.stack([o * each + k for o in owners for k in range(each)]).astype(jnp.int32)

    lanes = width + 2 * STATE
    packed = pl.pallas_call(
        functools.partial(pack_kernel, width, targets),
        out_shape=jax.ShapeDtypeStruct((ways, tokens + EXTRA, lanes), BF16),
        compiler_params=vmem(16),
        cost_estimate=cost(1 << 20, 4 * MIB),
        name="pack",
    )(head_input[0], b_input[0], c_input[0], step_input[0])
    got = lax.all_to_all(packed, "sp", split_axis=0, concat_axis=0, tiled=True)

    def whole(shape):
        return pl.BlockSpec(shape, lambda i, s: (0,) * len(shape))

    y = pl.pallas_call(
        functools.partial(scan_kernel, heads),
        out_shape=jax.ShapeDtypeStruct((ways, tokens, width), BF16),
        grid_spec=pltpu.PrefetchScalarGridSpec(
            num_scalar_prefetch=1,
            grid=(1,),
            in_specs=[
                whole(got.shape),
                pl.BlockSpec((conv_weight.shape[0], width), lambda i, s: (0, s[0])),
                pl.BlockSpec(
                    (conv_weight.shape[0], STATE), lambda i, s: (0, s[0] * local // per_group)
                ),
                pl.BlockSpec(
                    (conv_weight.shape[0], STATE), lambda i, s: (0, s[0] * local // per_group)
                ),
                whole((1, heads)),
                whole((1, heads)),
                whole((1, heads)),
            ],
            out_specs=whole((ways, tokens, width)),
            scratch_shapes=[
                pltpu.VMEM((8 + ways * tokens, lanes), F32),
                pltpu.VMEM((width, STATE), F32),
            ],
        ),
        compiler_params=vmem(32),
        cost_estimate=cost(1 << 30, 4 * MIB),
        name="scan",
    )(
        place[None], got, conv_weight, conv_b_weight, conv_c_weight,
        step_bias[None], decay_log[None], skip[None],
    )
    back = lax.all_to_all(y, "sp", split_axis=0, concat_axis=0, tiled=True)

    vm = pl.BlockSpec(memory_space=pltpu.VMEM)
    mixed, x, send = pl.pallas_call(
        functools.partial(mix_kernel, blocks, experts, slots),
        out_shape=(
            jax.ShapeDtypeStruct((tokens, features), BF16),
            jax.ShapeDtypeStruct((tokens, features), BF16),
            jax.ShapeDtypeStruct((experts * slots, features), BF16),
        ),
        in_specs=[pl.BlockSpec(memory_space=pltpu.SMEM)]
        + [vm] * 6
        + [pl.BlockSpec(memory_space=pl.ANY)] * len(ws),
        out_specs=(vm, vm, vm),
        scratch_shapes=[
            pltpu.VMEM((groups, span, features), BF16),
            pltpu.VMEM((tokens, features), F32),
            pltpu.SemaphoreType.DMA((groups,)),
        ],
        compiler_params=vmem(48),
        cost_estimate=cost(3 << 30, 16 * MIB),
        name="mix",
    )(
        order, back, gate_input[0], norm_gain[None], residual[0], ffn_gain[None], routes[0], *ws
    )

    base = pl.pallas_call(
        shared_kernel,
        out_shape=jax.ShapeDtypeStruct((tokens, features), F32),
        compiler_params=vmem(32),
        cost_estimate=cost(1 << 30, 8 * MIB),
        name="shared",
    )(x, mixed, shared_gate, shared_up, shared_down)

    arrived = lax.all_to_all(
        send.reshape(experts, slots, features), ("sp", "dp"), split_axis=0, concat_axis=0, tiled=True
    )
    own = expert_gate.shape[0]
    ff = expert_gate.shape[2]
    if own > 1:
        arrived = arrived.reshape(-1, own, slots, features).swapaxes(0, 1)
    arrived = arrived.reshape(own, -1, features)
    m = arrived.shape[1]
    bn = min(256, ff)
    done = pl.pallas_call(
        expert_kernel,
        out_shape=jax.ShapeDtypeStruct((own, m, features), BF16),
        grid=(own, ff // bn),
        in_specs=[
            pl.BlockSpec((None, m, features), lambda e, j: (e, 0, 0)),
            pl.BlockSpec((1, features, bn), lambda e, j: (e, 0, j)),
            pl.BlockSpec((1, features, bn), lambda e, j: (e, 0, j)),
            pl.BlockSpec((1, bn, features), lambda e, j: (e, j, 0)),
        ],
        out_specs=pl.BlockSpec((None, m, features), lambda e, j: (e, 0, 0)),
        scratch_shapes=[pltpu.VMEM((m, features), F32)],
        compiler_params=vmem(48),
        cost_estimate=cost(4 << 30, 10 * MIB),
        name="experts",
    )(arrived, expert_gate, expert_up, expert_down)
    if own > 1:
        done = done.reshape(own, -1, slots, features).swapaxes(0, 1)
    done = done.reshape(experts, slots, features)
    returned = lax.all_to_all(done, ("sp", "dp"), split_axis=0, concat_axis=0, tiled=True)
    out = pl.pallas_call(
        functools.partial(combine_kernel, experts, slots),
        out_shape=jax.ShapeDtypeStruct((tokens, features), BF16),
        compiler_params=vmem(32),
        cost_estimate=cost(1 << 30, 8 * MIB),
        name="combine",
    )(returned.reshape(experts * slots, features), base, routes[0], route_weights[0])
    return out[None]


def solution(mesh):
    tok = P("dp", "sp", None)
    exp = P(("sp", "dp"), None, None)
    return jax.shard_map(
        body,
        mesh=mesh,
        in_specs=(tok,) * 6
        + (P(),) * 7
        + (P("dp", None),)
        + (P(),) * 4
        + (exp,) * 3
        + (tok, tok),
        out_specs=tok,
        check_vma=False,
    )
```

time: 294 us -> 198 us (0.67)
  other arithmetic: 55.4 us -> 0 us
  matrix products: 38 us -> 0 us
  local copies, waits for them, and re-layouts: 43.4 us -> 13.1 us
  waiting for transfers between devices: 64.1 us -> 90.7 us
  Pallas kernels: 0 us -> 22.8 us
  between operations: 13.8 us -> 0.22 us
  starting transfers between devices: 24.9 us -> 18.6 us
    dot_general x9 -> x0, matrix products: 38 us -> none  [the longest x1 7 us: block_scan(): jnp.einsum('clhn,chpn->clhp', cc * jnp.exp(cum)[..., None], before, preci...]
    ppermute x0 -> x3, waiting for transfers between devices: none -> 35.1 us  [the longest x1 35.1 us: gather_rows(): across = lax.ppermute(w, 'dp', [(j, j ^ 2) for j in range(4)])]
    another operation x3 -> x0, other arithmetic: 23.9 us -> none  [the longest x1 23.3 us: block_scan(): cum = jnp.cumsum(logs, axis=1)]
    pallas_call x0 -> x6, Pallas kernels: none -> 22.8 us  [the longest x1 6.87 us: body(): pl.pallas_call(functools.partial(scan_kernel, heads), out_shape=jax.Shape...]
    all_to_all x4 -> x2, starting transfers between devices: 21.1 us -> 11.9 us  [the longest x1 6.09 us: body(): back = lax.all_to_all(y, 'sp', split_axis=0, concat_axis=0, tiled=True)]
    add x8 -> x0, other arithmetic: 7.87 us -> none  [advance(): return (carry * factor[:, None, None] + fresh, carry)]
    reduce_sum x3 -> x0, other arithmetic: 7.56 us -> none  [the longest x1 5.71 us: body(): jnp.sum(pair_out.reshape(tokens, TOP_K, D).astype(jnp.float32) * route_we...]
    scatter x1 -> x0, local copies, waits for them, and re-layouts: 7.19 us -> none  [body(): jnp.zeros((experts * slots, D), jnp.bfloat16).at[target]]
  transfers between devices with their start and end apart: 6 -> 6, of which waited for: 4 -> 3; matrix products, arithmetic and copies ran while one was open for 32% -> 1% of each run, Pallas kernels for 0% -> 5%
where the time goes in v1:
time: 198 us
  waiting for transfers between devices  90.7 us (46%)
  blocking collectives  52.1 us (26%)
  Pallas kernels  22.8 us (12%)
  starting transfers between devices  18.6 us (9%)
  local copies, waits for them, and re-layouts  13.1 us (7%)
    all_to_all x1, blocking collectives, body(): lax.all_to_all(send.reshape(experts, slots, features), ('sp', 'dp'), spli...  52.1 us
    all_to_all x1, waiting for transfers between devices, body(): lax.all_to_all(done, ('sp', 'dp'), split_axis=0, concat_axis=0, tiled=True)  40.6 us
    ppermute x1, waiting for transfers between devices, gather_rows(): across = lax.ppermute(w, 'dp', [(j, j ^ 2) for j in range(4)])  35.1 us
    all_to_all x1, waiting for transfers between devices, body(): back = lax.all_to_all(y, 'sp', split_axis=0, concat_axis=0, tiled=True)  15 us
    unnamed x49, local copies, waits for them, and re-layouts  13 us
    pallas_call x1, Pallas kernels, body(): pl.pallas_call(functools.partial(scan_kernel, heads), out_shape=jax.Shape...  6.87 us
    pallas_call x1, Pallas kernels, body(): pl.pallas_call(expert_kernel, out_shape=jax.ShapeDtypeStruct((own, m, fea...  6.37 us
    all_to_all x1, starting transfers between devices, body(): back = lax.all_to_all(y, 'sp', split_axis=0, concat_axis=0, tiled=True)  6.09 us
  transfers between devices with their start and end apart: 6, of which 3 were waited for; matrix products, arithmetic and copies ran while one was open for 1% of the time, Pallas kernels for 5%

profile of v1, /device:TPU:0, one launch (start us, length us, event | category | flops | bytes accessed | tf_op | source)
XLA Modules:
  0.0 197.5 jit_solution(7195752949095461392)
XLA Ops:
  0.0 3.0 %collective-permute-start.1 = (bf16[512,2048]{1,0:T(8,128)(2,1)}, bf16[512,2048]{1,0:T(8,128)(2,1)}, u32[]{:S(2)}, u32[]{:S(2)}) collective-permute-start(bf16[512,2048]{1,0:T(8,128)(2,1)} %refs_0_.1), channel_id=1, source_target_pairs={{0,2},{1,3},{2,0},{3,1},{4,6},{5,7},{6,4},{7,5},{8,10},{9,11},{10,... | collective-permute-start | bytes 6291464 | tf_op jit(solution)/shard_map/ppermute | solution.py:217
  3.0 0.8 copy.24
  3.8 0.0 copy-start.8
  3.8 1.0 copy-done.8
  4.8 0.0 copy-start.9
  4.8 0.9 copy-done.9
  5.8 0.0 copy-start.10
  5.8 0.9 copy-done.10
  6.7 0.0 copy-start.13
  6.7 0.0 copy-start.14
  6.7 0.0 copy-start.15
  6.7 0.0 copy-start.18
  6.7 0.0 copy-start.19
  6.8 0.0 copy-start.20
  6.8 1.2 pack.1
  7.9 5.8 %all-to-all-start = ((bf16[8,136,512]{2,1,0:T(8,128)(2,1)}), bf16[8,136,512]{2,1,0:T(8,128)(2,1)S(1)}, u32[]{:S(2)}, u32[]{:S(2)}) async-start(bf16[8,136,512]{2,1,0:T(8,128)(2,1)} %pack.1), calls=%async_computation | async-start | bytes 2228224 | tf_op jit(solution)/shard_map/all_to_all | solution.py:263
  13.8 0.0 collective-permute-start
  13.8 35.1 %collective-permute-done.1.refs_2_ = bf16[512,2048]{1,0:T(8,128)(2,1)} collective-permute-done((bf16[512,2048]{1,0:T(8,128)(2,1)}, bf16[512,2048]{1,0:T(8,128)(2,1)}, u32[]{:S(2)}, u32[]{:S(2)}) %collective-permute-start.1) | collective-permute-done | bytes 2097184 | tf_op jit(solution)/shard_map/ppermute | solution.py:217
  48.9 0.0 collective-permute-start.2
  48.9 0.0 all-to-all-done.got_ref
  48.9 0.0 copy-done.13
  48.9 0.0 copy-done.14
  48.9 0.0 copy-done.15
  48.9 0.0 copy-done.18
  49.0 0.0 copy-done.19
  49.0 0.0 copy-done.20
  49.0 0.0 copy-start.21
  49.0 0.0 copy-start.11
  49.0 0.0 copy-start.12
  49.0 0.0 copy-start.16
  49.0 0.0 copy-start.17
  49.0 6.9 %scan.1 = bf16[8,128,256]{2,1,0:T(8,128)(2,1)} custom-call(s32[1]{0:T(128)} %bitcast.8.place_ref, bf16[8,136,512]{2,1,0:T(8,128)(2,1)S(1)} %all-to-all-done.got_ref, bf16[4,2048]{1,0:T(4,128)(2,1)S(1)} %copy-done.13, bf16[4,1024]{1,0:T(4,128)(2,1)S(1)} %copy-done.14, bf16[4,1024]{1,0:T(4,128)(2,1)S(1)} %copy-done.15, f32[1,32]{1,0:T(1,128)S(1)} %bitcast.42, ...), custom_call_target="tpu_custom_call" | custom-call | flops 1073741824 | bytes 4194304 | tf_op jit(solution)/shard_map/scan/pallas_call | solution.py:268
  55.9 6.1 %all-to-all-start.1 = ((bf16[8,128,256]{2,1,0:T(8,128)(2,1)}), bf16[8,128,256]{2,1,0:T(8,128)(2,1)S(1)}, u32[]{:S(2)}, u32[]{:S(2)}) async-start(bf16[8,128,256]{2,1,0:T(8,128)(2,1)} %scan.1), calls=%async_computation.1 | async-start | bytes 1048576 | tf_op jit(solution)/shard_map/all_to_all | solution.py:300
  62.0 0.0 copy-done.21
  62.0 0.1 copy.25
  62.1 0.1 stack.35.order_ref
  62.2 0.0 collective-permute-done.refs_1_
  62.2 15.0 %all-to-all-done.1.got_ref = bf16[8,128,256]{2,1,0:T(8,128)(2,1)S(1)} async-done(((bf16[8,128,256]{2,1,0:T(8,128)(2,1)}), bf16[8,128,256]{2,1,0:T(8,128)(2,1)S(1)}, u32[]{:S(2)}, u32[]{:S(2)}) %all-to-all-start.1) | async-done | bytes 524320 | tf_op jit(solution)/shard_map/all_to_all | solution.py:300
  77.2 0.0 collective-permute-done.2.refs_3_
  77.2 0.0 copy-done.11
  77.2 0.0 copy-done.12
  77.2 0.0 copy-done.16
  77.2 0.0 copy-done.17
  77.2 5.3 %mix.1 = (bf16[128,2048]{1,0:T(8,128)(2,1)S(1)}, bf16[128,2048]{1,0:T(8,128)(2,1)S(1)}, bf16[512,2048]{1,0:T(8,128)(2,1)S(1)}) custom-call(s32[8]{0:T(128)S(1)} %stack.35.order_ref, bf16[8,128,256]{2,1,0:T(8,128)(2,1)S(1)} %all-to-all-done.1.got_ref, bf16[128,2048]{1,0:T(8,128)(2,1)S(1)} %bitcast.38, f32[1,2048]{1,0:T(1,128)S(1)} %bitcast.40, ...), custom_call_target="tpu_custom_call" | custom-call | flops 3221225472 | bytes 16777216 | tf_op jit(solution)/shard_map/mix/pallas_call | solution.py:303
  82.5 0.0 copy-start.6
  82.5 0.8 copy-done.6
  83.3 0.0 copy-start.4
  83.3 52.1 %all_to_all.20 = bf16[32,16,2048]{2,1,0:T(8,128)(2,1)S(1)} all-to-all(bf16[32,16,2048]{2,1,0:T(8,128)(2,1)S(1)} %bitcast.29), channel_id=1, replica_groups=mesh['sp'=8,'dp'=4] {'sp','dp'}, dimensions={0} | all-to-all | bytes 4194304 | tf_op jit(solution)/shard_map/all_to_all | solution.py:334
  135.4 0.0 copy-done.4
  135.4 6.4 %experts.1 = bf16[1,512,2048]{2,1,0:T(8,128)(2,1)S(1)} custom-call(bf16[1,512,2048]{2,1,0:T(8,128)(2,1)S(1)} %bitcast.30, bf16[1,2048,512]{2,1,0:T(8,128)(2,1)} %wg_ref.2, bf16[1,2048,512]{2,1,0:T(8,128)(2,1)} %wu_ref.2, bf16[1,512,2048]{2,1,0:T(8,128)(2,1)} %wd_ref.2), custom_call_target="tpu_custom_call" | custom-call | flops 4294967296 | bytes 10485760 | tf_op jit(solution)/shard_map/experts/pallas_call | solution.py:344
  141.8 0.0 copy-start
  141.8 1.4 copy-done
  143.2 0.0 copy-start.22
  143.2 3.7 %all-to-all-start.3 = ((bf16[32,16,2048]{2,1,0:T(8,128)(2,1)}), bf16[32,16,2048]{2,1,0:T(8,128)(2,1)S(1)}, u32[]{:S(2)}, u32[]{:S(2)}) async-start(bf16[32,16,2048]{2,1,0:T(8,128)(2,1)} %bitcast.28), calls=%async_computation.3 | async-start | bytes 4194304 | tf_op jit(solution)/shard_map/all_to_all | solution.py:363
  146.8 0.0 copy-done.22
  146.9 0.1 copy.26
  147.0 1.6 copy-done.1
  148.6 1.6 copy-done.2
  150.2 1.6 copy-done.3
  151.7 1.0 copy-done.5
  152.8 1.0 copy-done.7
  153.8 1.1 shared.1.base_ref
  154.9 40.6 %all-to-all-done.3 = bf16[32,16,2048]{2,1,0:T(8,128)(2,1)S(1)} async-done(((bf16[32,16,2048]{2,1,0:T(8,128)(2,1)}), bf16[32,16,2048]{2,1,0:T(8,128)(2,1)S(1)}, u32[]{:S(2)}, u32[]{:S(2)}) %all-to-all-start.3) | async-done | bytes 2097184 | tf_op jit(solution)/shard_map/all_to_all | solution.py:363
  195.6 1.9 combine.1
  (5 shorter events, 0.0 us)
Async XLA Ops:
  0.0 48.9 %collective-permute-start.1 = (bf16[512,2048]{1,0:T(8,128)(2,1)}, bf16[512,2048]{1,0:T(8,128)(2,1)}, u32[]{:S(2)}, u32[]{:S(2)}) collective-permute-start(bf16[512,2048]{1,0:T(8,128)(2,1)} %refs_0_.1), channel_id=1, source_target_pairs={{0,2},{1,3},{2,0},{3,1},{4,6},{5,7},{6,4},{7,5},{8,10},{9,11},{10,... | collective-permute-start | bytes 6291464 | tf_op jit(solution)/shard_map/ppermute | solution.py:217
  3.8 1.0 copy-start.8
  4.8 0.9 copy-start.9
  5.8 0.9 copy-start.10
  6.7 42.2 %copy-start.13 = (bf16[4,2048]{1,0:T(4,128)(2,1)S(1)}, bf16[4,2048]{1,0:T(4,128)(2,1)}, u32[]{:S(2)}) copy-start(bf16[4,2048]{1,0:T(4,128)(2,1)} %wx_ref.1) | copy-start | bytes 49156
  6.7 42.2 %copy-start.14 = (bf16[4,1024]{1,0:T(4,128)(2,1)S(1)}, bf16[4,1024]{1,0:T(4,128)(2,1)}, u32[]{:S(2)}) copy-start(bf16[4,1024]{1,0:T(4,128)(2,1)} %wb_ref.1) | copy-start | bytes 24580
  6.7 42.2 %copy-start.15 = (bf16[4,1024]{1,0:T(4,128)(2,1)S(1)}, bf16[4,1024]{1,0:T(4,128)(2,1)}, u32[]{:S(2)}) copy-start(bf16[4,1024]{1,0:T(4,128)(2,1)} %wc_ref.1) | copy-start | bytes 24580
  6.7 42.2 %copy-start.18 = (f32[32]{0:T(128)S(1)}, f32[32]{0:T(128)}, u32[]{:S(2)}) copy-start(f32[32]{0:T(128)} %param.32) | copy-start | bytes 388
  6.7 42.2 %copy-start.19 = (f32[32]{0:T(128)S(1)}, f32[32]{0:T(128)}, u32[]{:S(2)}) copy-start(f32[32]{0:T(128)} %param.33) | copy-start | bytes 388
  6.8 42.2 %copy-start.20 = (f32[32]{0:T(128)S(1)}, f32[32]{0:T(128)}, u32[]{:S(2)}) copy-start(f32[32]{0:T(128)} %param.34) | copy-start | bytes 388
  7.9 41.0 %all-to-all-start = ((bf16[8,136,512]{2,1,0:T(8,128)(2,1)}), bf16[8,136,512]{2,1,0:T(8,128)(2,1)S(1)}, u32[]{:S(2)}, u32[]{:S(2)}) async-start(bf16[8,136,512]{2,1,0:T(8,128)(2,1)} %pack.1), calls=%async_computation | async-start | bytes 2228224 | tf_op jit(solution)/shard_map/all_to_all | solution.py:263
  13.8 48.4 %collective-permute-start = (bf16[512,2048]{1,0:T(8,128)(2,1)}, bf16[512,2048]{1,0:T(8,128)(2,1)}, u32[]{:S(2)}, u32[]{:S(2)}) collective-permute-start(bf16[512,2048]{1,0:T(8,128)(2,1)} %refs_0_.1), channel_id=1, source_target_pairs={{0,1},{1,0},{2,3},{3,2},{4,5},{5,4},{6,7},{7,6},{8,9},{9,8},{10,11... | collective-permute-start | bytes 6291464 | tf_op jit(solution)/shard_map/ppermute | solution.py:218
  48.9 28.3 %collective-permute-start.2 = (bf16[512,2048]{1,0:T(8,128)(2,1)}, bf16[512,2048]{1,0:T(8,128)(2,1)}, u32[]{:S(2)}, u32[]{:S(2)}) collective-permute-start(bf16[512,2048]{1,0:T(8,128)(2,1)} %collective-permute-done.1.refs_2_), channel_id=1, source_target_pairs={{0,1},{1,0},{2,3},{3,2},{4,5},{5,4},{6,7},{7,6},{8,9},{9,8},{10,11... | collective-permute-start | bytes 6291464 | tf_op jit(solution)/shard_map/ppermute | solution.py:219
  49.0 13.0 %copy-start.21 = (s32[1,128,2]{1,2,0:T(2,128)S(1)}, s32[1,128,2]{1,2,0:T(2,128)}, u32[]{:S(2)}) copy-start(s32[1,128,2]{1,2,0:T(2,128)} %param.44) | copy-start | bytes 3076
  49.0 28.2 %copy-start.11 = (bf16[1,128,2048]{2,1,0:T(8,128)(2,1)S(1)}, bf16[1,128,2048]{2,1,0:T(8,128)(2,1)}, u32[]{:S(2)}) copy-start(bf16[1,128,2048]{2,1,0:T(8,128)(2,1)} %param.25) | copy-start | bytes 1572868
  49.0 28.2 %copy-start.12 = (bf16[1,128,2048]{2,1,0:T(8,128)(2,1)S(1)}, bf16[1,128,2048]{2,1,0:T(8,128)(2,1)}, u32[]{:S(2)}) copy-start(bf16[1,128,2048]{2,1,0:T(8,128)(2,1)} %param.23) | copy-start | bytes 1572868
  49.0 28.2 %copy-start.16 = (f32[2048]{0:T(1024)S(1)}, f32[2048]{0:T(1024)}, u32[]{:S(2)}) copy-start(f32[2048]{0:T(1024)} %param.35) | copy-start | bytes 24580
  49.0 28.2 %copy-start.17 = (f32[2048]{0:T(1024)S(1)}, f32[2048]{0:T(1024)}, u32[]{:S(2)}) copy-start(f32[2048]{0:T(1024)} %param.37) | copy-start | bytes 24580
  55.9 21.3 %all-to-all-start.1 = ((bf16[8,128,256]{2,1,0:T(8,128)(2,1)}), bf16[8,128,256]{2,1,0:T(8,128)(2,1)S(1)}, u32[]{:S(2)}, u32[]{:S(2)}) async-start(bf16[8,128,256]{2,1,0:T(8,128)(2,1)} %scan.1), calls=%async_computation.1 | async-start | bytes 1048576 | tf_op jit(solution)/shard_map/all_to_all | solution.py:300
  82.5 0.8 copy-start.6
  83.3 52.1 %copy-start.4 = (bf16[128,2048]{1,0:T(8,128)(2,1)}, bf16[128,2048]{1,0:T(8,128)(2,1)S(1)}, u32[]{:S(2)}) copy-start(bf16[128,2048]{1,0:T(8,128)(2,1)S(1)} %get-tuple-element.10.mixed_ref) | copy-start | bytes 1572868
  141.8 1.4 copy-start
  143.2 3.7 %copy-start.22 = (f32[1,128,2]{1,2,0:T(2,128)S(1)}, f32[1,128,2]{1,2,0:T(2,128)}, u32[]{:S(2)}) copy-start(f32[1,128,2]{1,2,0:T(2,128)} %param.45) | copy-start | bytes 3076
  143.2 52.4 %all-to-all-start.3 = ((bf16[32,16,2048]{2,1,0:T(8,128)(2,1)}), bf16[32,16,2048]{2,1,0:T(8,128)(2,1)S(1)}, u32[]{:S(2)}, u32[]{:S(2)}) async-start(bf16[32,16,2048]{2,1,0:T(8,128)(2,1)} %bitcast.28), calls=%async_computation.3 | async-start | bytes 4194304 | tf_op jit(solution)/shard_map/all_to_all | solution.py:363
  147.0 1.6 copy-start.1
  148.6 1.6 copy-start.2
  150.2 1.6 copy-start.3
  151.7 1.0 copy-start.5
  152.8 1.0 copy-start.7

commit v2 on v1

v2 whole, which is shorter than its diff:
```python
import functools

import jax
import jax.numpy as jnp
from jax import lax
from jax.experimental import pallas as pl
from jax.experimental.pallas import tpu as pltpu
from jax.sharding import PartitionSpec as P


HEAD_DIM = 64
STATE = 128
EPS = 1e-06
HIGH = lax.Precision.HIGHEST
F32 = jnp.float32
BF16 = jnp.bfloat16
EXTRA = 8
TOP = 2
SP = ("half", "sub")
MIB = 1 << 20


def dot(a, b, ca, cb, precision=None):
    return lax.dot_general(
        a, b, (((ca,), (cb,)), ((), ())), preferred_element_type=F32, precision=precision
    )


def iota(shape, axis):
    return lax.broadcasted_iota(jnp.int32, shape, axis)


def silu(v):
    return v / (1.0 + jnp.exp(-v))


def vmem(limit):
    return pltpu.CompilerParams(vmem_limit_bytes=limit * MIB)


def cost(flops, nbytes):
    return pl.CostEstimate(flops=flops, bytes_accessed=nbytes, transcendentals=0)


def tail_kernel(x_ref, b_ref, c_ref, out_ref, sem):
    copies = []
    start = 0
    rows = out_ref.shape[0]
    for i, ref in enumerate((x_ref, b_ref, c_ref)):
        size = ref.shape[1]
        copies.append(
            pltpu.make_async_copy(
                ref.at[pl.ds(ref.shape[0] - rows, rows), :],
                out_ref.at[:, pl.ds(start, size)],
                sem.at[i],
            )
        )
        copies[-1].start()
        start += size
    for copy in copies:
        copy.wait()


def conv_silu(rows_in, tail, taps, rows_ref):
    tokens = rows_in.shape[0]
    rows_ref[0:8] = tail.astype(F32)
    rows_ref[8 : 8 + tokens] = rows_in.astype(F32)
    taps = taps.astype(F32)
    act = rows_ref[8 : 8 + tokens] * taps[3:4]
    for k in range(3):
        act = act + rows_ref[5 + k : 5 + k + tokens] * taps[k : k + 1]
    return silu(act)


def decays(s_ref, bias_ref, dlog_ref):
    heads, tokens = s_ref.shape
    same = iota((heads, heads), 0) == iota((heads, heads), 1)
    bias, dlog = (
        jnp.sum(jnp.where(same, ref[...], 0.0), axis=1, keepdims=True)
        for ref in (bias_ref, dlog_ref)
    )
    pre = s_ref[...].astype(F32) + bias
    step = jnp.maximum(pre, 0.0) + jnp.log1p(jnp.exp(-jnp.abs(pre)))
    upper = (iota((tokens, tokens), 0) <= iota((tokens, tokens), 1)).astype(F32)
    cum = dot(step * -jnp.exp(dlog), upper, 1, 0, HIGH)
    return step, cum, cum[:, tokens - 1 : tokens]


def spread(v, inner):
    heads = v.shape[0]
    a = v.astype(BF16)
    rest = v - a.astype(F32)
    b = rest.astype(BF16)
    c = (rest - b.astype(F32)).astype(BF16)
    own = (iota((heads, inner), 0) == iota((heads, inner), 1) // HEAD_DIM).astype(BF16)
    return dot(jnp.concatenate([a, b, c], axis=0), jnp.concatenate([own] * 3, axis=0), 0, 0)


def state_kernel(
    s_ref, bias_ref, dlog_ref, tail_ref, wx_ref, wb_ref, x_ref, b_ref, out_ref, rx_ref, rb_ref
):
    inner = x_ref.shape[1]
    ways = out_ref.shape[0]
    rows = out_ref.shape[1] - EXTRA
    local = rows // HEAD_DIM
    span = inner // (b_ref.shape[1] // STATE)
    step, cum, total = decays(s_ref, bias_ref, dlog_ref)
    wide = spread(step * jnp.exp(total - cum), inner)
    fade = jnp.exp(jnp.broadcast_to(total, (total.shape[0], STATE)))
    high = fade.astype(BF16).astype(F32)
    low = fade - high
    bm = conv_silu(b_ref[...], tail_ref[:, inner : inner + b_ref.shape[1]], wb_ref[...], rb_ref)
    bm = bm.astype(BF16)
    xs = conv_silu(x_ref[...], tail_ref[:, :inner], wx_ref[...], rx_ref)
    xw = (xs * wide).astype(BF16)
    blank = jnp.zeros((EXTRA // 2 - local, STATE), F32)
    for d in range(ways):
        g = d * rows // span
        st = dot(xw[:, d * rows : (d + 1) * rows], bm[:, g * STATE : (g + 1) * STATE], 0, 0)
        out_ref[d, 0:rows, :] = st.astype(BF16)
        own = slice(d * local, (d + 1) * local)
        parts = [high[own], low[own]]
        if local < EXTRA // 2:
            parts = [high[own], blank, low[own], blank]
        out_ref[d, rows : rows + EXTRA, :] = jnp.concatenate(parts, axis=0).astype(BF16)


def prefix_kernel(in_hbm, out_hbm, in_ref, out_ref, sem_in, sem_out):
    ways, rows, _ = out_ref.shape
    gets = [pltpu.make_async_copy(in_hbm.at[j], in_ref.at[j], sem_in.at[j]) for j in range(ways)]
    puts = [pltpu.make_async_copy(out_ref.at[j], out_hbm.at[j], sem_out.at[j]) for j in range(ways)]
    for get in gets:
        get.start()
    state = jnp.zeros((rows, STATE), F32)
    for j in range(ways):
        gets[j].wait()
        fade = in_ref[j, rows : rows + EXTRA, :].astype(F32)
        old = jnp.concatenate(
            [
                state[h * HEAD_DIM : (h + 1) * HEAD_DIM]
                * (fade[h : h + 1] + fade[h + EXTRA // 2 : h + 1 + EXTRA // 2])
                for h in range(rows // HEAD_DIM)
            ],
            axis=0,
        )
        out_ref[j] = old.astype(BF16)
        puts[j].start()
        state = old + in_ref[j, 0:rows, :].astype(F32)
    for put in puts:
        put.wait()


def inner_kernel(
    s_ref, bias_ref, dlog_ref, skip_ref, tail_ref, wx_ref, wb_ref, wc_ref, x_ref, b_ref, c_ref,
    y_ref, grow_ref, cm_ref, rx_ref, rb_ref,
):
    tokens, inner = x_ref.shape
    heads = s_ref.shape[0]
    narrow = b_ref.shape[1]
    groups = narrow // STATE
    span = inner // groups
    step, cum, total = decays(s_ref, bias_ref, dlog_ref)
    wide = spread(step * jnp.exp(total - cum), inner)
    grow = spread(jnp.exp(cum - total), inner)
    grow_ref[...] = grow
    own = (iota((heads, inner), 0) == iota((heads, inner), 1) // HEAD_DIM).astype(F32)
    skip = dot(skip_ref[...], own, 1, 0, HIGH)
    bm = conv_silu(b_ref[...], tail_ref[:, inner : inner + narrow], wb_ref[...], rb_ref)
    bm = bm.astype(BF16)
    cm = conv_silu(c_ref[...], tail_ref[:, inner + narrow :], wc_ref[...], rb_ref).astype(BF16)
    cm_ref[...] = cm
    xs = conv_silu(x_ref[...], tail_ref[:, :inner], wx_ref[...], rx_ref)
    xw = (xs * wide).astype(BF16)
    lower = iota((tokens, tokens), 0) >= iota((tokens, tokens), 1)
    for g in range(groups):
        n = slice(g * STATE, (g + 1) * STATE)
        at = slice(g * span, (g + 1) * span)
        scores = jnp.where(lower, dot(cm[:, n], bm[:, n], 1, 1), 0.0).astype(BF16)
        y_ref[:, at] = grow[:, at] * dot(scores, xw[:, at], 1, 0) + skip[:, at] * xs[:, at]


def slot_of(meta, experts, slots):
    tokens = meta.shape[1]
    top = TOP
    same = (iota((tokens, tokens), 0) == iota((tokens, tokens), 1)).astype(F32)
    cols = dot(same, meta, 1, 1, HIGH)
    lane = iota((tokens, experts), 1).astype(F32)
    hot = [lane == cols[:, k : k + 1] for k in range(top)]
    count = sum(h.astype(F32) for h in hot).astype(BF16)
    before = (iota((tokens, tokens), 0) > iota((tokens, tokens), 1)).astype(BF16)
    ahead = dot(before, count, 1, 0)
    out = []
    for k in range(top):
        rank = jnp.sum(jnp.where(hot[k], ahead, 0.0), axis=1, keepdims=True)
        out.append((cols[:, k : k + 1] * slots + rank, cols[:, top + k : top + k + 1]))
    return out


def hits(meta, experts, slots, half, rows):
    lane = (iota((meta.shape[1], rows), 1) + half * rows).astype(F32)
    found = [lane == s for s, _ in slot_of(meta, experts, slots)]
    return functools.reduce(jnp.logical_or, found).astype(BF16)


def weighted(meta, experts, slots, half, got):
    lane = (iota((meta.shape[1], got.shape[0]), 1) + half * got.shape[0]).astype(F32)
    w = jnp.zeros(lane.shape, F32)
    for s, value in slot_of(meta, experts, slots):
        w = w + jnp.where(lane == s, value, 0.0)
    high = w.astype(BF16)
    low = (w - high.astype(F32)).astype(BF16)
    return dot(high, got, 1, 0) + dot(low, got, 1, 0)


def mix_kernel(
    blocks, experts, slots, order_ref, gain_ref, fgain_ref, meta_ref, state_in, y_in, grow_in,
    cm_in, gate_in, res_in, *refs,
):
    count = len(blocks)
    w_refs, (mixed_ref, x_ref, send_ref) = refs[:-19], refs[-19:-16]
    wbuf, state_ref, y_ref, grow_ref, cm_ref, gate_ref, res_ref = refs[-16:-9]
    acc, mbuf, xbuf, sbuf, sem_w, sem_v, sem_m, sem_x, sem_s = refs[-9:]
    per = wbuf.shape[1]
    odd = order_ref[count + 1]
    copies = []
    for i, pieces in enumerate(blocks):
        at = pl.multiple_of(order_ref[i] * per, per)
        col = pl.multiple_of(order_ref[i] * STATE, STATE)
        wide = pl.ds(at, per)
        pairs = [
            (state_in.at[wide, :], state_ref.at[i]),
            (cm_in.at[:, pl.ds(col, STATE)], cm_ref.at[i]),
            (y_in.at[:, wide], y_ref.at[i]),
            (grow_in.at[:, wide], grow_ref.at[i]),
            (gate_in.at[:, wide], gate_ref.at[i]),
        ]
        small = [pltpu.make_async_copy(a, b, sem_v.at[i, k]) for k, (a, b) in enumerate(pairs)]
        large = []
        for k, (which, row, size, side) in enumerate(pieces):
            if side is None:
                to = pl.ds(0, size)
            else:
                to = pl.ds(pl.multiple_of((odd if side == 0 else 1 - odd) * size, size), size)
            large.append(
                pltpu.make_async_copy(
                    w_refs[which].at[pl.ds(row, size), :], wbuf.at[i, to], sem_w.at[i, k]
                )
            )
        for copy in small + large:
            copy.start()
        copies.append((small, large))
    residual = pltpu.make_async_copy(res_in, res_ref, sem_v.at[count, 0])
    residual.start()
    for i in range(count):
        at = pl.multiple_of(order_ref[i] * per, per)
        for copy in copies[i][0]:
            copy.wait()
        v = y_ref[i] + grow_ref[i] * dot(cm_ref[i], state_ref[i], 1, 1)
        v = v.astype(BF16).astype(F32)
        v = v * silu(gate_ref[i].astype(F32))
        v = v * lax.rsqrt(jnp.mean(v * v, axis=1, keepdims=True) + EPS)
        v = (v * gain_ref[:, pl.ds(at, per)]).astype(BF16)
        for copy in copies[i][1]:
            copy.wait()
        part = dot(v, wbuf[i], 1, 0)
        if i == 0:
            acc[...] = part
        else:
            acc[...] += part
    residual.wait()
    mixed = (res_ref[...].astype(F32) + acc[...]).astype(BF16)
    mbuf[...] = mixed
    out_mixed = pltpu.make_async_copy(mbuf, mixed_ref, sem_m)
    out_mixed.start()
    m = mixed.astype(F32)
    x = m * lax.rsqrt(jnp.mean(m * m, axis=1, keepdims=True) + EPS) * fgain_ref[...]
    x = x.astype(BF16)
    xbuf[...] = x
    out_x = pltpu.make_async_copy(xbuf, x_ref, sem_x)
    out_x.start()
    place_rows(
        hits(meta_ref[...], experts, slots, order_ref[count], send_ref.shape[0]),
        x, sbuf, send_ref, sem_s,
    )
    out_x.wait()
    out_mixed.wait()


def place_rows(hit, x, sbuf, send_ref, sem):
    pieces = sem.shape[0]
    rows = send_ref.shape[0] // pieces
    copies = []
    for i in range(pieces):
        part = slice(i * rows, (i + 1) * rows)
        sbuf[part] = dot(hit[:, part], x, 0, 0).astype(BF16)
        copies.append(
            pltpu.make_async_copy(
                sbuf.at[pl.ds(i * rows, rows)], send_ref.at[pl.ds(i * rows, rows)], sem.at[i]
            )
        )
        copies[-1].start()
    for copy in copies:
        copy.wait()


def relay_kernel(experts, slots, half_ref, meta_ref, x_in, send_ref, x_ref, sbuf, sem_x, sem):
    copy = pltpu.make_async_copy(x_in, x_ref, sem_x)
    copy.start()
    hit = hits(meta_ref[...], experts, slots, half_ref[0], send_ref.shape[0])
    copy.wait()
    place_rows(hit, x_ref[...], sbuf, send_ref, sem)


def shared_kernel(x_in, mixed_in, wg_in, wu_in, wd_in, out_ref, x_ref, m_ref, wg, wu, wd, sem):
    copies = [
        pltpu.make_async_copy(src, dst, sem.at[i])
        for i, (src, dst) in enumerate(
            ((x_in, x_ref), (wg_in, wg), (wu_in, wu), (wd_in, wd), (mixed_in, m_ref))
        )
    ]
    for copy in copies:
        copy.start()
    for copy in copies[:3]:
        copy.wait()
    x = x_ref[...]
    h = (silu(dot(x, wg[...], 1, 0)) * dot(x, wu[...], 1, 0)).astype(BF16)
    for copy in copies[3:]:
        copy.wait()
    out_ref[...] = m_ref[...].astype(F32) + dot(h, wd[...], 1, 0)


def expert_kernel(x_ref, wg_ref, wu_ref, wd_ref, out_ref, acc, obuf, sem):
    e = pl.program_id(0)
    j = pl.program_id(1)
    x = x_ref[...]
    h = (silu(dot(x, wg_ref[0], 1, 0)) * dot(x, wu_ref[0], 1, 0)).astype(BF16)
    part = dot(h, wd_ref[0], 1, 0)

    @pl.when(j == 0)
    def _():
        acc[...] = part

    @pl.when(j == pl.num_programs(1) - 1)
    def _():
        pieces = sem.shape[0]
        rows = obuf.shape[0] // pieces
        copies = []
        for i in range(pieces):
            at = slice(i * rows, (i + 1) * rows)
            obuf[at] = (acc[at] + part[at]).astype(BF16)
            copies.append(
                pltpu.make_async_copy(
                    obuf.at[pl.ds(i * rows, rows)], out_ref.at[e, pl.ds(i * rows, rows)], sem.at[i]
                )
            )
            copies[-1].start()
        for copy in copies:
            copy.wait()


def part_kernel(experts, slots, half_ref, meta_ref, got_ref, out_ref, obuf, sem):
    obuf[...] = weighted(meta_ref[...], experts, slots, half_ref[0], got_ref[...]).astype(BF16)
    copy = pltpu.make_async_copy(obuf, out_ref, sem)
    copy.start()
    copy.wait()


def combine_kernel(experts, slots, half_ref, meta_ref, got_ref, base_ref, other_ref, out_ref):
    own = weighted(meta_ref[...], experts, slots, half_ref[0], got_ref[...])
    out_ref[...] = (base_ref[...] + own + other_ref[...].astype(F32)).astype(BF16)


def gather_rows(w, ways, span):
    if ways == 4 and w.shape[0] == 2 * span and lax.axis_size("sub") % 2 == 0:
        me = lax.axis_index("dp")
        odd = lax.rem(lax.axis_index("sub"), 2).astype(jnp.int32)
        part = span // 2
        over = [(j, j ^ 2) for j in range(4)]
        core = [(j, j ^ 1) for j in range(4)]
        flip = [(j, j ^ 1) for j in range(lax.axis_size("sub"))]
        xa = lax.ppermute(lax.dynamic_slice_in_dim(w, odd * part, part, 0), "dp", over)
        xb = lax.ppermute(w[span:], "dp", over)
        ya = lax.ppermute(xa, "sub", flip)
        beside = lax.ppermute(w, "dp", core)
        fa = lax.ppermute(xa, "dp", core)
        fy = lax.ppermute(ya, "dp", core)
        fb = lax.ppermute(xb, "dp", core)
        arrays = [w, beside, xa, ya, xb, fa, fy, fb]
        blocks = [[(i, k * span, span, None)] for i in range(2) for k in range(2)]
        for i in (2, 5):
            blocks.append([(i, 0, part, 0), (i + 1, 0, part, 1)])
            blocks.append([(i + 2, 0, span, None)])
        order = [(me ^ i) * 2 + k for i in range(4) for k in range(2)]
        return arrays, blocks, order, odd
    whole = lax.all_gather(w, "dp", axis=0, tiled=True)
    count = whole.shape[0] // span
    blocks = [[(0, g * span, span, None)] for g in range(count)]
    return [whole], blocks, list(range(count)), jnp.int32(0)


def layer(
    residual, head_input, gate_input, b_input, c_input, step_input, conv_weight, conv_b_weight,
    conv_c_weight, step_bias, decay_log, skip, norm_gain, out_weight, ffn_gain, shared_gate,
    shared_up, shared_down, expert_gate, expert_up, expert_down, routes, route_weights,
):
    _, tokens, inner = head_input.shape
    features = residual.shape[2]
    heads = step_input.shape[2]
    groups = b_input.shape[2] // STATE
    top = routes.shape[2]
    ways = lax.axis_size(SP)
    ways_dp = lax.axis_size("dp")
    experts = ways * ways_dp * expert_gate.shape[0]
    slots = 2 * tokens * top // experts
    local = heads // ways
    width = local * HEAD_DIM
    span = inner // groups

    ws, blocks, order, odd = gather_rows(out_weight, ways_dp, span)
    half = lax.axis_index("half").astype(jnp.int32)
    order = jnp.stack([jnp.asarray(o, jnp.int32) for o in order + [half, odd]])
    meta = jnp.concatenate([routes[0].T.astype(F32), route_weights[0].T], axis=0)
    meta = jnp.concatenate([meta, jnp.zeros((8 - 2 * top, tokens), F32)], axis=0)
    mirror = [(0, 1), (1, 0)]
    meta_far = lax.ppermute(meta, "half", mirror)
    rows = experts * slots // 2
    pieces = 4

    hbm = pl.BlockSpec(memory_space=pltpu.HBM)
    vm = pl.BlockSpec(memory_space=pltpu.VMEM)
    x_in, b_in, c_in = head_input[0], b_input[0], c_input[0]
    turned = (step_input[0].T, step_bias[None], decay_log[None])
    tail = pl.pallas_call(
        tail_kernel,
        out_shape=jax.ShapeDtypeStruct((8, inner + 2 * b_in.shape[1]), BF16),
        in_specs=[hbm] * 3,
        out_specs=vm,
        scratch_shapes=[pltpu.SemaphoreType.DMA((3,))],
        compiler_params=vmem(60),
        cost_estimate=cost(1 << 10, 1 << 17),
        name="tails",
    )(x_in, b_in, c_in)
    tail = lax.ppermute(tail, SP, [(i, i + 1) for i in range(ways - 1)])
    fresh = pl.pallas_call(
        state_kernel,
        out_shape=jax.ShapeDtypeStruct((ways, width + EXTRA, STATE), BF16),
        in_specs=[vm] * 8,
        out_specs=vm,
        scratch_shapes=[
            pltpu.VMEM((8 + tokens, inner), F32),
            pltpu.VMEM((8 + tokens, b_in.shape[1]), F32),
        ],
        compiler_params=vmem(60),
        cost_estimate=cost(1 << 30, 4 * MIB),
        name="states",
    )(*turned, tail, conv_weight, conv_b_weight, x_in, b_in)
    fresh = lax.all_to_all(fresh, SP, split_axis=0, concat_axis=0, tiled=True)
    y, grow, cm = pl.pallas_call(
        inner_kernel,
        out_shape=(
            jax.ShapeDtypeStruct((tokens, inner), F32),
            jax.ShapeDtypeStruct((tokens, inner), F32),
            jax.ShapeDtypeStruct((tokens, b_in.shape[1]), BF16),
        ),
        in_specs=[vm] * 11,
        out_specs=(vm,) * 3,
        scratch_shapes=[
            pltpu.VMEM((8 + tokens, inner), F32),
            pltpu.VMEM((8 + tokens, b_in.shape[1]), F32),
        ],
        compiler_params=vmem(60),
        cost_estimate=cost(2 << 30, 8 * MIB),
        name="within",
    )(
        *turned, skip[None], tail, conv_weight, conv_b_weight, conv_c_weight, x_in, b_in, c_in
    )
    entering = pl.pallas_call(
        prefix_kernel,
        out_shape=jax.ShapeDtypeStruct((ways, width, STATE), BF16),
        in_specs=[hbm],
        out_specs=hbm,
        scratch_shapes=[
            pltpu.VMEM(fresh.shape, BF16),
            pltpu.VMEM((ways, width, STATE), BF16),
            pltpu.SemaphoreType.DMA((ways,)),
            pltpu.SemaphoreType.DMA((ways,)),
        ],
        compiler_params=vmem(60),
        cost_estimate=cost(1 << 26, 2 * MIB),
        name="prefix",
    )(fresh)
    entering = lax.all_to_all(entering, SP, split_axis=0, concat_axis=0, tiled=True)
    entering = entering.reshape(inner, STATE)

    sm = pl.BlockSpec(memory_space=pltpu.SMEM)
    mixed, x, send = pl.pallas_call(
        functools.partial(mix_kernel, blocks, experts, slots),
        out_shape=(
            jax.ShapeDtypeStruct((tokens, features), BF16),
            jax.ShapeDtypeStruct((tokens, features), BF16),
            jax.ShapeDtypeStruct((rows, features), BF16),
        ),
        in_specs=[sm] + [vm] * 3 + [hbm] * (6 + len(ws)),
        out_specs=(hbm, hbm, hbm),
        scratch_shapes=[
            pltpu.VMEM((groups, span, features), BF16),
            pltpu.VMEM((groups, span, STATE), BF16),
            pltpu.VMEM((groups, tokens, span), F32),
            pltpu.VMEM((groups, tokens, span), F32),
            pltpu.VMEM((groups, tokens, STATE), BF16),
            pltpu.VMEM((groups, tokens, span), BF16),
            pltpu.VMEM((tokens, features), BF16),
            pltpu.VMEM((tokens, features), F32),
            pltpu.VMEM((tokens, features), BF16),
            pltpu.VMEM((tokens, features), BF16),
            pltpu.VMEM((rows, features), BF16),
            pltpu.SemaphoreType.DMA((groups, 2)),
            pltpu.SemaphoreType.DMA((groups + 1, 5)),
            pltpu.SemaphoreType.DMA,
            pltpu.SemaphoreType.DMA,
            pltpu.SemaphoreType.DMA((pieces,)),
        ],
        compiler_params=vmem(62),
        cost_estimate=cost(3 << 30, 16 * MIB),
        name="mix",
    )(
        order, norm_gain[None], ffn_gain[None], meta, entering, y, grow, cm, gate_input[0],
        residual[0], *ws,
    )

    x_far = lax.ppermute(x, "half", mirror)
    group = ("sub", "dp")

    def exchange(v):
        v = v.reshape(-1, slots, features)
        return lax.all_to_all(v, group, split_axis=0, concat_axis=0, tiled=True)

    own = expert_gate.shape[0]
    ff = expert_gate.shape[2]
    bn = ff // 2

    def serve(arrived):
        if own > 1:
            arrived = arrived.reshape(-1, own, slots, features).swapaxes(0, 1)
        arrived = arrived.reshape(own, -1, features)
        m = arrived.shape[1]
        done = pl.pallas_call(
            expert_kernel,
            out_shape=jax.ShapeDtypeStruct((own, m, features), BF16),
            grid=(own, ff // bn),
            in_specs=[
                pl.BlockSpec((None, m, features), lambda e, j: (e, 0, 0)),
                pl.BlockSpec((1, features, bn), lambda e, j: (e, 0, j)),
                pl.BlockSpec((1, features, bn), lambda e, j: (e, 0, j)),
                pl.BlockSpec((1, bn, features), lambda e, j: (e, j, 0)),
            ],
            out_specs=hbm,
            scratch_shapes=[
                pltpu.VMEM((m, features), F32),
                pltpu.VMEM((m, features), BF16),
                pltpu.SemaphoreType.DMA((pieces,)),
            ],
            compiler_params=vmem(48),
            cost_estimate=cost(2 << 30, 8 * MIB),
            name="experts",
        )(arrived, expert_gate, expert_up, expert_down)
        if own > 1:
            done = done.reshape(own, -1, slots, features).swapaxes(0, 1)
        return done

    near = exchange(send)
    base = pl.pallas_call(
        shared_kernel,
        out_shape=jax.ShapeDtypeStruct((tokens, features), F32),
        in_specs=[hbm] * 5,
        out_specs=vm,
        scratch_shapes=[
            pltpu.VMEM(v.shape, BF16) for v in (x, mixed, shared_gate, shared_up, shared_down)
        ]
        + [pltpu.SemaphoreType.DMA((5,))],
        compiler_params=vmem(62),
        cost_estimate=cost(1 << 30, 8 * MIB),
        name="shared",
    )(x, mixed, shared_gate, shared_up, shared_down)
    near = serve(near)
    relay = pl.pallas_call(
        functools.partial(relay_kernel, experts, slots),
        out_shape=jax.ShapeDtypeStruct((rows, features), BF16),
        in_specs=[sm, vm, hbm],
        out_specs=hbm,
        scratch_shapes=[
            pltpu.VMEM((tokens, features), BF16),
            pltpu.VMEM((rows, features), BF16),
            pltpu.SemaphoreType.DMA,
            pltpu.SemaphoreType.DMA((pieces,)),
        ],
        compiler_params=vmem(32),
        cost_estimate=cost(1 << 28, 3 * MIB),
        name="relay",
    )(half[None], meta_far, x_far)
    far = exchange(relay)
    far = serve(far)
    far = exchange(far)
    part = pl.pallas_call(
        functools.partial(part_kernel, experts, slots),
        out_shape=jax.ShapeDtypeStruct((tokens, features), BF16),
        in_specs=[sm, vm, vm],
        out_specs=hbm,
        scratch_shapes=[pltpu.VMEM((tokens, features), BF16), pltpu.SemaphoreType.DMA],
        compiler_params=vmem(32),
        cost_estimate=cost(1 << 29, 3 * MIB),
        name="part",
    )(half[None], meta_far, far.reshape(rows, features))
    other = lax.ppermute(part, "half", mirror)
    near = exchange(near)
    out = pl.pallas_call(
        functools.partial(combine_kernel, experts, slots),
        out_shape=jax.ShapeDtypeStruct((tokens, features), BF16),
        in_specs=[sm] + [vm] * 4,
        out_specs=vm,
        compiler_params=vmem(32),
        cost_estimate=cost(1 << 29, 4 * MIB),
        name="combine",
    )(half[None], meta, near.reshape(rows, features), base, other)
    return out[None]


def solution(mesh):
    ways, ways_dp = mesh.devices.shape
    mesh = jax.sharding.Mesh(mesh.devices.reshape(2, ways // 2, ways_dp), SP + ("dp",))
    tok = P("dp", SP, None)
    exp = P(SP + ("dp",), None, None)
    return jax.shard_map(
        layer,
        mesh=mesh,
        in_specs=(tok,) * 6
        + (P(),) * 7
        + (P("dp", None),)
        + (P(),) * 4
        + (exp,) * 3
        + (tok, tok),
        out_specs=tok,
        check_vma=False,
    )
```

time: 198 us -> 204 us (1.030)
  blocking collectives: 52.1 us -> 20.3 us
  Pallas kernels: 22.8 us -> 41.8 us
  starting transfers between devices: 18.6 us -> 36.6 us
  waiting for transfers between devices: 90.7 us -> 94.2 us
  local copies, waits for them, and re-layouts: 13.1 us -> 9.67 us
    all_to_all x1, blocking collectives: 52.1 us -> 20.3 us  [exchange(): return lax.all_to_all(v, group, split_axis=0, concat_axis=0, tiled=True)]
    ppermute x3 -> x11, waiting for transfers between devices: 35.1 us -> 55.1 us  [the longest x1 23.2 us: gather_rows(): lax.ppermute(lax.dynamic_slice_in_dim(w, odd * part, part, 0), 'dp', over)]
    pallas_call x6 -> x11, Pallas kernels: 22.8 us -> 41.8 us  [the longest x1 9.21 us: layer(): pl.pallas_call(functools.partial(mix_kernel, blocks, experts, slots), out...]
    all_to_all x3 -> x5, waiting for transfers between devices: 55.6 us -> 39.1 us  [the longest x3 35.2 us: exchange(): return lax.all_to_all(v, group, split_axis=0, concat_axis=0, tiled=True)]
    ppermute x3 -> x11, starting transfers between devices: 2.97 us -> 14.9 us  [the longest x1 4.9 us: layer(): tail = lax.ppermute(tail, SP, [(i, i + 1) for i in range(ways - 1)])]
    unnamed x49 -> x26, local copies, waits for them, and re-layouts: 13 us -> 6.61 us
    all_to_all x3 -> x5, starting transfers between devices: 15.6 us -> 21.7 us  [the longest x3 11.8 us: exchange(): return lax.all_to_all(v, group, split_axis=0, concat_axis=0, tiled=True)]
    slice x0 -> x1, local copies, waits for them, and re-layouts: none -> 2.31 us  [gather_rows(): xb = lax.ppermute(w[span:], 'dp', over)]
  transfers between devices with their start and end apart: 6 -> 16, of which waited for: 3 -> 8; matrix products, arithmetic and copies ran while one was open for 1% -> 2% of each run, Pallas kernels for 5% -> 13%
where the time goes in v2:
time: 204 us
  waiting for transfers between devices  94.2 us (46%)
  Pallas kernels  41.8 us (20%)
  starting transfers between devices  36.6 us (18%)
  blocking collectives  20.3 us (10%)
  local copies, waits for them, and re-layouts  9.67 us (5%)
    all_to_all x3, waiting for transfers between devices, exchange(): return lax.all_to_all(v, group, split_axis=0, concat_axis=0, tiled=True)  35.2 us
    ppermute x1, waiting for transfers between devices, gather_rows(): lax.ppermute(lax.dynamic_slice_in_dim(w, odd * part, part, 0), 'dp', over)  23.2 us
    ppermute x1, waiting for transfers between devices, layer(): meta_far = lax.ppermute(meta, 'half', mirror)  22.4 us
    all_to_all x1, blocking collectives, exchange(): return lax.all_to_all(v, group, split_axis=0, concat_axis=0, tiled=True)  20.3 us
    all_to_all x3, starting transfers between devices, exchange(): return lax.all_to_all(v, group, split_axis=0, concat_axis=0, tiled=True)  11.8 us
    pallas_call x1, Pallas kernels, layer(): pl.pallas_call(functools.partial(mix_kernel, blocks, experts, slots), out...  9.21 us
    pallas_call x2, Pallas kernels, serve(): pl.pallas_call(expert_kernel, out_shape=jax.ShapeDtypeStruct((own, m, fea...  8.44 us
    unnamed x26, local copies, waits for them, and re-layouts  6.61 us
  transfers between devices with their start and end apart: 16, of which 8 were waited for; matrix products, arithmetic and copies ran while one was open for 2% of the time, Pallas kernels for 13%

profile of v2, /device:TPU:0, one launch (start us, length us, event | category | flops | bytes accessed | tf_op | source)
XLA Modules:
  0.0 203.6 jit_solution(9082491427911059888)
XLA Ops:
  0.0 1.6 tails.1
  1.6 4.9 %collective-permute-start = (bf16[8,4096]{1,0:T(8,128)(2,1)}, bf16[8,4096]{1,0:T(8,128)(2,1)S(1)}, u32[]{:S(2)}, u32[]{:S(2)}) collective-permute-start(bf16[8,4096]{1,0:T(8,128)(2,1)} %tails.1), channel_id=1, source_target_pairs={{0,4},{4,8},{8,12},{12,16},{16,20},{20,24},{24,28},{1,5},{5,9},{9,... | collective-permute-start | bytes 196616 | tf_op jit(solution)/shard_map/ppermute | solution.py:443
  6.5 2.3 %slice.3 = bf16[256,2048]{1,0:T(8,128)(2,1)} slice(bf16[512,2048]{1,0:T(8,128)(2,1)} %refs_0_.1), slice={[256:512], [0:2048]} | slice | bytes 2097152 | tf_op jit(solution)/shard_map/slice | solution.py:382
  8.8 1.5 collective-permute-start.4
  10.3 0.0 copy-done.6
  10.3 0.0 collective-permute-start.1
  10.3 0.0 collective-permute-done.tail_ref
  10.3 0.0 copy-start.12
  10.3 0.6 copy-done.12
  10.9 4.0 %states.1 = bf16[8,264,128]{2,1,0:T(8,128)(2,1)} custom-call(bf16[32,128]{1,0:T(8,128)(2,1)} %bitcast.61, f32[1,32]{1,0:T(1,128)} %bitcast.63, f32[1,32]{1,0:T(1,128)} %bitcast.65, bf16[8,4096]{1,0:T(8,128)(2,1)} %copy-done.12, bf16[4,2048]{1,0:T(4,128)(2,1)} %wx_ref.3, bf16[4,1024]{1,0:T(4,128)(2,1)} %wb_ref.3, bf16[128,2048]{1,0:T(8,128)(2,1)} %bitcast.51, ...), custom_call_target="tpu_custom_call" | custom-call | flops 1073741824 | bytes 4194304 | tf_op jit(solution)/shard_map/states/pallas_call | solution.py:444
  14.9 5.1 %all-to-all-start = ((bf16[8,264,128]{2,1,0:T(8,128)(2,1)}), bf16[8,264,128]{2,1,0:T(8,128)(2,1)S(1)}, u32[]{:S(2)}, u32[]{:S(2)}) async-start(bf16[8,264,128]{2,1,0:T(8,128)(2,1)} %states.1), calls=%async_computation | async-start | bytes 1081344 | tf_op jit(solution)/shard_map/all_to_all | solution.py:457
  20.1 1.6 collective-permute-start.2
  21.6 23.2 %collective-permute-done.2.refs_2_ = bf16[128,2048]{1,0:T(8,128)(2,1)S(1)} collective-permute-done((bf16[128,2048]{1,0:T(8,128)(2,1)S(1)}, bf16[128,2048]{1,0:T(8,128)(2,1)S(1)}, u32[]{:S(2)}, u32[]{:S(2)}) %collective-permute-start.2) | collective-permute-done | bytes 524320 | tf_op jit(solution)/shard_map/ppermute | solution.py:381
  44.9 1.5 collective-permute-start.3
  46.4 0.0 collective-permute-done.4.refs_4_
  46.4 0.0 collective-permute-start.7
  46.4 0.0 all-to-all-done.in_hbm
  46.4 0.0 copy-start.7
  46.4 0.8 copy-done.7
  47.2 1.9 prefix.1
  49.1 4.8 %all-to-all-start.1 = ((bf16[8,256,128]{2,1,0:T(8,128)(2,1)}), bf16[8,256,128]{2,1,0:T(8,128)(2,1)S(1)}, u32[]{:S(2)}, u32[]{:S(2)}) async-start(bf16[8,256,128]{2,1,0:T(8,128)(2,1)} %prefix.1), calls=%async_computation.1 | async-start | bytes 1048576 | tf_op jit(solution)/shard_map/all_to_all | solution.py:492
  53.9 0.2 collective-permute-start.5
  54.2 4.4 %collective-permute-done.3.refs_3_ = bf16[128,2048]{1,0:T(8,128)(2,1)} collective-permute-done((bf16[128,2048]{1,0:T(8,128)(2,1)S(1)}, bf16[128,2048]{1,0:T(8,128)(2,1)}, u32[]{:S(2)}, u32[]{:S(2)}) %collective-permute-start.3) | collective-permute-done | bytes 524320 | tf_op jit(solution)/shard_map/ppermute | solution.py:383
  58.6 0.0 collective-permute-start.6
  58.6 0.0 copy-done.10
  58.6 0.1 pad.2.clone
  58.7 0.6 stack.40.order_ref
  59.3 0.0 copy-done.11
  59.3 0.7 maximum_maximum_fusion.meta_ref
  60.0 5.2 %within.1 = (f32[128,2048]{1,0:T(8,128)}, f32[128,2048]{1,0:T(8,128)}, bf16[128,1024]{1,0:T(8,128)(2,1)}) custom-call(bf16[32,128]{1,0:T(8,128)(2,1)} %bitcast.62, f32[1,32]{1,0:T(1,128)} %bitcast.64, f32[1,32]{1,0:T(1,128)} %bitcast.66, f32[1,32]{1,0:T(1,128)} %bitcast.67, bf16[8,4096]{1,0:T(8,128)(2,1)} %copy-done.12, bf16[4,2048]{1,0:T(4,128)(2,1)} %wx_ref.3, ...), custom_call_target="tpu_custom_call" | custom-call | flops 2147483648 | bytes 8388608 | tf_op jit(solution)/shard_map/within/pallas_call | solution.py:458
  65.1 0.0 collective-permute-done.5.refs_5_
  65.1 0.0 collective-permute-done.6.refs_6_
  65.2 3.9 %all-to-all-done.1 = bf16[8,256,128]{2,1,0:T(8,128)(2,1)S(1)} async-done(((bf16[8,256,128]{2,1,0:T(8,128)(2,1)}), bf16[8,256,128]{2,1,0:T(8,128)(2,1)S(1)}, u32[]{:S(2)}, u32[]{:S(2)}) %all-to-all-start.1) | async-done | bytes 524320 | tf_op jit(solution)/shard_map/all_to_all | solution.py:492
  69.1 0.0 collective-permute-done.7.refs_7_
  69.1 0.0 collective-permute-done.1.refs_1_
  69.1 0.0 copy-done.9
  69.1 0.8 copy-done.8
  69.9 9.2 %mix.1 = (bf16[128,2048]{1,0:T(8,128)(2,1)}, bf16[128,2048]{1,0:T(8,128)(2,1)}, bf16[256,2048]{1,0:T(8,128)(2,1)}) custom-call(s32[10]{0:T(128)} %stack.40.order_ref, f32[1,2048]{1,0:T(1,128)} %bitcast.58, f32[1,2048]{1,0:T(1,128)} %bitcast.59, f32[8,128]{1,0:T(8,128)} %maximum_maximum_fusion.meta_ref, bf16[2048,128]{1,0:T(8,128)(2,1)} %bitcast.46, ...), custom_call_target="tpu_custom_call" | custom-call | flops 3221225472 | bytes 16777216 | tf_op jit(solution)/shard_map/mix/pallas_call | solution.py:496
  79.1 0.2 collective-permute-start.9
  79.3 0.0 copy-done.5
  79.3 2.8 %collective-permute-start.8 = (f32[8,128]{1,0:T(8,128)S(1)}, f32[8,128]{1,0:T(8,128)S(1)}, u32[]{:S(2)}, u32[]{:S(2)}) collective-permute-start(f32[8,128]{1,0:T(8,128)S(1)} %copy-done.5), channel_id=1, source_target_pairs={{0,16},{16,0},{1,17},{17,1},{2,18},{18,2},{3,19},{19,3},{4,20},{20... | collective-permute-start | bytes 12296 | tf_op jit(solution)/shard_map/ppermute | solution.py:425
  82.1 22.4 %collective-permute-done.8.meta_ref = f32[8,128]{1,0:T(8,128)S(1)} collective-permute-done((f32[8,128]{1,0:T(8,128)S(1)}, f32[8,128]{1,0:T(8,128)S(1)}, u32[]{:S(2)}, u32[]{:S(2)}) %collective-permute-start.8) | collective-permute-done | bytes 4128 | tf_op jit(solution)/shard_map/ppermute | solution.py:425
  104.5 0.0 collective-permute-done.9.x_in
  104.5 2.0 relay.1
  106.5 0.0 copy-start
  106.5 20.3 %all_to_all.30 = bf16[16,16,2048]{2,1,0:T(8,128)(2,1)} all-to-all(bf16[16,16,2048]{2,1,0:T(8,128)(2,1)S(1)} %bitcast.40), channel_id=1, replica_groups=mesh['half'=2,'sub'=4,'dp'=4] {'sub','dp'}, dimensions={0} | all-to-all | bytes 2097152 | tf_op jit(solution)/shard_map/all_to_all | solution.py:536
  126.8 3.7 %all-to-all-start.2 = ((bf16[16,16,2048]{2,1,0:T(8,128)(2,1)}), bf16[16,16,2048]{2,1,0:T(8,128)(2,1)S(1)}, u32[]{:S(2)}, u32[]{:S(2)}) async-start(bf16[16,16,2048]{2,1,0:T(8,128)(2,1)} %bitcast.47), calls=%async_computation.2 | async-start | bytes 2097152 | tf_op jit(solution)/shard_map/all_to_all | solution.py:536
  130.5 1.2 copy-done.3
  131.7 4.2 %experts.3 = bf16[1,256,2048]{2,1,0:T(8,128)(2,1)S(1)} custom-call(bf16[1,256,2048]{2,1,0:T(8,128)(2,1)S(1)} %bitcast.45, bf16[1,2048,512]{2,1,0:T(8,128)(2,1)S(1)} %copy-done, bf16[1,2048,512]{2,1,0:T(8,128)(2,1)} %wu_ref.3, bf16[1,512,2048]{2,1,0:T(8,128)(2,1)} %wd_ref.3), custom_call_target="tpu_custom_call" | custom-call | flops 2147483648 | bytes 8388608 | tf_op jit(solution)/shard_map/experts/pallas_call | solution.py:547
  136.0 1.0 copy-done.2
  136.9 9.7 %all-to-all-done.2 = bf16[16,16,2048]{2,1,0:T(8,128)(2,1)S(1)} async-done(((bf16[16,16,2048]{2,1,0:T(8,128)(2,1)}), bf16[16,16,2048]{2,1,0:T(8,128)(2,1)S(1)}, u32[]{:S(2)}, u32[]{:S(2)}) %all-to-all-start.2) | async-done | bytes 1048608 | tf_op jit(solution)/shard_map/all_to_all | solution.py:536
  146.6 4.5 %all-to-all-start.5 = ((bf16[16,16,2048]{2,1,0:T(8,128)(2,1)}), bf16[16,16,2048]{2,1,0:T(8,128)(2,1)}, u32[]{:S(2)}, u32[]{:S(2)}) async-start(bf16[16,16,2048]{2,1,0:T(8,128)(2,1)} %bitcast.44), calls=%async_computation.5 | async-start | bytes 2097152 | tf_op jit(solution)/shard_map/all_to_all | solution.py:536
  151.1 4.2 %experts.2 = bf16[1,256,2048]{2,1,0:T(8,128)(2,1)S(1)} custom-call(bf16[1,256,2048]{2,1,0:T(8,128)(2,1)S(1)} %bitcast.43, bf16[1,2048,512]{2,1,0:T(8,128)(2,1)S(1)} %copy-done, bf16[1,2048,512]{2,1,0:T(8,128)(2,1)} %wu_ref.3, bf16[1,512,2048]{2,1,0:T(8,128)(2,1)} %wd_ref.3), custom_call_target="tpu_custom_call" | custom-call | flops 2147483648 | bytes 8388608 | tf_op jit(solution)/shard_map/experts/pallas_call | solution.py:547
  155.4 0.0 copy-start.1
  155.4 1.0 copy-done.1
  156.3 10.7 %all-to-all-done.5 = bf16[16,16,2048]{2,1,0:T(8,128)(2,1)} async-done(((bf16[16,16,2048]{2,1,0:T(8,128)(2,1)}), bf16[16,16,2048]{2,1,0:T(8,128)(2,1)}, u32[]{:S(2)}, u32[]{:S(2)}) %all-to-all-start.5) | async-done | bytes 1048608 | tf_op jit(solution)/shard_map/all_to_all | solution.py:536
  167.1 3.7 %all-to-all-start.3 = ((bf16[16,16,2048]{2,1,0:T(8,128)(2,1)}), bf16[16,16,2048]{2,1,0:T(8,128)(2,1)S(1)}, u32[]{:S(2)}, u32[]{:S(2)}) async-start(bf16[16,16,2048]{2,1,0:T(8,128)(2,1)} %bitcast.42), calls=%async_computation.3 | async-start | bytes 2097152 | tf_op jit(solution)/shard_map/all_to_all | solution.py:536
  170.7 3.1 %part.1 = bf16[128,2048]{1,0:T(8,128)(2,1)} custom-call(s32[1]{0:T(128)} %bitcast.half_ref, f32[8,128]{1,0:T(8,128)S(1)} %collective-permute-done.8.meta_ref, bf16[256,2048]{1,0:T(8,128)(2,1)} %bitcast.35.got_ref), custom_call_target="tpu_custom_call" | custom-call | flops 536870912 | bytes 3145728 | tf_op jit(solution)/shard_map/part/pallas_call | solution.py:604
  173.9 2.2 %collective-permute-start.10 = (bf16[128,2048]{1,0:T(8,128)(2,1)}, bf16[128,2048]{1,0:T(8,128)(2,1)S(1)}, u32[]{:S(2)}, u32[]{:S(2)}) collective-permute-start(bf16[128,2048]{1,0:T(8,128)(2,1)} %part.1), channel_id=1, source_target_pairs={{0,16},{16,0},{1,17},{17,1},{2,18},{18,2},{3,19},{19,3},{4,20},{20... | collective-permute-start | bytes 1572872 | tf_op jit(solution)/shard_map/ppermute | solution.py:614
  176.1 4.6 %shared.1.base_ref = f32[128,2048]{1,0:T(8,128)} custom-call(bf16[128,2048]{1,0:T(8,128)(2,1)} %get-tuple-element.15.x_in, bf16[128,2048]{1,0:T(8,128)(2,1)} %get-tuple-element.16.mixed_in, bf16[2048,512]{1,0:T(8,128)(2,1)} %wg_in.1, bf16[2048,512]{1,0:T(8,128)(2,1)} %wu_in.1, bf16[512,2048]{1,0:T(8,128)(2,1)} %wd_in.1), custom_call_target="tpu_custom_call" | custom-call | flops 1073741824 | bytes 8388608 | tf_op jit(solution)/shard_map/shared/pallas_call | solution.py:572
  180.7 14.7 %all-to-all-done.3 = bf16[16,16,2048]{2,1,0:T(8,128)(2,1)S(1)} async-done(((bf16[16,16,2048]{2,1,0:T(8,128)(2,1)}), bf16[16,16,2048]{2,1,0:T(8,128)(2,1)S(1)}, u32[]{:S(2)}, u32[]{:S(2)}) %all-to-all-start.3) | async-done | bytes 1048608 | tf_op jit(solution)/shard_map/all_to_all | solution.py:536
  195.4 5.1 %collective-permute-done.10.other_ref = bf16[128,2048]{1,0:T(8,128)(2,1)S(1)} collective-permute-done((bf16[128,2048]{1,0:T(8,128)(2,1)}, bf16[128,2048]{1,0:T(8,128)(2,1)S(1)}, u32[]{:S(2)}, u32[]{:S(2)}) %collective-permute-start.10) | collective-permute-done | bytes 524320 | tf_op jit(solution)/shard_map/ppermute | solution.py:614
  200.4 1.2 copy-done.4
  201.7 1.9 combine.1
  (13 shorter events, 0.1 us)
Async XLA Ops:
  0.0 10.3 %copy-start.6 = (bf16[512,2048]{1,0:T(8,128)(2,1)S(1)}, bf16[512,2048]{1,0:T(8,128)(2,1)}, u32[]{:S(2)}) copy-start(bf16[512,2048]{1,0:T(8,128)(2,1)} %refs_0_.1) | copy-start | bytes 6291460
  1.6 8.7 %collective-permute-start = (bf16[8,4096]{1,0:T(8,128)(2,1)}, bf16[8,4096]{1,0:T(8,128)(2,1)S(1)}, u32[]{:S(2)}, u32[]{:S(2)}) collective-permute-start(bf16[8,4096]{1,0:T(8,128)(2,1)} %tails.1), channel_id=1, source_target_pairs={{0,4},{4,8},{8,12},{12,16},{16,20},{20,24},{24,28},{1,5},{5,9},{9,... | collective-permute-start | bytes 196616 | tf_op jit(solution)/shard_map/ppermute | solution.py:443
  8.8 37.6 %collective-permute-start.4 = (bf16[256,2048]{1,0:T(8,128)(2,1)}, bf16[256,2048]{1,0:T(8,128)(2,1)}, u32[]{:S(2)}, u32[]{:S(2)}) collective-permute-start(bf16[256,2048]{1,0:T(8,128)(2,1)} %slice.3), channel_id=1, source_target_pairs={{0,2},{1,3},{2,0},{3,1},{4,6},{5,7},{6,4},{7,5},{8,10},{9,11},{10,... | collective-permute-start | bytes 3145736 | tf_op jit(solution)/shard_map/ppermute | solution.py:382
  10.3 58.8 %collective-permute-start.1 = (bf16[512,2048]{1,0:T(8,128)(2,1)S(1)}, bf16[512,2048]{1,0:T(8,128)(2,1)}, u32[]{:S(2)}, u32[]{:S(2)}) collective-permute-start(bf16[512,2048]{1,0:T(8,128)(2,1)S(1)} %copy-done.6), channel_id=1, source_target_pairs={{0,1},{1,0},{2,3},{3,2},{4,5},{5,4},{6,7},{7,6},{8,9},{9,8},{10,11... | collective-permute-start | bytes 6291464 | tf_op jit(solution)/shard_map/ppermute | solution.py:384
  10.3 0.6 copy-start.12
  14.9 43.6 %copy-start.10 = (s32[1,128,2]{1,2,0:T(2,128)S(1)}, s32[1,128,2]{1,2,0:T(2,128)}, u32[]{:S(2)}) copy-start(s32[1,128,2]{1,2,0:T(2,128)} %param.44) | copy-start | bytes 3076
  14.9 44.4 %copy-start.11 = (f32[1,128,2]{1,2,0:T(2,128)S(1)}, f32[1,128,2]{1,2,0:T(2,128)}, u32[]{:S(2)}) copy-start(f32[1,128,2]{1,2,0:T(2,128)} %param.45) | copy-start | bytes 3076
  14.9 31.4 %all-to-all-start = ((bf16[8,264,128]{2,1,0:T(8,128)(2,1)}), bf16[8,264,128]{2,1,0:T(8,128)(2,1)S(1)}, u32[]{:S(2)}, u32[]{:S(2)}) async-start(bf16[8,264,128]{2,1,0:T(8,128)(2,1)} %states.1), calls=%async_computation | async-start | bytes 1081344 | tf_op jit(solution)/shard_map/all_to_all | solution.py:457
  20.1 24.8 %collective-permute-start.2 = (bf16[128,2048]{1,0:T(8,128)(2,1)S(1)}, bf16[128,2048]{1,0:T(8,128)(2,1)S(1)}, u32[]{:S(2)}, u32[]{:S(2)}) collective-permute-start(bf16[128,2048]{1,0:T(8,128)(2,1)S(1)} %constant_dynamic-slice_fusion), channel_id=1, source_target_pairs={{0,2},{1,3},{2,0},{3,1},{4,6},{5,7},{6,4},{7,5},{8,10},{9,11},{10,... | collective-permute-start | bytes 1572872 | tf_op jit(solution)/shard_map/ppermute | solution.py:381
  44.9 24.3 %copy-start.9 = (bf16[128,2048]{1,0:T(8,128)(2,1)}, bf16[128,2048]{1,0:T(8,128)(2,1)S(1)}, u32[]{:S(2)}) copy-start(bf16[128,2048]{1,0:T(8,128)(2,1)S(1)} %collective-permute-done.2.refs_2_) | copy-start | bytes 1572868
  44.9 13.7 %collective-permute-start.3 = (bf16[128,2048]{1,0:T(8,128)(2,1)S(1)}, bf16[128,2048]{1,0:T(8,128)(2,1)}, u32[]{:S(2)}, u32[]{:S(2)}) collective-permute-start(bf16[128,2048]{1,0:T(8,128)(2,1)S(1)} %collective-permute-done.2.refs_2_), channel_id=1, source_target_pairs={{0,4},{4,0},{8,12},{12,8},{1,5},{5,1},{9,13},{13,9},{2,6},{6,2},{1... | collective-permute-start | bytes 1572872 | tf_op jit(solution)/shard_map/ppermute | solution.py:383
  46.4 22.7 %collective-permute-start.7 = (bf16[256,2048]{1,0:T(8,128)(2,1)}, bf16[256,2048]{1,0:T(8,128)(2,1)}, u32[]{:S(2)}, u32[]{:S(2)}) collective-permute-start(bf16[256,2048]{1,0:T(8,128)(2,1)} %collective-permute-done.4.refs_4_), channel_id=1, source_target_pairs={{0,1},{1,0},{2,3},{3,2},{4,5},{5,4},{6,7},{7,6},{8,9},{9,8},{10,11... | collective-permute-start | bytes 3145736 | tf_op jit(solution)/shard_map/ppermute | solution.py:387
  46.4 0.8 copy-start.7
  49.1 20.0 %all-to-all-start.1 = ((bf16[8,256,128]{2,1,0:T(8,128)(2,1)}), bf16[8,256,128]{2,1,0:T(8,128)(2,1)S(1)}, u32[]{:S(2)}, u32[]{:S(2)}) async-start(bf16[8,256,128]{2,1,0:T(8,128)(2,1)} %prefix.1), calls=%async_computation.1 | async-start | bytes 1048576 | tf_op jit(solution)/shard_map/all_to_all | solution.py:492
  53.9 11.2 %collective-permute-start.5 = (bf16[128,2048]{1,0:T(8,128)(2,1)S(1)}, bf16[128,2048]{1,0:T(8,128)(2,1)}, u32[]{:S(2)}, u32[]{:S(2)}) collective-permute-start(bf16[128,2048]{1,0:T(8,128)(2,1)S(1)} %collective-permute-done.2.refs_2_), channel_id=1, source_target_pairs={{0,1},{1,0},{2,3},{3,2},{4,5},{5,4},{6,7},{7,6},{8,9},{9,8},{10,11... | collective-permute-start | bytes 1572872 | tf_op jit(solution)/shard_map/ppermute | solution.py:385
  58.6 6.6 %collective-permute-start.6 = (bf16[128,2048]{1,0:T(8,128)(2,1)}, bf16[128,2048]{1,0:T(8,128)(2,1)}, u32[]{:S(2)}, u32[]{:S(2)}) collective-permute-start(bf16[128,2048]{1,0:T(8,128)(2,1)} %collective-permute-done.3.refs_3_), channel_id=1, source_target_pairs={{0,1},{1,0},{2,3},{3,2},{4,5},{5,4},{6,7},{7,6},{8,9},{9,8},{10,11... | collective-permute-start | bytes 1572872 | tf_op jit(solution)/shard_map/ppermute | solution.py:386
  69.1 0.8 copy-start.8
  69.9 9.4 %copy-start.5 = (f32[8,128]{1,0:T(8,128)S(1)}, f32[8,128]{1,0:T(8,128)}, u32[]{:S(2)}) copy-start(f32[8,128]{1,0:T(8,128)} %maximum_maximum_fusion.meta_ref) | copy-start | bytes 12292
  79.1 25.4 %collective-permute-start.9 = (bf16[128,2048]{1,0:T(8,128)(2,1)}, bf16[128,2048]{1,0:T(8,128)(2,1)S(1)}, u32[]{:S(2)}, u32[]{:S(2)}) collective-permute-start(bf16[128,2048]{1,0:T(8,128)(2,1)} %get-tuple-element.15.x_in), channel_id=1, source_target_pairs={{0,16},{16,0},{1,17},{17,1},{2,18},{18,2},{3,19},{19,3},{4,20},{20... | collective-permute-start | bytes 1572872 | tf_op jit(solution)/shard_map/ppermute | solution.py:531
  79.3 25.2 %collective-permute-start.8 = (f32[8,128]{1,0:T(8,128)S(1)}, f32[8,128]{1,0:T(8,128)S(1)}, u32[]{:S(2)}, u32[]{:S(2)}) collective-permute-start(f32[8,128]{1,0:T(8,128)S(1)} %copy-done.5), channel_id=1, source_target_pairs={{0,16},{16,0},{1,17},{17,1},{2,18},{18,2},{3,19},{19,3},{4,20},{20... | collective-permute-start | bytes 12296 | tf_op jit(solution)/shard_map/ppermute | solution.py:425
  106.5 24.0 %copy-start = (bf16[1,2048,512]{2,1,0:T(8,128)(2,1)S(1)}, bf16[1,2048,512]{2,1,0:T(8,128)(2,1)}, u32[]{:S(2)}) copy-start(bf16[1,2048,512]{2,1,0:T(8,128)(2,1)} %wg_ref.3) | copy-start | bytes 6291460
  126.8 19.8 %all-to-all-start.2 = ((bf16[16,16,2048]{2,1,0:T(8,128)(2,1)}), bf16[16,16,2048]{2,1,0:T(8,128)(2,1)S(1)}, u32[]{:S(2)}, u32[]{:S(2)}) async-start(bf16[16,16,2048]{2,1,0:T(8,128)(2,1)} %bitcast.47), calls=%async_computation.2 | async-start | bytes 2097152 | tf_op jit(solution)/shard_map/all_to_all | solution.py:536
  130.5 1.2 copy-start.3
  135.9 1.0 copy-start.2
  146.6 20.5 %all-to-all-start.5 = ((bf16[16,16,2048]{2,1,0:T(8,128)(2,1)}), bf16[16,16,2048]{2,1,0:T(8,128)(2,1)}, u32[]{:S(2)}, u32[]{:S(2)}) async-start(bf16[16,16,2048]{2,1,0:T(8,128)(2,1)} %bitcast.44), calls=%async_computation.5 | async-start | bytes 2097152 | tf_op jit(solution)/shard_map/all_to_all | solution.py:536
  155.4 1.0 copy-start.1
  167.1 28.3 %all-to-all-start.3 = ((bf16[16,16,2048]{2,1,0:T(8,128)(2,1)}), bf16[16,16,2048]{2,1,0:T(8,128)(2,1)S(1)}, u32[]{:S(2)}, u32[]{:S(2)}) async-start(bf16[16,16,2048]{2,1,0:T(8,128)(2,1)} %bitcast.42), calls=%async_computation.3 | async-start | bytes 2097152 | tf_op jit(solution)/shard_map/all_to_all | solution.py:536
  173.9 26.6 %collective-permute-start.10 = (bf16[128,2048]{1,0:T(8,128)(2,1)}, bf16[128,2048]{1,0:T(8,128)(2,1)S(1)}, u32[]{:S(2)}, u32[]{:S(2)}) collective-permute-start(bf16[128,2048]{1,0:T(8,128)(2,1)} %part.1), channel_id=1, source_target_pairs={{0,16},{16,0},{1,17},{17,1},{2,18},{18,2},{3,19},{19,3},{4,20},{20... | collective-permute-start | bytes 1572872 | tf_op jit(solution)/shard_map/ppermute | solution.py:614
  200.4 1.2 copy-start.4

commit v3 on v2

--- a/solution.py
+++ b/solution.py
@@ -36,6 +36,14 @@
 
 def vmem(limit):
     return pltpu.CompilerParams(vmem_limit_bytes=limit * MIB)
+
+
+def inside(v):
+    return pltpu.with_memory_space_constraint(v, pltpu.VMEM)
+
+
+def outside(v):
+    return pltpu.with_memory_space_constraint(v, pltpu.HBM)
 
 
 def cost(flops, nbytes):
@@ -125,15 +133,11 @@
         out_ref[d, rows : rows + EXTRA, :] = jnp.concatenate(parts, axis=0).astype(BF16)
 
 
-def prefix_kernel(in_hbm, out_hbm, in_ref, out_ref, sem_in, sem_out):
+def prefix_kernel(in_ref, out_hbm, out_ref, sem_out):
     ways, rows, _ = out_ref.shape
-    gets = [pltpu.make_async_copy(in_hbm.at[j], in_ref.at[j], sem_in.at[j]) for j in range(ways)]
     puts = [pltpu.make_async_copy(out_ref.at[j], out_hbm.at[j], sem_out.at[j]) for j in range(ways)]
-    for get in gets:
-        get.start()
     state = jnp.zeros((rows, STATE), F32)
     for j in range(ways):
-        gets[j].wait()
         fade = in_ref[j, rows : rows + EXTRA, :].astype(F32)
         old = jnp.concatenate(
             [
@@ -161,8 +165,8 @@
     span = inner // groups
     step, cum, total = decays(s_ref, bias_ref, dlog_ref)
     wide = spread(step * jnp.exp(total - cum), inner)
-    grow = spread(jnp.exp(cum - total), inner)
-    grow_ref[...] = grow
+    grow_ref[...] = jnp.exp(cum - total)
+    grow = spread(grow_ref[...], inner)
     own = (iota((heads, inner), 0) == iota((heads, inner), 1) // HEAD_DIM).astype(F32)
     skip = dot(skip_ref[...], own, 1, 0, HIGH)
     bm = conv_silu(b_ref[...], tail_ref[:, inner : inner + narrow], wb_ref[...], rb_ref)
@@ -212,69 +216,72 @@
     return dot(high, got, 1, 0) + dot(low, got, 1, 0)
 
 
+def warm_kernel(*refs):
+    count = len(refs) // 2
+    sem = refs[-1]
+    copies = [
+        pltpu.make_async_copy(refs[i], refs[count + i], sem.at[i]) for i in range(count)
+    ]
+    for copy in copies:
+        copy.start()
+    for copy in copies:
+        copy.wait()
+
+
 def mix_kernel(
-    blocks, experts, slots, order_ref, gain_ref, fgain_ref, meta_ref, state_in, y_in, grow_in,
-    cm_in, gate_in, res_in, *refs,
+    blocks, experts, slots, order_ref, gain_ref, fgain_ref, meta_ref, factor_ref, gate_ref,
+    y_ref, cm_ref, res_ref, state_ref, *refs,
 ):
     count = len(blocks)
-    w_refs, (mixed_ref, x_ref, send_ref) = refs[:-19], refs[-19:-16]
-    wbuf, state_ref, y_ref, grow_ref, cm_ref, gate_ref, res_ref = refs[-16:-9]
-    acc, mbuf, xbuf, sbuf, sem_w, sem_v, sem_m, sem_x, sem_s = refs[-9:]
-    per = wbuf.shape[1]
+    w_refs, (mixed_ref, x_ref, send_ref) = refs[:-13], refs[-13:-10]
+    wbuf, acc, vbuf, mbuf, xbuf, sbuf, sem_w, sem_m, sem_x, sem_s = refs[-10:]
+    per = gate_ref.shape[1] // count
     odd = order_ref[count + 1]
-    copies = []
-    for i, pieces in enumerate(blocks):
-        at = pl.multiple_of(order_ref[i] * per, per)
-        col = pl.multiple_of(order_ref[i] * STATE, STATE)
-        wide = pl.ds(at, per)
-        pairs = [
-            (state_in.at[wide, :], state_ref.at[i]),
-            (cm_in.at[:, pl.ds(col, STATE)], cm_ref.at[i]),
-            (y_in.at[:, wide], y_ref.at[i]),
-            (grow_in.at[:, wide], grow_ref.at[i]),
-            (gate_in.at[:, wide], gate_ref.at[i]),
-        ]
-        small = [pltpu.make_async_copy(a, b, sem_v.at[i, k]) for k, (a, b) in enumerate(pairs)]
-        large = []
-        for k, (which, row, size, side) in enumerate(pieces):
-            if side is None:
-                to = pl.ds(0, size)
-            else:
-                to = pl.ds(pl.multiple_of((odd if side == 0 else 1 - odd) * size, size), size)
-            large.append(
-                pltpu.make_async_copy(
-                    w_refs[which].at[pl.ds(row, size), :], wbuf.at[i, to], sem_w.at[i, k]
-                )
+    weights = []
+    for i in range(count):
+        weights.append([])
+        for k, (which, row, size, side) in enumerate(blocks[i]):
+            to = i * per
+            if side is not None:
+                to = to + (odd if side == 0 else 1 - odd) * size
+                to = pl.multiple_of(to, size)
+            copy = pltpu.make_async_copy(
+                w_refs[which].at[pl.ds(row, size), :], wbuf.at[pl.ds(to, size), :], sem_w.at[i, k]
             )
-        for copy in small + large:
             copy.start()
-        copies.append((small, large))
-    residual = pltpu.make_async_copy(res_in, res_ref, sem_v.at[count, 0])
-    residual.start()
+            weights[-1].append(copy)
+    vbuf[...] = spread(factor_ref[...], gate_ref.shape[1])
+    normed = []
     for i in range(count):
-        at = pl.multiple_of(order_ref[i] * per, per)
-        for copy in copies[i][0]:
+        wide = pl.ds(pl.multiple_of(order_ref[i] * per, per), per)
+        col = pl.ds(pl.multiple_of(order_ref[i] * STATE, STATE), STATE)
+        v = y_ref[:, wide] + vbuf[:, wide] * dot(cm_ref[:, col], state_ref[wide, :], 1, 1)
+        v = v.astype(BF16).astype(F32)
+        v = v * silu(gate_ref[:, wide].astype(F32))
+        v = v * lax.rsqrt(jnp.mean(v * v, axis=1, keepdims=True) + EPS)
+        normed.append((v * gain_ref[:, wide]).astype(BF16))
+    features = mbuf.shape[1]
+    step = features // 4
+    squares = 0.0
+    for i in range(0, count, 2):
+        for copy in weights[i] + weights[i + 1]:
             copy.wait()
-        v = y_ref[i] + grow_ref[i] * dot(cm_ref[i], state_ref[i], 1, 1)
-        v = v.astype(BF16).astype(F32)
-        v = v * silu(gate_ref[i].astype(F32))
-        v = v * lax.rsqrt(jnp.mean(v * v, axis=1, keepdims=True) + EPS)
-        v = (v * gain_ref[:, pl.ds(at, per)]).astype(BF16)
-        for copy in copies[i][1]:
-            copy.wait()
-        part = dot(v, wbuf[i], 1, 0)
-        if i == 0:
-            acc[...] = part
-        else:
-            acc[...] += part
-    residual.wait()
-    mixed = (res_ref[...].astype(F32) + acc[...]).astype(BF16)
-    mbuf[...] = mixed
+        v = jnp.concatenate(normed[i : i + 2], axis=1)
+        for n in range(0, features, step):
+            at = slice(n, n + step)
+            out = res_ref[:, at].astype(F32) if i == 0 else acc[:, at]
+            out = out + dot(v, wbuf[i * per : (i + 2) * per, at], 1, 0)
+            if i < count - 2:
+                acc[:, at] = out
+                continue
+            out = out.astype(BF16)
+            mbuf[:, at] = out
+            m = out.astype(F32)
+            squares = squares + jnp.sum(m * m, axis=1, keepdims=True)
     out_mixed = pltpu.make_async_copy(mbuf, mixed_ref, sem_m)
     out_mixed.start()
-    m = mixed.astype(F32)
-    x = m * lax.rsqrt(jnp.mean(m * m, axis=1, keepdims=True) + EPS) * fgain_ref[...]
-    x = x.astype(BF16)
+    scale = lax.rsqrt(squares / features + EPS)
+    x = (mbuf[...].astype(F32) * scale * fgain_ref[...]).astype(BF16)
     xbuf[...] = x
     out_x = pltpu.make_async_copy(xbuf, x_ref, sem_x)
     out_x.start()
@@ -443,14 +450,14 @@
     tail = lax.ppermute(tail, SP, [(i, i + 1) for i in range(ways - 1)])
     fresh = pl.pallas_call(
         state_kernel,
-        out_shape=jax.ShapeDtypeStruct((ways, width + EXTRA, STATE), BF16),
+        out_shape=pltpu.HBM((ways, width + EXTRA, STATE), BF16),
         in_specs=[vm] * 8,
         out_specs=vm,
         scratch_shapes=[
             pltpu.VMEM((8 + tokens, inner), F32),
             pltpu.VMEM((8 + tokens, b_in.shape[1]), F32),
         ],
-        compiler_params=vmem(60),
+        compiler_params=vmem(24),
         cost_estimate=cost(1 << 30, 4 * MIB),
         name="states",
     )(*turned, tail, conv_weight, conv_b_weight, x_in, b_in)
@@ -458,9 +465,9 @@
     y, grow, cm = pl.pallas_call(
         inner_kernel,
         out_shape=(
-            jax.ShapeDtypeStruct((tokens, inner), F32),
-            jax.ShapeDtypeStruct((tokens, inner), F32),
-            jax.ShapeDtypeStruct((tokens, b_in.shape[1]), BF16),
+            pltpu.HBM((tokens, inner), F32),
+            pltpu.HBM((heads, tokens), F32),
+            pltpu.HBM((tokens, b_in.shape[1]), BF16),
         ),
         in_specs=[vm] * 11,
         out_specs=(vm,) * 3,
@@ -468,7 +475,7 @@
             pltpu.VMEM((8 + tokens, inner), F32),
             pltpu.VMEM((8 + tokens, b_in.shape[1]), F32),
         ],
-        compiler_params=vmem(60),
+        compiler_params=vmem(24),
         cost_estimate=cost(2 << 30, 8 * MIB),
         name="within",
     )(
@@ -477,55 +484,56 @@
     entering = pl.pallas_call(
         prefix_kernel,
         out_shape=jax.ShapeDtypeStruct((ways, width, STATE), BF16),
-        in_specs=[hbm],
+        in_specs=[vm],
         out_specs=hbm,
-        scratch_shapes=[
-            pltpu.VMEM(fresh.shape, BF16),
-            pltpu.VMEM((ways, width, STATE), BF16),
-            pltpu.SemaphoreType.DMA((ways,)),
-            pltpu.SemaphoreType.DMA((ways,)),
-        ],
-        compiler_params=vmem(60),
+        scratch_shapes=[pltpu.VMEM((ways, width, STATE), BF16), pltpu.SemaphoreType.DMA((ways,))],
+        compiler_params=vmem(24),
         cost_estimate=cost(1 << 26, 2 * MIB),
         name="prefix",
-    )(fresh)
+    )(inside(fresh))
     entering = lax.all_to_all(entering, SP, split_axis=0, concat_axis=0, tiled=True)
     entering = entering.reshape(inner, STATE)
 
     sm = pl.BlockSpec(memory_space=pltpu.SMEM)
+    warm = [gate_input[0], y, cm, residual[0]]
+    warm = pl.pallas_call(
+        warm_kernel,
+        out_shape=tuple(pltpu.VMEM(v.shape, v.dtype) for v in warm),
+        in_specs=[hbm] * len(warm),
+        out_specs=(vm,) * len(warm),
+        scratch_shapes=[pltpu.SemaphoreType.DMA((len(warm),))],
+        compiler_params=vmem(24),
+        cost_estimate=cost(1 << 28, 8 * MIB),
+        name="warm",
+    )(*[outside(v) for v in warm])
+    warm = [inside(v) for v in warm]
     mixed, x, send = pl.pallas_call(
         functools.partial(mix_kernel, blocks, experts, slots),
         out_shape=(
-            jax.ShapeDtypeStruct((tokens, features), BF16),
-            jax.ShapeDtypeStruct((tokens, features), BF16),
-            jax.ShapeDtypeStruct((rows, features), BF16),
+            pltpu.HBM((tokens, features), BF16),
+            pltpu.HBM((tokens, features), BF16),
+            pltpu.HBM((rows, features), BF16),
         ),
-        in_specs=[sm] + [vm] * 3 + [hbm] * (6 + len(ws)),
+        in_specs=[sm] + [vm] * 9 + [hbm] * len(ws),
         out_specs=(hbm, hbm, hbm),
         scratch_shapes=[
-            pltpu.VMEM((groups, span, features), BF16),
-            pltpu.VMEM((groups, span, STATE), BF16),
-            pltpu.VMEM((groups, tokens, span), F32),
-            pltpu.VMEM((groups, tokens, span), F32),
-            pltpu.VMEM((groups, tokens, STATE), BF16),
-            pltpu.VMEM((groups, tokens, span), BF16),
-            pltpu.VMEM((tokens, features), BF16),
+            pltpu.VMEM((groups * span, features), BF16),
             pltpu.VMEM((tokens, features), F32),
+            pltpu.VMEM((tokens, inner), F32),
             pltpu.VMEM((tokens, features), BF16),
             pltpu.VMEM((tokens, features), BF16),
             pltpu.VMEM((rows, features), BF16),
             pltpu.SemaphoreType.DMA((groups, 2)),
-            pltpu.SemaphoreType.DMA((groups + 1, 5)),
             pltpu.SemaphoreType.DMA,
             pltpu.SemaphoreType.DMA,
             pltpu.SemaphoreType.DMA((pieces,)),
         ],
-        compiler_params=vmem(62),
+        compiler_params=vmem(36),
         cost_estimate=cost(3 << 30, 16 * MIB),
         name="mix",
     )(
-        order, norm_gain[None], ffn_gain[None], meta, entering, y, grow, cm, gate_input[0],
-        residual[0], *ws,
+        order, norm_gain[None], ffn_gain[None], meta, grow,
+        *warm, inside(entering), *[outside(v) for v in ws],
     )
 
     x_far = lax.ppermute(x, "half", mirror)

time: 204 us -> 201 us (0.985)
  Pallas kernels: 41.8 us -> 37.9 us
  local copies, waits for them, and re-layouts: 9.67 us -> 7.02 us
  waiting for transfers between devices: 94.2 us -> 96.8 us
    ppermute x1, waiting for transfers between devices: 4.4 us -> 8.87 us  [gather_rows(): ya = lax.ppermute(xa, 'sub', flip)]
    all_to_all x1, waiting for transfers between devices: 3.95 us -> 0.21 us  [layer(): lax.all_to_all(entering, SP, split_axis=0, concat_axis=0, tiled=True)]
    ppermute x1, starting transfers between devices: 0.19 us -> 2.89 us  [layer(): x_far = lax.ppermute(x, 'half', mirror)]
    ppermute x1, starting transfers between devices: 2.8 us -> 0.1 us  [layer(): meta_far = lax.ppermute(meta, 'half', mirror)]
    unnamed x26 -> x40, local copies, waits for them, and re-layouts: 6.61 us -> 4.48 us
    pallas_call x1, Pallas kernels: 9.21 us -> 7.16 us  [layer(): pl.pallas_call(functools.partial(mix_kernel, blocks, experts, slots), out...]
    pallas_call x2 -> x3, Pallas kernels: 9.2 us -> 8.29 us  [the longest x1 3.87 us: layer(): pl.pallas_call(inner_kernel, out_shape=(pltpu.HBM((tokens, inner), F32),...]
  transfers between devices with their start and end apart: 16 -> 16, of which waited for: 8 -> 8; matrix products, arithmetic and copies ran while one was open for 2% -> 1% of each run, Pallas kernels for 13% -> 13%
where the time goes in v3:
time: 201 us; the launch traced here: 200 us
  waiting for transfers between devices  96.8 us (48%)
  Pallas kernels  37.9 us (19%)
  starting transfers between devices  37.2 us (19%)
  blocking collectives  21 us (10%)
  local copies, waits for them, and re-layouts  7.02 us (3%)
    all_to_all x3, waiting for transfers between devices, exchange(): return lax.all_to_all(v, group, split_axis=0, concat_axis=0, tiled=True)  35 us
    ppermute x1, waiting for transfers between devices, layer(): meta_far = lax.ppermute(meta, 'half', mirror)  24.1 us
    ppermute x1, waiting for transfers between devices, gather_rows(): lax.ppermute(lax.dynamic_slice_in_dim(w, odd * part, part, 0), 'dp', over)  22.9 us
    all_to_all x1, blocking collectives, exchange(): return lax.all_to_all(v, group, split_axis=0, concat_axis=0, tiled=True)  21 us
    all_to_all x3, starting transfers between devices, exchange(): return lax.all_to_all(v, group, split_axis=0, concat_axis=0, tiled=True)  11.8 us
    ppermute x1, waiting for transfers between devices, gather_rows(): ya = lax.ppermute(xa, 'sub', flip)  8.87 us
    pallas_call x2, Pallas kernels, serve(): pl.pallas_call(expert_kernel, out_shape=jax.ShapeDtypeStruct((own, m, fea...  8.47 us
    pallas_call x1, Pallas kernels, layer(): pl.pallas_call(functools.partial(mix_kernel, blocks, experts, slots), out...  7.16 us
  transfers between devices with their start and end apart: 16, of which 8 were waited for; matrix products, arithmetic and copies ran while one was open for 1% of the time, Pallas kernels for 13%

profile of v3, /device:TPU:0, one launch (start us, length us, event | category | flops | bytes accessed | tf_op | source)
XLA Modules:
  0.0 200.2 jit_solution(430728229268323706)
XLA Ops:
  0.0 0.0 copy-start.8
  0.0 0.0 copy-start.10
  0.0 1.5 tails.1
  1.5 4.9 %collective-permute-start = (bf16[8,4096]{1,0:T(8,128)(2,1)}, bf16[8,4096]{1,0:T(8,128)(2,1)S(1)}, u32[]{:S(2)}, u32[]{:S(2)}) collective-permute-start(bf16[8,4096]{1,0:T(8,128)(2,1)} %tails.1), channel_id=1, source_target_pairs={{0,4},{4,8},{8,12},{12,16},{16,20},{20,24},{24,28},{1,5},{5,9},{9,... | collective-permute-start | bytes 196616 | tf_op jit(solution)/shard_map/ppermute | solution.py:450
  6.4 1.3 slice.3
  7.7 1.6 collective-permute-start.4
  9.3 0.0 collective-permute-start.1
  9.3 0.0 collective-permute-done.tail_ref
  9.3 0.0 copy-done.5
  9.3 0.0 copy-done.6
  9.4 2.8 %states.1 = bf16[8,264,128]{2,1,0:T(8,128)(2,1)} custom-call(bf16[32,128]{1,0:T(8,128)(2,1)S(1)} %bitcast.55, f32[1,32]{1,0:T(1,128)S(1)} %bitcast.59, f32[1,32]{1,0:T(1,128)S(1)} %bitcast.61, bf16[8,4096]{1,0:T(8,128)(2,1)S(1)} %collective-permute-done.tail_ref, bf16[4,2048]{1,0:T(4,128)(2,1)S(1)} %copy-done.8, bf16[4,1024]{1,0:T(4,128)(2,1)S(1)} %copy-done.10, ...), custom_call_target="tpu_custom_call" | custom-call | flops 1073741824 | bytes 4194304 | tf_op jit(solution)/shard_map/states/pallas_call | solution.py:451
  12.1 0.0 copy-start.16
  12.2 6.0 %all-to-all-start = ((bf16[8,264,128]{2,1,0:T(8,128)(2,1)}), bf16[8,264,128]{2,1,0:T(8,128)(2,1)S(1)}, u32[]{:S(2)}, u32[]{:S(2)}) async-start(bf16[8,264,128]{2,1,0:T(8,128)(2,1)} %states.1), calls=%async_computation | async-start | bytes 1081344 | tf_op jit(solution)/shard_map/all_to_all | solution.py:464
  18.2 1.1 constant_dynamic-slice_fusion
  19.3 1.6 collective-permute-start.2
  20.8 22.9 %collective-permute-done.2.refs_2_ = bf16[128,2048]{1,0:T(8,128)(2,1)} collective-permute-done((bf16[128,2048]{1,0:T(8,128)(2,1)S(1)}, bf16[128,2048]{1,0:T(8,128)(2,1)}, u32[]{:S(2)}, u32[]{:S(2)}) %collective-permute-start.2) | collective-permute-done | bytes 524320 | tf_op jit(solution)/shard_map/ppermute | solution.py:388
  43.8 1.5 collective-permute-start.3
  45.3 0.0 collective-permute-done.4.refs_4_
  45.3 0.0 collective-permute-start.7
  45.3 0.0 all-to-all-done.in_ref
  45.3 0.9 prefix.1
  46.2 4.8 %all-to-all-start.1 = ((bf16[8,256,128]{2,1,0:T(8,128)(2,1)}), bf16[8,256,128]{2,1,0:T(8,128)(2,1)S(1)}, u32[]{:S(2)}, u32[]{:S(2)}) async-start(bf16[8,256,128]{2,1,0:T(8,128)(2,1)} %prefix.1), calls=%async_computation.1 | async-start | bytes 1048576 | tf_op jit(solution)/shard_map/all_to_all | solution.py:494
  51.0 0.2 collective-permute-start.5
  51.3 8.9 %collective-permute-done.3.refs_3_ = bf16[128,2048]{1,0:T(8,128)(2,1)} collective-permute-done((bf16[128,2048]{1,0:T(8,128)(2,1)}, bf16[128,2048]{1,0:T(8,128)(2,1)}, u32[]{:S(2)}, u32[]{:S(2)}) %collective-permute-start.3) | collective-permute-done | bytes 524320 | tf_op jit(solution)/shard_map/ppermute | solution.py:390
  60.1 0.0 collective-permute-start.6
  60.2 0.1 pad.2.clone
  60.2 0.1 stack.40.order_ref
  60.3 0.0 copy-done.19
  60.3 0.1 maximum_maximum_fusion.meta_ref
  60.4 0.0 copy-done.7
  60.4 3.9 %within.1 = (f32[128,2048]{1,0:T(8,128)}, f32[32,128]{1,0:T(8,128)}, bf16[128,1024]{1,0:T(8,128)(2,1)}) custom-call(bf16[32,128]{1,0:T(8,128)(2,1)S(1)} %bitcast.56, f32[1,32]{1,0:T(1,128)S(1)} %bitcast.60, f32[1,32]{1,0:T(1,128)S(1)} %bitcast.62, f32[1,32]{1,0:T(1,128)S(1)} %bitcast.63, bf16[8,4096]{1,0:T(8,128)(2,1)S(1)} %collective-permute-done.tail_ref, ...), custom_call_target="tpu_custom_call" | custom-call | flops 2147483648 | bytes 8388608 | tf_op jit(solution)/shard_map/within/pallas_call | solution.py:465
  64.3 1.7 warm.1
  66.0 0.0 collective-permute-done.5.refs_5_
  66.0 0.0 collective-permute-done.6.refs_6_
  66.0 0.2 all-to-all-done.1
  66.2 0.0 collective-permute-done.7.refs_7_
  66.2 0.0 collective-permute-done.1.refs_1_
  66.2 0.0 copy-done.13
  66.2 0.0 copy-done.17
  66.2 7.2 %mix.1 = (bf16[128,2048]{1,0:T(8,128)(2,1)}, bf16[128,2048]{1,0:T(8,128)(2,1)}, bf16[256,2048]{1,0:T(8,128)(2,1)}) custom-call(s32[10]{0:T(128)S(1)} %stack.40.order_ref, f32[1,2048]{1,0:T(1,128)S(1)} %bitcast.57, f32[1,2048]{1,0:T(1,128)S(1)} %bitcast.58, f32[8,128]{1,0:T(8,128)S(1)} %maximum_maximum_fusion.meta_ref, f32[32,128]{1,0:T(8,128)S(1)} %copy-done.17, ...), custom_call_target="tpu_custom_call" | custom-call | flops 3221225472 | bytes 16777216 | tf_op jit(solution)/shard_map/mix/pallas_call | solution.py:510
  73.4 2.9 %collective-permute-start.9 = (bf16[128,2048]{1,0:T(8,128)(2,1)}, bf16[128,2048]{1,0:T(8,128)(2,1)S(1)}, u32[]{:S(2)}, u32[]{:S(2)}) collective-permute-start(bf16[128,2048]{1,0:T(8,128)(2,1)} %get-tuple-element.23.x_in), channel_id=1, source_target_pairs={{0,16},{16,0},{1,17},{17,1},{2,18},{18,2},{3,19},{19,3},{4,20},{20... | collective-permute-start | bytes 1572872 | tf_op jit(solution)/shard_map/ppermute | solution.py:539
  76.3 0.1 collective-permute-start.8
  76.4 24.1 %collective-permute-done.8.meta_ref = f32[8,128]{1,0:T(8,128)S(1)} collective-permute-done((f32[8,128]{1,0:T(8,128)S(1)}, f32[8,128]{1,0:T(8,128)S(1)}, u32[]{:S(2)}, u32[]{:S(2)}) %collective-permute-start.8) | collective-permute-done | bytes 4128 | tf_op jit(solution)/shard_map/ppermute | solution.py:432
  100.5 0.0 collective-permute-done.9.x_in
  100.5 2.0 relay.1
  102.5 0.0 copy-start
  102.5 21.0 %all_to_all.30 = bf16[16,16,2048]{2,1,0:T(8,128)(2,1)} all-to-all(bf16[16,16,2048]{2,1,0:T(8,128)(2,1)S(1)} %bitcast.40), channel_id=1, replica_groups=mesh['half'=2,'sub'=4,'dp'=4] {'sub','dp'}, dimensions={0} | all-to-all | bytes 2097152 | tf_op jit(solution)/shard_map/all_to_all | solution.py:544
  123.5 3.7 %all-to-all-start.2 = ((bf16[16,16,2048]{2,1,0:T(8,128)(2,1)}), bf16[16,16,2048]{2,1,0:T(8,128)(2,1)S(1)}, u32[]{:S(2)}, u32[]{:S(2)}) async-start(bf16[16,16,2048]{2,1,0:T(8,128)(2,1)} %bitcast.64), calls=%async_computation.2 | async-start | bytes 2097152 | tf_op jit(solution)/shard_map/all_to_all | solution.py:544
  127.1 1.2 copy-done.3
  128.4 4.2 %experts.3 = bf16[1,256,2048]{2,1,0:T(8,128)(2,1)S(1)} custom-call(bf16[1,256,2048]{2,1,0:T(8,128)(2,1)S(1)} %bitcast.45, bf16[1,2048,512]{2,1,0:T(8,128)(2,1)S(1)} %copy-done, bf16[1,2048,512]{2,1,0:T(8,128)(2,1)} %wu_ref.3, bf16[1,512,2048]{2,1,0:T(8,128)(2,1)} %wd_ref.3), custom_call_target="tpu_custom_call" | custom-call | flops 2147483648 | bytes 8388608 | tf_op jit(solution)/shard_map/experts/pallas_call | solution.py:555
  132.6 1.0 copy-done.2
  133.6 9.6 %all-to-all-done.2 = bf16[16,16,2048]{2,1,0:T(8,128)(2,1)S(1)} async-done(((bf16[16,16,2048]{2,1,0:T(8,128)(2,1)}), bf16[16,16,2048]{2,1,0:T(8,128)(2,1)S(1)}, u32[]{:S(2)}, u32[]{:S(2)}) %all-to-all-start.2) | async-done | bytes 1048608 | tf_op jit(solution)/shard_map/all_to_all | solution.py:544
  143.2 4.5 %all-to-all-start.5 = ((bf16[16,16,2048]{2,1,0:T(8,128)(2,1)}), bf16[16,16,2048]{2,1,0:T(8,128)(2,1)}, u32[]{:S(2)}, u32[]{:S(2)}) async-start(bf16[16,16,2048]{2,1,0:T(8,128)(2,1)} %bitcast.44), calls=%async_computation.5 | async-start | bytes 2097152 | tf_op jit(solution)/shard_map/all_to_all | solution.py:544
  147.7 4.2 %experts.2 = bf16[1,256,2048]{2,1,0:T(8,128)(2,1)S(1)} custom-call(bf16[1,256,2048]{2,1,0:T(8,128)(2,1)S(1)} %bitcast.43, bf16[1,2048,512]{2,1,0:T(8,128)(2,1)S(1)} %copy-done, bf16[1,2048,512]{2,1,0:T(8,128)(2,1)} %wu_ref.3, bf16[1,512,2048]{2,1,0:T(8,128)(2,1)} %wd_ref.3), custom_call_target="tpu_custom_call" | custom-call | flops 2147483648 | bytes 8388608 | tf_op jit(solution)/shard_map/experts/pallas_call | solution.py:555
  152.0 1.0 copy-done.1
  153.0 10.7 %all-to-all-done.5 = bf16[16,16,2048]{2,1,0:T(8,128)(2,1)} async-done(((bf16[16,16,2048]{2,1,0:T(8,128)(2,1)}), bf16[16,16,2048]{2,1,0:T(8,128)(2,1)}, u32[]{:S(2)}, u32[]{:S(2)}) %all-to-all-start.5) | async-done | bytes 1048608 | tf_op jit(solution)/shard_map/all_to_all | solution.py:544
  163.7 3.7 %all-to-all-start.3 = ((bf16[16,16,2048]{2,1,0:T(8,128)(2,1)}), bf16[16,16,2048]{2,1,0:T(8,128)(2,1)S(1)}, u32[]{:S(2)}, u32[]{:S(2)}) async-start(bf16[16,16,2048]{2,1,0:T(8,128)(2,1)} %bitcast.42), calls=%async_computation.3 | async-start | bytes 2097152 | tf_op jit(solution)/shard_map/all_to_all | solution.py:544
  167.4 3.1 %part.1 = bf16[128,2048]{1,0:T(8,128)(2,1)} custom-call(s32[1]{0:T(128)} %bitcast.half_ref, f32[8,128]{1,0:T(8,128)S(1)} %collective-permute-done.8.meta_ref, bf16[256,2048]{1,0:T(8,128)(2,1)} %bitcast.35.got_ref), custom_call_target="tpu_custom_call" | custom-call | flops 536870912 | bytes 3145728 | tf_op jit(solution)/shard_map/part/pallas_call | solution.py:612
  170.5 1.7 collective-permute-start.10
  172.3 4.6 %shared.1.base_ref = f32[128,2048]{1,0:T(8,128)} custom-call(bf16[128,2048]{1,0:T(8,128)(2,1)} %get-tuple-element.23.x_in, bf16[128,2048]{1,0:T(8,128)(2,1)} %get-tuple-element.24.mixed_in, bf16[2048,512]{1,0:T(8,128)(2,1)} %wg_in.1, bf16[2048,512]{1,0:T(8,128)(2,1)} %wu_in.1, bf16[512,2048]{1,0:T(8,128)(2,1)} %wd_in.1), custom_call_target="tpu_custom_call" | custom-call | flops 1073741824 | bytes 8388608 | tf_op jit(solution)/shard_map/shared/pallas_call | solution.py:580
  176.8 14.7 %all-to-all-done.3 = bf16[16,16,2048]{2,1,0:T(8,128)(2,1)S(1)} async-done(((bf16[16,16,2048]{2,1,0:T(8,128)(2,1)}), bf16[16,16,2048]{2,1,0:T(8,128)(2,1)S(1)}, u32[]{:S(2)}, u32[]{:S(2)}) %all-to-all-start.3) | async-done | bytes 1048608 | tf_op jit(solution)/shard_map/all_to_all | solution.py:544
  191.5 5.6 %collective-permute-done.10.other_ref = bf16[128,2048]{1,0:T(8,128)(2,1)S(1)} collective-permute-done((bf16[128,2048]{1,0:T(8,128)(2,1)}, bf16[128,2048]{1,0:T(8,128)(2,1)S(1)}, u32[]{:S(2)}, u32[]{:S(2)}) %collective-permute-start.10) | collective-permute-done | bytes 524320 | tf_op jit(solution)/shard_map/ppermute | solution.py:622
  197.1 1.2 copy-done.4
  198.3 1.9 combine.1
  (28 shorter events, 0.1 us)
Async XLA Ops:
  0.0 9.3 %copy-start.5 = (bf16[1,128,2048]{2,1,0:T(8,128)(2,1)S(1)}, bf16[1,128,2048]{2,1,0:T(8,128)(2,1)}, u32[]{:S(2)}) copy-start(bf16[1,128,2048]{2,1,0:T(8,128)(2,1)} %param.24) | copy-start | bytes 1572868
  0.0 9.3 %copy-start.6 = (bf16[1,128,1024]{2,1,0:T(8,128)(2,1)S(1)}, bf16[1,128,1024]{2,1,0:T(8,128)(2,1)}, u32[]{:S(2)}) copy-start(bf16[1,128,1024]{2,1,0:T(8,128)(2,1)} %param.26) | copy-start | bytes 786436
  0.0 9.3 %copy-start.9 = (bf16[1,128,32]{1,2,0:T(8,128)(2,1)S(1)}, bf16[1,128,32]{1,2,0:T(8,128)(2,1)}, u32[]{:S(2)}) copy-start(bf16[1,128,32]{1,2,0:T(8,128)(2,1)} %param.28) | copy-start | bytes 24580
  0.0 9.3 %copy-start.14 = (f32[32]{0:T(128)S(1)}, f32[32]{0:T(128)}, u32[]{:S(2)}) copy-start(f32[32]{0:T(128)} %param.32) | copy-start | bytes 388
  0.0 9.3 %copy-start.15 = (f32[32]{0:T(128)S(1)}, f32[32]{0:T(128)}, u32[]{:S(2)}) copy-start(f32[32]{0:T(128)} %param.33) | copy-start | bytes 388
  0.0 9.3 %copy-start.8 = (bf16[4,2048]{1,0:T(4,128)(2,1)S(1)}, bf16[4,2048]{1,0:T(4,128)(2,1)}, u32[]{:S(2)}) copy-start(bf16[4,2048]{1,0:T(4,128)(2,1)} %wx_ref.3) | copy-start | bytes 49156
  0.0 9.3 %copy-start.10 = (bf16[4,1024]{1,0:T(4,128)(2,1)S(1)}, bf16[4,1024]{1,0:T(4,128)(2,1)}, u32[]{:S(2)}) copy-start(bf16[4,1024]{1,0:T(4,128)(2,1)} %wb_ref.3) | copy-start | bytes 24580
  1.5 7.8 %collective-permute-start = (bf16[8,4096]{1,0:T(8,128)(2,1)}, bf16[8,4096]{1,0:T(8,128)(2,1)S(1)}, u32[]{:S(2)}, u32[]{:S(2)}) collective-permute-start(bf16[8,4096]{1,0:T(8,128)(2,1)} %tails.1), channel_id=1, source_target_pairs={{0,4},{4,8},{8,12},{12,16},{16,20},{20,24},{24,28},{1,5},{5,9},{9,... | collective-permute-start | bytes 196616 | tf_op jit(solution)/shard_map/ppermute | solution.py:450
  7.7 37.5 %collective-permute-start.4 = (bf16[256,2048]{1,0:T(8,128)(2,1)S(1)}, bf16[256,2048]{1,0:T(8,128)(2,1)}, u32[]{:S(2)}, u32[]{:S(2)}) collective-permute-start(bf16[256,2048]{1,0:T(8,128)(2,1)S(1)} %slice.3), channel_id=1, source_target_pairs={{0,2},{1,3},{2,0},{3,1},{4,6},{5,7},{6,4},{7,5},{8,10},{9,11},{10,... | collective-permute-start | bytes 3145736 | tf_op jit(solution)/shard_map/ppermute | solution.py:389
  9.3 56.9 %collective-permute-start.1 = (bf16[512,2048]{1,0:T(8,128)(2,1)}, bf16[512,2048]{1,0:T(8,128)(2,1)}, u32[]{:S(2)}, u32[]{:S(2)}) collective-permute-start(bf16[512,2048]{1,0:T(8,128)(2,1)} %refs_0_.1), channel_id=1, source_target_pairs={{0,1},{1,0},{2,3},{3,2},{4,5},{5,4},{6,7},{7,6},{8,9},{9,8},{10,11... | collective-permute-start | bytes 6291464 | tf_op jit(solution)/shard_map/ppermute | solution.py:391
  12.1 48.0 %copy-start.18 = (s32[1,128,2]{1,2,0:T(2,128)S(1)}, s32[1,128,2]{1,2,0:T(2,128)}, u32[]{:S(2)}) copy-start(s32[1,128,2]{1,2,0:T(2,128)} %param.44) | copy-start | bytes 3076
  12.1 48.2 %copy-start.19 = (f32[1,128,2]{1,2,0:T(2,128)S(1)}, f32[1,128,2]{1,2,0:T(2,128)}, u32[]{:S(2)}) copy-start(f32[1,128,2]{1,2,0:T(2,128)} %param.45) | copy-start | bytes 3076
  12.1 48.3 %copy-start.7 = (bf16[1,128,1024]{2,1,0:T(8,128)(2,1)S(1)}, bf16[1,128,1024]{2,1,0:T(8,128)(2,1)}, u32[]{:S(2)}) copy-start(bf16[1,128,1024]{2,1,0:T(8,128)(2,1)} %param.27) | copy-start | bytes 786436
  12.1 48.3 %copy-start.11 = (bf16[4,1024]{1,0:T(4,128)(2,1)S(1)}, bf16[4,1024]{1,0:T(4,128)(2,1)}, u32[]{:S(2)}) copy-start(bf16[4,1024]{1,0:T(4,128)(2,1)} %wc_ref.1) | copy-start | bytes 24580
  12.1 48.3 %copy-start.16 = (f32[32]{0:T(128)S(1)}, f32[32]{0:T(128)}, u32[]{:S(2)}) copy-start(f32[32]{0:T(128)} %param.34) | copy-start | bytes 388
  12.2 33.1 %all-to-all-start = ((bf16[8,264,128]{2,1,0:T(8,128)(2,1)}), bf16[8,264,128]{2,1,0:T(8,128)(2,1)S(1)}, u32[]{:S(2)}, u32[]{:S(2)}) async-start(bf16[8,264,128]{2,1,0:T(8,128)(2,1)} %states.1), calls=%async_computation | async-start | bytes 1081344 | tf_op jit(solution)/shard_map/all_to_all | solution.py:464
  19.3 24.5 %collective-permute-start.2 = (bf16[128,2048]{1,0:T(8,128)(2,1)S(1)}, bf16[128,2048]{1,0:T(8,128)(2,1)}, u32[]{:S(2)}, u32[]{:S(2)}) collective-permute-start(bf16[128,2048]{1,0:T(8,128)(2,1)S(1)} %constant_dynamic-slice_fusion), channel_id=1, source_target_pairs={{0,2},{1,3},{2,0},{3,1},{4,6},{5,7},{6,4},{7,5},{8,10},{9,11},{10,... | collective-permute-start | bytes 1572872 | tf_op jit(solution)/shard_map/ppermute | solution.py:388
  43.8 16.4 %collective-permute-start.3 = (bf16[128,2048]{1,0:T(8,128)(2,1)}, bf16[128,2048]{1,0:T(8,128)(2,1)}, u32[]{:S(2)}, u32[]{:S(2)}) collective-permute-start(bf16[128,2048]{1,0:T(8,128)(2,1)} %collective-permute-done.2.refs_2_), channel_id=1, source_target_pairs={{0,4},{4,0},{8,12},{12,8},{1,5},{5,1},{9,13},{13,9},{2,6},{6,2},{1... | collective-permute-start | bytes 1572872 | tf_op jit(solution)/shard_map/ppermute | solution.py:390
  45.3 20.9 %collective-permute-start.7 = (bf16[256,2048]{1,0:T(8,128)(2,1)}, bf16[256,2048]{1,0:T(8,128)(2,1)}, u32[]{:S(2)}, u32[]{:S(2)}) collective-permute-start(bf16[256,2048]{1,0:T(8,128)(2,1)} %collective-permute-done.4.refs_4_), channel_id=1, source_target_pairs={{0,1},{1,0},{2,3},{3,2},{4,5},{5,4},{6,7},{7,6},{8,9},{9,8},{10,11... | collective-permute-start | bytes 3145736 | tf_op jit(solution)/shard_map/ppermute | solution.py:394
  46.2 20.0 %all-to-all-start.1 = ((bf16[8,256,128]{2,1,0:T(8,128)(2,1)}), bf16[8,256,128]{2,1,0:T(8,128)(2,1)S(1)}, u32[]{:S(2)}, u32[]{:S(2)}) async-start(bf16[8,256,128]{2,1,0:T(8,128)(2,1)} %prefix.1), calls=%async_computation.1 | async-start | bytes 1048576 | tf_op jit(solution)/shard_map/all_to_all | solution.py:494
  51.0 14.9 %collective-permute-start.5 = (bf16[128,2048]{1,0:T(8,128)(2,1)}, bf16[128,2048]{1,0:T(8,128)(2,1)}, u32[]{:S(2)}, u32[]{:S(2)}) collective-permute-start(bf16[128,2048]{1,0:T(8,128)(2,1)} %collective-permute-done.2.refs_2_), channel_id=1, source_target_pairs={{0,1},{1,0},{2,3},{3,2},{4,5},{5,4},{6,7},{7,6},{8,9},{9,8},{10,11... | collective-permute-start | bytes 1572872 | tf_op jit(solution)/shard_map/ppermute | solution.py:392
  60.1 5.8 %collective-permute-start.6 = (bf16[128,2048]{1,0:T(8,128)(2,1)}, bf16[128,2048]{1,0:T(8,128)(2,1)}, u32[]{:S(2)}, u32[]{:S(2)}) collective-permute-start(bf16[128,2048]{1,0:T(8,128)(2,1)} %collective-permute-done.3.refs_3_), channel_id=1, source_target_pairs={{0,1},{1,0},{2,3},{3,2},{4,5},{5,4},{6,7},{7,6},{8,9},{9,8},{10,11... | collective-permute-start | bytes 1572872 | tf_op jit(solution)/shard_map/ppermute | solution.py:393
  64.3 1.9 copy-start.12
  64.3 1.9 copy-start.13
  64.3 1.9 copy-start.17
  73.4 27.1 %collective-permute-start.9 = (bf16[128,2048]{1,0:T(8,128)(2,1)}, bf16[128,2048]{1,0:T(8,128)(2,1)S(1)}, u32[]{:S(2)}, u32[]{:S(2)}) collective-permute-start(bf16[128,2048]{1,0:T(8,128)(2,1)} %get-tuple-element.23.x_in), channel_id=1, source_target_pairs={{0,16},{16,0},{1,17},{17,1},{2,18},{18,2},{3,19},{19,3},{4,20},{20... | collective-permute-start | bytes 1572872 | tf_op jit(solution)/shard_map/ppermute | solution.py:539
  76.3 24.2 %collective-permute-start.8 = (f32[8,128]{1,0:T(8,128)S(1)}, f32[8,128]{1,0:T(8,128)S(1)}, u32[]{:S(2)}, u32[]{:S(2)}) collective-permute-start(f32[8,128]{1,0:T(8,128)S(1)} %maximum_maximum_fusion.meta_ref), channel_id=1, source_target_pairs={{0,16},{16,0},{1,17},{17,1},{2,18},{18,2},{3,19},{19,3},{4,20},{20... | collective-permute-start | bytes 12296 | tf_op jit(solution)/shard_map/ppermute | solution.py:432
  102.5 24.6 %copy-start = (bf16[1,2048,512]{2,1,0:T(8,128)(2,1)S(1)}, bf16[1,2048,512]{2,1,0:T(8,128)(2,1)}, u32[]{:S(2)}) copy-start(bf16[1,2048,512]{2,1,0:T(8,128)(2,1)} %wg_ref.3) | copy-start | bytes 6291460
  123.5 19.8 %all-to-all-start.2 = ((bf16[16,16,2048]{2,1,0:T(8,128)(2,1)}), bf16[16,16,2048]{2,1,0:T(8,128)(2,1)S(1)}, u32[]{:S(2)}, u32[]{:S(2)}) async-start(bf16[16,16,2048]{2,1,0:T(8,128)(2,1)} %bitcast.64), calls=%async_computation.2 | async-start | bytes 2097152 | tf_op jit(solution)/shard_map/all_to_all | solution.py:544
  127.1 1.2 copy-start.3
  132.6 1.0 copy-start.2
  143.2 20.5 %all-to-all-start.5 = ((bf16[16,16,2048]{2,1,0:T(8,128)(2,1)}), bf16[16,16,2048]{2,1,0:T(8,128)(2,1)}, u32[]{:S(2)}, u32[]{:S(2)}) async-start(bf16[16,16,2048]{2,1,0:T(8,128)(2,1)} %bitcast.44), calls=%async_computation.5 | async-start | bytes 2097152 | tf_op jit(solution)/shard_map/all_to_all | solution.py:544
  152.0 1.0 copy-start.1
  163.7 27.8 %all-to-all-start.3 = ((bf16[16,16,2048]{2,1,0:T(8,128)(2,1)}), bf16[16,16,2048]{2,1,0:T(8,128)(2,1)S(1)}, u32[]{:S(2)}, u32[]{:S(2)}) async-start(bf16[16,16,2048]{2,1,0:T(8,128)(2,1)} %bitcast.42), calls=%async_computation.3 | async-start | bytes 2097152 | tf_op jit(solution)/shard_map/all_to_all | solution.py:544
  170.5 26.6 %collective-permute-start.10 = (bf16[128,2048]{1,0:T(8,128)(2,1)}, bf16[128,2048]{1,0:T(8,128)(2,1)S(1)}, u32[]{:S(2)}, u32[]{:S(2)}) collective-permute-start(bf16[128,2048]{1,0:T(8,128)(2,1)} %part.1), channel_id=1, source_target_pairs={{0,16},{16,0},{1,17},{17,1},{2,18},{18,2},{3,19},{19,3},{4,20},{20... | collective-permute-start | bytes 1572872 | tf_op jit(solution)/shard_map/ppermute | solution.py:622
  197.1 1.2 copy-start.4

commit v4 on v3

--- a/solution.py
+++ b/solution.py
@@ -206,14 +206,25 @@
     return functools.reduce(jnp.logical_or, found).astype(BF16)
 
 
-def weighted(meta, experts, slots, half, got):
-    lane = (iota((meta.shape[1], got.shape[0]), 1) + half * got.shape[0]).astype(F32)
+def shares(meta, experts, slots, half, rows):
+    lane = (iota((meta.shape[1], rows), 1) + half * rows).astype(F32)
     w = jnp.zeros(lane.shape, F32)
     for s, value in slot_of(meta, experts, slots):
         w = w + jnp.where(lane == s, value, 0.0)
     high = w.astype(BF16)
-    low = (w - high.astype(F32)).astype(BF16)
-    return dot(high, got, 1, 0) + dot(low, got, 1, 0)
+    return high, (w - high.astype(F32)).astype(BF16)
+
+
+def weighted(shares_ref, got):
+    return dot(shares_ref[0], got, 1, 0) + dot(shares_ref[1], got, 1, 0)
+
+
+def plan_kernel(experts, slots, half_ref, meta_ref, far_ref, hit_ref, near_ref, over_ref):
+    rows = hit_ref.shape[1]
+    half = half_ref[0]
+    hit_ref[...] = hits(far_ref[...], experts, slots, half, rows)
+    for meta, ref in ((meta_ref, near_ref), (far_ref, over_ref)):
+        ref[0], ref[1] = shares(meta[...], experts, slots, half, rows)
 
 
 def warm_kernel(*refs):
@@ -310,12 +321,22 @@
         copy.wait()
 
 
-def relay_kernel(experts, slots, half_ref, meta_ref, x_in, send_ref, x_ref, sbuf, sem_x, sem):
-    copy = pltpu.make_async_copy(x_in, x_ref, sem_x)
-    copy.start()
-    hit = hits(meta_ref[...], experts, slots, half_ref[0], send_ref.shape[0])
-    copy.wait()
-    place_rows(hit, x_ref[...], sbuf, send_ref, sem)
+def relay_kernel(hit_ref, x_in, send_ref, x_ref, sbuf, sem_x, sem):
+    pieces = sem.shape[0]
+    step = x_ref.shape[1] // pieces
+    wide = [pl.ds(i * step, step) for i in range(pieces)]
+    gets = [pltpu.make_async_copy(x_in.at[:, w], x_ref.at[:, w], sem_x.at[i]) for i, w in enumerate(wide)]
+    puts = [pltpu.make_async_copy(sbuf.at[:, w], send_ref.at[:, w], sem.at[i]) for i, w in enumerate(wide)]
+    for get in gets:
+        get.start()
+    hit = hit_ref[...]
+    for i in range(pieces):
+        gets[i].wait()
+        at = slice(i * step, (i + 1) * step)
+        sbuf[:, at] = dot(hit, x_ref[:, at], 0, 0).astype(BF16)
+        puts[i].start()
+    for put in puts:
+        put.wait()
 
 
 def shared_kernel(x_in, mixed_in, wg_in, wu_in, wd_in, out_ref, x_ref, m_ref, wg, wu, wd, sem):
@@ -365,16 +386,19 @@
             copy.wait()
 
 
-def part_kernel(experts, slots, half_ref, meta_ref, got_ref, out_ref, obuf, sem):
-    obuf[...] = weighted(meta_ref[...], experts, slots, half_ref[0], got_ref[...]).astype(BF16)
+def part_kernel(shares_ref, got_ref, out_ref, obuf, sem):
+    obuf[...] = weighted(shares_ref, got_ref[...]).astype(BF16)
     copy = pltpu.make_async_copy(obuf, out_ref, sem)
     copy.start()
     copy.wait()
 
 
-def combine_kernel(experts, slots, half_ref, meta_ref, got_ref, base_ref, other_ref, out_ref):
-    own = weighted(meta_ref[...], experts, slots, half_ref[0], got_ref[...])
-    out_ref[...] = (base_ref[...] + own + other_ref[...].astype(F32)).astype(BF16)
+def sum_kernel(base_ref, other_ref, out_ref):
+    out_ref[...] = base_ref[...] + other_ref[...].astype(F32)
+
+
+def combine_kernel(shares_ref, got_ref, base_ref, out_ref):
+    out_ref[...] = (base_ref[...] + weighted(shares_ref, got_ref[...])).astype(BF16)
 
 
 def gather_rows(w, ways, span):
@@ -386,7 +410,8 @@
         core = [(j, j ^ 1) for j in range(4)]
         flip = [(j, j ^ 1) for j in range(lax.axis_size("sub"))]
         xa = lax.ppermute(lax.dynamic_slice_in_dim(w, odd * part, part, 0), "dp", over)
-        xb = lax.ppermute(w[span:], "dp", over)
+        low = w[span:]
+        xb = lax.ppermute(low, "dp", over)
         ya = lax.ppermute(xa, "sub", flip)
         beside = lax.ppermute(w, "dp", core)
         fa = lax.ppermute(xa, "dp", core)
@@ -591,45 +616,67 @@
         name="shared",
     )(x, mixed, shared_gate, shared_up, shared_down)
     near = serve(near)
+    hit_far, near_shares, far_shares = pl.pallas_call(
+        functools.partial(plan_kernel, experts, slots),
+        out_shape=(
+            jax.ShapeDtypeStruct((tokens, rows), BF16),
+            jax.ShapeDtypeStruct((2, tokens, rows), BF16),
+            jax.ShapeDtypeStruct((2, tokens, rows), BF16),
+        ),
+        in_specs=[sm, vm, vm],
+        out_specs=(vm,) * 3,
+        compiler_params=vmem(24),
+        cost_estimate=cost(1 << 27, 1 << 19),
+        name="plan",
+    )(half[None], meta, meta_far)
     relay = pl.pallas_call(
-        functools.partial(relay_kernel, experts, slots),
-        out_shape=jax.ShapeDtypeStruct((rows, features), BF16),
-        in_specs=[sm, vm, hbm],
+        relay_kernel,
+        out_shape=pltpu.HBM((rows, features), BF16),
+        in_specs=[vm, hbm],
         out_specs=hbm,
         scratch_shapes=[
             pltpu.VMEM((tokens, features), BF16),
             pltpu.VMEM((rows, features), BF16),
-            pltpu.SemaphoreType.DMA,
+            pltpu.SemaphoreType.DMA((pieces,)),
             pltpu.SemaphoreType.DMA((pieces,)),
         ],
         compiler_params=vmem(32),
         cost_estimate=cost(1 << 28, 3 * MIB),
         name="relay",
-    )(half[None], meta_far, x_far)
+    )(hit_far, x_far)
     far = exchange(relay)
     far = serve(far)
     far = exchange(far)
     part = pl.pallas_call(
-        functools.partial(part_kernel, experts, slots),
-        out_shape=jax.ShapeDtypeStruct((tokens, features), BF16),
-        in_specs=[sm, vm, vm],
+        part_kernel,
+        out_shape=pltpu.HBM((tokens, features), BF16),
+        in_specs=[vm, vm],
         out_specs=hbm,
         scratch_shapes=[pltpu.VMEM((tokens, features), BF16), pltpu.SemaphoreType.DMA],
         compiler_params=vmem(32),
         cost_estimate=cost(1 << 29, 3 * MIB),
         name="part",
-    )(half[None], meta_far, far.reshape(rows, features))
+    )(far_shares, far.reshape(rows, features))
     other = lax.ppermute(part, "half", mirror)
     near = exchange(near)
+    base = pl.pallas_call(
+        sum_kernel,
+        out_shape=jax.ShapeDtypeStruct((tokens, features), F32),
+        in_specs=[vm, vm],
+        out_specs=vm,
+        compiler_params=vmem(32),
+        cost_estimate=cost(1 << 20, 3 * MIB),
+        name="sum",
+    )(base, other)
     out = pl.pallas_call(
-        functools.partial(combine_kernel, experts, slots),
+        combine_kernel,
         out_shape=jax.ShapeDtypeStruct((tokens, features), BF16),
-        in_specs=[sm] + [vm] * 4,
+        in_specs=[vm] * 3,
         out_specs=vm,
         compiler_params=vmem(32),
         cost_estimate=cost(1 << 29, 4 * MIB),
         name="combine",
-    )(half[None], meta, near.reshape(rows, features), base, other)
+    )(near_shares, near.reshape(rows, features), base)
     return out[None]
 
 

time: 201 us -> 201 us (level)
    all_to_all x3, waiting for transfers between devices: 35 us -> 20.4 us  [exchange(): return lax.all_to_all(v, group, split_axis=0, concat_axis=0, tiled=True)]
    ppermute x1, waiting for transfers between devices: 5.56 us -> 20.1 us  [layer(): other = lax.ppermute(part, 'half', mirror)]
    pallas_call x3 -> x5, Pallas kernels: 6.99 us -> 6.99 us  [the longest x1 2.49 us: layer(): pl.pallas_call(part_kernel, out_shape=pltpu.HBM((tokens, features), BF16)...]
    unnamed x40 -> x42, local copies, waits for them, and re-layouts: 4.48 us -> 4.48 us
  transfers between devices with their start and end apart: 16 -> 16, of which waited for: 8 -> 7; matrix products, arithmetic and copies ran while one was open for 1% -> 1% of each run, Pallas kernels for 13% -> 13%
where the time goes in v4:
time: 201 us; the launch traced here: 200 us
  waiting for transfers between devices  96.2 us (48%)
  Pallas kernels  37.8 us (19%)
  starting transfers between devices  37.4 us (19%)
  blocking collectives  21.1 us (10%)
  local copies, waits for them, and re-layouts  7.01 us (3%)
    ppermute x1, waiting for transfers between devices, layer(): meta_far = lax.ppermute(meta, 'half', mirror)  23.8 us
    ppermute x1, waiting for transfers between devices, gather_rows(): lax.ppermute(lax.dynamic_slice_in_dim(w, odd * part, part, 0), 'dp', over)  22.8 us
    all_to_all x1, blocking collectives, exchange(): return lax.all_to_all(v, group, split_axis=0, concat_axis=0, tiled=True)  21.1 us
    all_to_all x3, waiting for transfers between devices, exchange(): return lax.all_to_all(v, group, split_axis=0, concat_axis=0, tiled=True)  20.4 us
    ppermute x1, waiting for transfers between devices, layer(): other = lax.ppermute(part, 'half', mirror)  20.1 us
    all_to_all x3, starting transfers between devices, exchange(): return lax.all_to_all(v, group, split_axis=0, concat_axis=0, tiled=True)  11.8 us
    ppermute x1, waiting for transfers between devices, gather_rows(): ya = lax.ppermute(xa, 'sub', flip)  8.59 us
    pallas_call x2, Pallas kernels, serve(): pl.pallas_call(expert_kernel, out_shape=jax.ShapeDtypeStruct((own, m, fea...  8.47 us
  transfers between devices with their start and end apart: 16, of which 7 were waited for; matrix products, arithmetic and copies ran while one was open for 1% of the time, Pallas kernels for 13%

profile of v4, /device:TPU:0, one launch (start us, length us, event | category | flops | bytes accessed | tf_op | source)
XLA Modules:
  0.0 199.9 jit_solution(4787947364984046910)
XLA Ops:
  0.0 0.0 copy-start.8
  0.0 0.0 copy-start.10
  0.0 1.5 tails.1
  1.5 4.9 %collective-permute-start.1 = (bf16[8,4096]{1,0:T(8,128)(2,1)}, bf16[8,4096]{1,0:T(8,128)(2,1)S(1)}, u32[]{:S(2)}, u32[]{:S(2)}) collective-permute-start(bf16[8,4096]{1,0:T(8,128)(2,1)} %tails.1), channel_id=1, source_target_pairs={{0,4},{4,8},{8,12},{12,16},{16,20},{20,24},{24,28},{1,5},{5,9},{9,... | collective-permute-start | bytes 196616 | tf_op jit(solution)/shard_map/ppermute | solution.py:475
  6.4 1.3 slice.3
  7.7 1.6 collective-permute-start.5
  9.3 0.0 collective-permute-start.2
  9.3 0.0 collective-permute-done.1.tail_ref
  9.4 2.8 %states.1 = bf16[8,264,128]{2,1,0:T(8,128)(2,1)} custom-call(bf16[32,128]{1,0:T(8,128)(2,1)S(1)} %bitcast.54, f32[1,32]{1,0:T(1,128)S(1)} %bitcast.58, f32[1,32]{1,0:T(1,128)S(1)} %bitcast.60, bf16[8,4096]{1,0:T(8,128)(2,1)S(1)} %collective-permute-done.1.tail_ref, bf16[4,2048]{1,0:T(4,128)(2,1)S(1)} %copy-done.8, bf16[4,1024]{1,0:T(4,128)(2,1)S(1)} %copy-done.10, ...), custom_call_target="tpu_custom_call" | custom-call | flops 1073741824 | bytes 4194304 | tf_op jit(solution)/shard_map/states/pallas_call | solution.py:476
  12.2 0.0 copy-start.16
  12.2 6.0 %all-to-all-start = ((bf16[8,264,128]{2,1,0:T(8,128)(2,1)}), bf16[8,264,128]{2,1,0:T(8,128)(2,1)S(1)}, u32[]{:S(2)}, u32[]{:S(2)}) async-start(bf16[8,264,128]{2,1,0:T(8,128)(2,1)} %states.1), calls=%async_computation | async-start | bytes 1081344 | tf_op jit(solution)/shard_map/all_to_all | solution.py:489
  18.2 1.1 constant_dynamic-slice_fusion
  19.3 1.6 collective-permute-start.3
  20.8 22.8 %collective-permute-done.3.refs_2_ = bf16[128,2048]{1,0:T(8,128)(2,1)S(1)} collective-permute-done((bf16[128,2048]{1,0:T(8,128)(2,1)S(1)}, bf16[128,2048]{1,0:T(8,128)(2,1)S(1)}, u32[]{:S(2)}, u32[]{:S(2)}) %collective-permute-start.3) | collective-permute-done | bytes 524320 | tf_op jit(solution)/shard_map/ppermute | solution.py:412
  43.7 1.5 collective-permute-start.4
  45.2 0.0 collective-permute-done.5.refs_4_
  45.2 0.0 collective-permute-start.8
  45.2 0.0 all-to-all-done.in_ref
  45.2 0.9 prefix.1
  46.1 4.8 %all-to-all-start.1 = ((bf16[8,256,128]{2,1,0:T(8,128)(2,1)}), bf16[8,256,128]{2,1,0:T(8,128)(2,1)S(1)}, u32[]{:S(2)}, u32[]{:S(2)}) async-start(bf16[8,256,128]{2,1,0:T(8,128)(2,1)} %prefix.1), calls=%async_computation.1 | async-start | bytes 1048576 | tf_op jit(solution)/shard_map/all_to_all | solution.py:519
  50.9 0.2 collective-permute-start.6
  51.2 8.6 %collective-permute-done.4.refs_3_ = bf16[128,2048]{1,0:T(8,128)(2,1)} collective-permute-done((bf16[128,2048]{1,0:T(8,128)(2,1)S(1)}, bf16[128,2048]{1,0:T(8,128)(2,1)}, u32[]{:S(2)}, u32[]{:S(2)}) %collective-permute-start.4) | collective-permute-done | bytes 524320 | tf_op jit(solution)/shard_map/ppermute | solution.py:415
  59.8 0.0 collective-permute-start.7
  59.8 0.1 pad.2.clone
  59.9 0.1 stack.40.order_ref
  59.9 0.1 maximum_maximum_fusion.meta_ref
  60.0 0.0 copy-done.11
  60.0 3.9 %within.1 = (f32[128,2048]{1,0:T(8,128)}, f32[32,128]{1,0:T(8,128)}, bf16[128,1024]{1,0:T(8,128)(2,1)}) custom-call(bf16[32,128]{1,0:T(8,128)(2,1)S(1)} %bitcast.55, f32[1,32]{1,0:T(1,128)S(1)} %bitcast.59, f32[1,32]{1,0:T(1,128)S(1)} %bitcast.61, f32[1,32]{1,0:T(1,128)S(1)} %bitcast.62, bf16[8,4096]{1,0:T(8,128)(2,1)S(1)} %collective-permute-done.1.tail_ref, ...), custom_call_target="tpu_custom_call" | custom-call | flops 2147483648 | bytes 8388608 | tf_op jit(solution)/shard_map/within/pallas_call | solution.py:490
  63.9 1.7 warm.1
  65.6 0.0 collective-permute-done.6.refs_5_
  65.6 0.0 collective-permute-done.7.refs_6_
  65.6 0.5 all-to-all-done.1
  66.1 0.0 collective-permute-done.8.refs_7_
  66.1 0.0 collective-permute-done.2.refs_1_
  66.1 0.0 copy-done.13
  66.1 0.0 copy-done.17
  66.1 7.1 %mix.1 = (bf16[128,2048]{1,0:T(8,128)(2,1)}, bf16[128,2048]{1,0:T(8,128)(2,1)}, bf16[256,2048]{1,0:T(8,128)(2,1)}) custom-call(s32[10]{0:T(128)S(1)} %stack.40.order_ref, f32[1,2048]{1,0:T(1,128)S(1)} %bitcast.56, f32[1,2048]{1,0:T(1,128)S(1)} %bitcast.57, f32[8,128]{1,0:T(8,128)S(1)} %maximum_maximum_fusion.meta_ref, f32[32,128]{1,0:T(8,128)S(1)} %copy-done.17, ...), custom_call_target="tpu_custom_call" | custom-call | flops 3221225472 | bytes 16777216 | tf_op jit(solution)/shard_map/mix/pallas_call | solution.py:535
  73.3 2.6 %collective-permute-start.9 = (bf16[128,2048]{1,0:T(8,128)(2,1)}, bf16[128,2048]{1,0:T(8,128)(2,1)S(1)}, u32[]{:S(2)}, u32[]{:S(2)}) collective-permute-start(bf16[128,2048]{1,0:T(8,128)(2,1)} %get-tuple-element.27.x_in), channel_id=1, source_target_pairs={{0,16},{16,0},{1,17},{17,1},{2,18},{18,2},{3,19},{19,3},{4,20},{20... | collective-permute-start | bytes 1572872 | tf_op jit(solution)/shard_map/ppermute | solution.py:564
  75.9 0.4 collective-permute-start
  76.3 23.8 %collective-permute-done.far_ref = f32[8,128]{1,0:T(8,128)S(1)} collective-permute-done((f32[8,128]{1,0:T(8,128)S(1)}, f32[8,128]{1,0:T(8,128)S(1)}, u32[]{:S(2)}, u32[]{:S(2)}) %collective-permute-start) | collective-permute-done | bytes 4128 | tf_op jit(solution)/shard_map/ppermute | solution.py:457
  100.1 1.3 plan.1
  101.4 0.0 collective-permute-done.9.x_in
  101.4 1.8 relay.1
  103.3 0.0 copy-start
  103.3 21.1 %all_to_all.30 = bf16[16,16,2048]{2,1,0:T(8,128)(2,1)} all-to-all(bf16[16,16,2048]{2,1,0:T(8,128)(2,1)} %bitcast.63), channel_id=1, replica_groups=mesh['half'=2,'sub'=4,'dp'=4] {'sub','dp'}, dimensions={0} | all-to-all | bytes 2097152 | tf_op jit(solution)/shard_map/all_to_all | solution.py:569
  124.3 3.7 %all-to-all-start.2 = ((bf16[16,16,2048]{2,1,0:T(8,128)(2,1)}), bf16[16,16,2048]{2,1,0:T(8,128)(2,1)S(1)}, u32[]{:S(2)}, u32[]{:S(2)}) async-start(bf16[16,16,2048]{2,1,0:T(8,128)(2,1)} %bitcast.64), calls=%async_computation.2 | async-start | bytes 2097152 | tf_op jit(solution)/shard_map/all_to_all | solution.py:569
  128.0 1.2 copy-done.4
  129.2 4.2 %experts.3 = bf16[1,256,2048]{2,1,0:T(8,128)(2,1)S(1)} custom-call(bf16[1,256,2048]{2,1,0:T(8,128)(2,1)S(1)} %bitcast.44, bf16[1,2048,512]{2,1,0:T(8,128)(2,1)S(1)} %copy-done, bf16[1,2048,512]{2,1,0:T(8,128)(2,1)} %wu_ref.3, bf16[1,512,2048]{2,1,0:T(8,128)(2,1)} %wd_ref.3), custom_call_target="tpu_custom_call" | custom-call | flops 2147483648 | bytes 8388608 | tf_op jit(solution)/shard_map/experts/pallas_call | solution.py:580
  133.5 1.0 copy-done.2
  134.4 9.6 %all-to-all-done.2 = bf16[16,16,2048]{2,1,0:T(8,128)(2,1)S(1)} async-done(((bf16[16,16,2048]{2,1,0:T(8,128)(2,1)}), bf16[16,16,2048]{2,1,0:T(8,128)(2,1)S(1)}, u32[]{:S(2)}, u32[]{:S(2)}) %all-to-all-start.2) | async-done | bytes 1048608 | tf_op jit(solution)/shard_map/all_to_all | solution.py:569
  144.1 4.5 %all-to-all-start.5 = ((bf16[16,16,2048]{2,1,0:T(8,128)(2,1)}), bf16[16,16,2048]{2,1,0:T(8,128)(2,1)}, u32[]{:S(2)}, u32[]{:S(2)}) async-start(bf16[16,16,2048]{2,1,0:T(8,128)(2,1)} %bitcast.43), calls=%async_computation.5 | async-start | bytes 2097152 | tf_op jit(solution)/shard_map/all_to_all | solution.py:569
  148.6 4.2 %experts.2 = bf16[1,256,2048]{2,1,0:T(8,128)(2,1)S(1)} custom-call(bf16[1,256,2048]{2,1,0:T(8,128)(2,1)S(1)} %bitcast.42, bf16[1,2048,512]{2,1,0:T(8,128)(2,1)S(1)} %copy-done, bf16[1,2048,512]{2,1,0:T(8,128)(2,1)} %wu_ref.3, bf16[1,512,2048]{2,1,0:T(8,128)(2,1)} %wd_ref.3), custom_call_target="tpu_custom_call" | custom-call | flops 2147483648 | bytes 8388608 | tf_op jit(solution)/shard_map/experts/pallas_call | solution.py:580
  152.9 0.0 copy-start.1
  152.9 1.0 copy-done.1
  153.9 10.7 %all-to-all-done.5 = bf16[16,16,2048]{2,1,0:T(8,128)(2,1)} async-done(((bf16[16,16,2048]{2,1,0:T(8,128)(2,1)}), bf16[16,16,2048]{2,1,0:T(8,128)(2,1)}, u32[]{:S(2)}, u32[]{:S(2)}) %all-to-all-start.5) | async-done | bytes 1048608 | tf_op jit(solution)/shard_map/all_to_all | solution.py:569
  164.6 3.7 %all-to-all-start.3 = ((bf16[16,16,2048]{2,1,0:T(8,128)(2,1)}), bf16[16,16,2048]{2,1,0:T(8,128)(2,1)S(1)}, u32[]{:S(2)}, u32[]{:S(2)}) async-start(bf16[16,16,2048]{2,1,0:T(8,128)(2,1)} %bitcast.41), calls=%async_computation.3 | async-start | bytes 2097152 | tf_op jit(solution)/shard_map/all_to_all | solution.py:569
  168.2 2.5 %part.1 = bf16[128,2048]{1,0:T(8,128)(2,1)} custom-call(bf16[2,128,256]{2,1,0:T(8,128)(2,1)S(1)} %get-tuple-element.29.shares_ref, bf16[256,2048]{1,0:T(8,128)(2,1)} %bitcast.35.got_ref), custom_call_target="tpu_custom_call" | custom-call | flops 536870912 | bytes 3145728 | tf_op jit(solution)/shard_map/part/pallas_call | solution.py:650
  170.7 1.9 collective-permute-start.10
  172.6 4.6 %shared.1.base_ref = f32[128,2048]{1,0:T(8,128)} custom-call(bf16[128,2048]{1,0:T(8,128)(2,1)} %get-tuple-element.27.x_in, bf16[128,2048]{1,0:T(8,128)(2,1)} %get-tuple-element.28.mixed_in, bf16[2048,512]{1,0:T(8,128)(2,1)} %wg_in.1, bf16[2048,512]{1,0:T(8,128)(2,1)} %wu_in.1, bf16[512,2048]{1,0:T(8,128)(2,1)} %wd_in.1), custom_call_target="tpu_custom_call" | custom-call | flops 1073741824 | bytes 8388608 | tf_op jit(solution)/shard_map/shared/pallas_call | solution.py:605
  177.2 20.1 %collective-permute-done.10.other_ref = bf16[128,2048]{1,0:T(8,128)(2,1)S(1)} collective-permute-done((bf16[128,2048]{1,0:T(8,128)(2,1)}, bf16[128,2048]{1,0:T(8,128)(2,1)S(1)}, u32[]{:S(2)}, u32[]{:S(2)}) %collective-permute-start.10) | collective-permute-done | bytes 524320 | tf_op jit(solution)/shard_map/ppermute | solution.py:660
  197.3 1.2 copy-done.3
  198.5 0.1 sum.1.base_ref
  198.6 0.0 all-to-all-done.3
  198.6 1.2 combine.1
  (32 shorter events, 0.1 us)
Async XLA Ops:
  0.0 9.3 %copy-start.5 = (bf16[1,128,2048]{2,1,0:T(8,128)(2,1)S(1)}, bf16[1,128,2048]{2,1,0:T(8,128)(2,1)}, u32[]{:S(2)}) copy-start(bf16[1,128,2048]{2,1,0:T(8,128)(2,1)} %param.24) | copy-start | bytes 1572868
  0.0 9.3 %copy-start.6 = (bf16[1,128,1024]{2,1,0:T(8,128)(2,1)S(1)}, bf16[1,128,1024]{2,1,0:T(8,128)(2,1)}, u32[]{:S(2)}) copy-start(bf16[1,128,1024]{2,1,0:T(8,128)(2,1)} %param.26) | copy-start | bytes 786436
  0.0 9.3 %copy-start.9 = (bf16[1,128,32]{1,2,0:T(8,128)(2,1)S(1)}, bf16[1,128,32]{1,2,0:T(8,128)(2,1)}, u32[]{:S(2)}) copy-start(bf16[1,128,32]{1,2,0:T(8,128)(2,1)} %param.28) | copy-start | bytes 24580
  0.0 9.3 %copy-start.14 = (f32[32]{0:T(128)S(1)}, f32[32]{0:T(128)}, u32[]{:S(2)}) copy-start(f32[32]{0:T(128)} %param.32) | copy-start | bytes 388
  0.0 9.3 %copy-start.15 = (f32[32]{0:T(128)S(1)}, f32[32]{0:T(128)}, u32[]{:S(2)}) copy-start(f32[32]{0:T(128)} %param.33) | copy-start | bytes 388
  0.0 9.3 %copy-start.8 = (bf16[4,2048]{1,0:T(4,128)(2,1)S(1)}, bf16[4,2048]{1,0:T(4,128)(2,1)}, u32[]{:S(2)}) copy-start(bf16[4,2048]{1,0:T(4,128)(2,1)} %wx_ref.3) | copy-start | bytes 49156
  0.0 9.3 %copy-start.10 = (bf16[4,1024]{1,0:T(4,128)(2,1)S(1)}, bf16[4,1024]{1,0:T(4,128)(2,1)}, u32[]{:S(2)}) copy-start(bf16[4,1024]{1,0:T(4,128)(2,1)} %wb_ref.3) | copy-start | bytes 24580
  1.5 7.8 %collective-permute-start.1 = (bf16[8,4096]{1,0:T(8,128)(2,1)}, bf16[8,4096]{1,0:T(8,128)(2,1)S(1)}, u32[]{:S(2)}, u32[]{:S(2)}) collective-permute-start(bf16[8,4096]{1,0:T(8,128)(2,1)} %tails.1), channel_id=1, source_target_pairs={{0,4},{4,8},{8,12},{12,16},{16,20},{20,24},{24,28},{1,5},{5,9},{9,... | collective-permute-start | bytes 196616 | tf_op jit(solution)/shard_map/ppermute | solution.py:475
  7.7 37.4 %collective-permute-start.5 = (bf16[256,2048]{1,0:T(8,128)(2,1)S(1)}, bf16[256,2048]{1,0:T(8,128)(2,1)}, u32[]{:S(2)}, u32[]{:S(2)}) collective-permute-start(bf16[256,2048]{1,0:T(8,128)(2,1)S(1)} %slice.3), channel_id=1, source_target_pairs={{0,2},{1,3},{2,0},{3,1},{4,6},{5,7},{6,4},{7,5},{8,10},{9,11},{10,... | collective-permute-start | bytes 3145736 | tf_op jit(solution)/shard_map/ppermute | solution.py:414
  9.3 56.8 %collective-permute-start.2 = (bf16[512,2048]{1,0:T(8,128)(2,1)}, bf16[512,2048]{1,0:T(8,128)(2,1)}, u32[]{:S(2)}, u32[]{:S(2)}) collective-permute-start(bf16[512,2048]{1,0:T(8,128)(2,1)} %refs_0_.1), channel_id=1, source_target_pairs={{0,1},{1,0},{2,3},{3,2},{4,5},{5,4},{6,7},{7,6},{8,9},{9,8},{10,11... | collective-permute-start | bytes 6291464 | tf_op jit(solution)/shard_map/ppermute | solution.py:416
  12.1 47.6 %copy-start.18 = (s32[1,128,2]{1,2,0:T(2,128)S(1)}, s32[1,128,2]{1,2,0:T(2,128)}, u32[]{:S(2)}) copy-start(s32[1,128,2]{1,2,0:T(2,128)} %param.44) | copy-start | bytes 3076
  12.1 47.8 %copy-start.19 = (f32[1,128,2]{1,2,0:T(2,128)S(1)}, f32[1,128,2]{1,2,0:T(2,128)}, u32[]{:S(2)}) copy-start(f32[1,128,2]{1,2,0:T(2,128)} %param.45) | copy-start | bytes 3076
  12.1 47.9 %copy-start.7 = (bf16[1,128,1024]{2,1,0:T(8,128)(2,1)S(1)}, bf16[1,128,1024]{2,1,0:T(8,128)(2,1)}, u32[]{:S(2)}) copy-start(bf16[1,128,1024]{2,1,0:T(8,128)(2,1)} %param.27) | copy-start | bytes 786436
  12.1 47.9 %copy-start.11 = (bf16[4,1024]{1,0:T(4,128)(2,1)S(1)}, bf16[4,1024]{1,0:T(4,128)(2,1)}, u32[]{:S(2)}) copy-start(bf16[4,1024]{1,0:T(4,128)(2,1)} %wc_ref.1) | copy-start | bytes 24580
  12.2 47.9 %copy-start.16 = (f32[32]{0:T(128)S(1)}, f32[32]{0:T(128)}, u32[]{:S(2)}) copy-start(f32[32]{0:T(128)} %param.34) | copy-start | bytes 388
  12.2 33.0 %all-to-all-start = ((bf16[8,264,128]{2,1,0:T(8,128)(2,1)}), bf16[8,264,128]{2,1,0:T(8,128)(2,1)S(1)}, u32[]{:S(2)}, u32[]{:S(2)}) async-start(bf16[8,264,128]{2,1,0:T(8,128)(2,1)} %states.1), calls=%async_computation | async-start | bytes 1081344 | tf_op jit(solution)/shard_map/all_to_all | solution.py:489
  19.3 24.4 %collective-permute-start.3 = (bf16[128,2048]{1,0:T(8,128)(2,1)S(1)}, bf16[128,2048]{1,0:T(8,128)(2,1)S(1)}, u32[]{:S(2)}, u32[]{:S(2)}) collective-permute-start(bf16[128,2048]{1,0:T(8,128)(2,1)S(1)} %constant_dynamic-slice_fusion), channel_id=1, source_target_pairs={{0,2},{1,3},{2,0},{3,1},{4,6},{5,7},{6,4},{7,5},{8,10},{9,11},{10,... | collective-permute-start | bytes 1572872 | tf_op jit(solution)/shard_map/ppermute | solution.py:412
  43.7 20.2 %copy-start.20 = (bf16[128,2048]{1,0:T(8,128)(2,1)}, bf16[128,2048]{1,0:T(8,128)(2,1)S(1)}, u32[]{:S(2)}) copy-start(bf16[128,2048]{1,0:T(8,128)(2,1)S(1)} %collective-permute-done.3.refs_2_) | copy-start | bytes 1572868
  43.7 16.1 %collective-permute-start.4 = (bf16[128,2048]{1,0:T(8,128)(2,1)S(1)}, bf16[128,2048]{1,0:T(8,128)(2,1)}, u32[]{:S(2)}, u32[]{:S(2)}) collective-permute-start(bf16[128,2048]{1,0:T(8,128)(2,1)S(1)} %collective-permute-done.3.refs_2_), channel_id=1, source_target_pairs={{0,4},{4,0},{8,12},{12,8},{1,5},{5,1},{9,13},{13,9},{2,6},{6,2},{1... | collective-permute-start | bytes 1572872 | tf_op jit(solution)/shard_map/ppermute | solution.py:415
  45.2 20.9 %collective-permute-start.8 = (bf16[256,2048]{1,0:T(8,128)(2,1)}, bf16[256,2048]{1,0:T(8,128)(2,1)}, u32[]{:S(2)}, u32[]{:S(2)}) collective-permute-start(bf16[256,2048]{1,0:T(8,128)(2,1)} %collective-permute-done.5.refs_4_), channel_id=1, source_target_pairs={{0,1},{1,0},{2,3},{3,2},{4,5},{5,4},{6,7},{7,6},{8,9},{9,8},{10,11... | collective-permute-start | bytes 3145736 | tf_op jit(solution)/shard_map/ppermute | solution.py:419
  46.1 20.0 %all-to-all-start.1 = ((bf16[8,256,128]{2,1,0:T(8,128)(2,1)}), bf16[8,256,128]{2,1,0:T(8,128)(2,1)S(1)}, u32[]{:S(2)}, u32[]{:S(2)}) async-start(bf16[8,256,128]{2,1,0:T(8,128)(2,1)} %prefix.1), calls=%async_computation.1 | async-start | bytes 1048576 | tf_op jit(solution)/shard_map/all_to_all | solution.py:519
  50.9 14.7 %collective-permute-start.6 = (bf16[128,2048]{1,0:T(8,128)(2,1)S(1)}, bf16[128,2048]{1,0:T(8,128)(2,1)}, u32[]{:S(2)}, u32[]{:S(2)}) collective-permute-start(bf16[128,2048]{1,0:T(8,128)(2,1)S(1)} %collective-permute-done.3.refs_2_), channel_id=1, source_target_pairs={{0,1},{1,0},{2,3},{3,2},{4,5},{5,4},{6,7},{7,6},{8,9},{9,8},{10,11... | collective-permute-start | bytes 1572872 | tf_op jit(solution)/shard_map/ppermute | solution.py:417
  59.8 5.8 %collective-permute-start.7 = (bf16[128,2048]{1,0:T(8,128)(2,1)}, bf16[128,2048]{1,0:T(8,128)(2,1)}, u32[]{:S(2)}, u32[]{:S(2)}) collective-permute-start(bf16[128,2048]{1,0:T(8,128)(2,1)} %collective-permute-done.4.refs_3_), channel_id=1, source_target_pairs={{0,1},{1,0},{2,3},{3,2},{4,5},{5,4},{6,7},{7,6},{8,9},{9,8},{10,11... | collective-permute-start | bytes 1572872 | tf_op jit(solution)/shard_map/ppermute | solution.py:418
  63.9 2.2 %copy-start.12 = (f32[2048]{0:T(1024)S(1)}, f32[2048]{0:T(1024)}, u32[]{:S(2)}) copy-start(f32[2048]{0:T(1024)} %param.35) | copy-start | bytes 24580
  63.9 2.2 %copy-start.13 = (f32[2048]{0:T(1024)S(1)}, f32[2048]{0:T(1024)}, u32[]{:S(2)}) copy-start(f32[2048]{0:T(1024)} %param.37) | copy-start | bytes 24580
  63.9 2.2 %copy-start.17 = (f32[32,128]{1,0:T(8,128)S(1)}, f32[32,128]{1,0:T(8,128)}, u32[]{:S(2)}) copy-start(f32[32,128]{1,0:T(8,128)} %get-tuple-element.19.factor_ref) | copy-start | bytes 49156
  73.3 28.1 %collective-permute-start.9 = (bf16[128,2048]{1,0:T(8,128)(2,1)}, bf16[128,2048]{1,0:T(8,128)(2,1)S(1)}, u32[]{:S(2)}, u32[]{:S(2)}) collective-permute-start(bf16[128,2048]{1,0:T(8,128)(2,1)} %get-tuple-element.27.x_in), channel_id=1, source_target_pairs={{0,16},{16,0},{1,17},{17,1},{2,18},{18,2},{3,19},{19,3},{4,20},{20... | collective-permute-start | bytes 1572872 | tf_op jit(solution)/shard_map/ppermute | solution.py:564
  75.9 24.2 %collective-permute-start = (f32[8,128]{1,0:T(8,128)S(1)}, f32[8,128]{1,0:T(8,128)S(1)}, u32[]{:S(2)}, u32[]{:S(2)}) collective-permute-start(f32[8,128]{1,0:T(8,128)S(1)} %maximum_maximum_fusion.meta_ref), channel_id=1, source_target_pairs={{0,16},{16,0},{1,17},{17,1},{2,18},{18,2},{3,19},{19,3},{4,20},{20... | collective-permute-start | bytes 12296 | tf_op jit(solution)/shard_map/ppermute | solution.py:457
  103.3 24.7 %copy-start = (bf16[1,2048,512]{2,1,0:T(8,128)(2,1)S(1)}, bf16[1,2048,512]{2,1,0:T(8,128)(2,1)}, u32[]{:S(2)}) copy-start(bf16[1,2048,512]{2,1,0:T(8,128)(2,1)} %wg_ref.3) | copy-start | bytes 6291460
  124.3 19.8 %all-to-all-start.2 = ((bf16[16,16,2048]{2,1,0:T(8,128)(2,1)}), bf16[16,16,2048]{2,1,0:T(8,128)(2,1)S(1)}, u32[]{:S(2)}, u32[]{:S(2)}) async-start(bf16[16,16,2048]{2,1,0:T(8,128)(2,1)} %bitcast.64), calls=%async_computation.2 | async-start | bytes 2097152 | tf_op jit(solution)/shard_map/all_to_all | solution.py:569
  128.0 1.2 copy-start.4
  133.4 1.0 copy-start.2
  144.1 20.5 %all-to-all-start.5 = ((bf16[16,16,2048]{2,1,0:T(8,128)(2,1)}), bf16[16,16,2048]{2,1,0:T(8,128)(2,1)}, u32[]{:S(2)}, u32[]{:S(2)}) async-start(bf16[16,16,2048]{2,1,0:T(8,128)(2,1)} %bitcast.43), calls=%async_computation.5 | async-start | bytes 2097152 | tf_op jit(solution)/shard_map/all_to_all | solution.py:569
  152.9 1.0 copy-start.1
  164.6 34.1 %all-to-all-start.3 = ((bf16[16,16,2048]{2,1,0:T(8,128)(2,1)}), bf16[16,16,2048]{2,1,0:T(8,128)(2,1)S(1)}, u32[]{:S(2)}, u32[]{:S(2)}) async-start(bf16[16,16,2048]{2,1,0:T(8,128)(2,1)} %bitcast.41), calls=%async_computation.3 | async-start | bytes 2097152 | tf_op jit(solution)/shard_map/all_to_all | solution.py:569
  170.7 26.6 %collective-permute-start.10 = (bf16[128,2048]{1,0:T(8,128)(2,1)}, bf16[128,2048]{1,0:T(8,128)(2,1)S(1)}, u32[]{:S(2)}, u32[]{:S(2)}) collective-permute-start(bf16[128,2048]{1,0:T(8,128)(2,1)} %part.1), channel_id=1, source_target_pairs={{0,16},{16,0},{1,17},{17,1},{2,18},{18,2},{3,19},{19,3},{4,20},{20... | collective-permute-start | bytes 1572872 | tf_op jit(solution)/shard_map/ppermute | solution.py:660
  197.3 1.2 copy-start.3

commit v5 on v4

--- a/solution.py
+++ b/solution.py
@@ -357,29 +357,32 @@
     out_ref[...] = m_ref[...].astype(F32) + dot(h, wd[...], 1, 0)
 
 
-def expert_kernel(x_ref, wg_ref, wu_ref, wd_ref, out_ref, acc, obuf, sem):
+def expert_kernel(x_ref, wg_ref, wu_ref, wd_ref, out_ref, hbuf, dbuf, obuf, sem, sem_d):
     e = pl.program_id(0)
     j = pl.program_id(1)
+    down = pltpu.make_async_copy(wd_ref.at[e], dbuf, sem_d)
+
+    @pl.when(j == 0)
+    def _():
+        down.start()
+
     x = x_ref[...]
     h = (silu(dot(x, wg_ref[0], 1, 0)) * dot(x, wu_ref[0], 1, 0)).astype(BF16)
-    part = dot(h, wd_ref[0], 1, 0)
-
-    @pl.when(j == 0)
-    def _():
-        acc[...] = part
+    hbuf[j] = h
 
     @pl.when(j == pl.num_programs(1) - 1)
     def _():
+        down.wait()
+        hidden = jnp.concatenate([hbuf[k] for k in range(hbuf.shape[0])], axis=1)
         pieces = sem.shape[0]
-        rows = obuf.shape[0] // pieces
+        step = obuf.shape[1] // pieces
         copies = []
         for i in range(pieces):
-            at = slice(i * rows, (i + 1) * rows)
-            obuf[at] = (acc[at] + part[at]).astype(BF16)
+            at = slice(i * step, (i + 1) * step)
+            wide = pl.ds(i * step, step)
+            obuf[:, at] = dot(hidden, dbuf[:, at], 1, 0).astype(BF16)
             copies.append(
-                pltpu.make_async_copy(
-                    obuf.at[pl.ds(i * rows, rows)], out_ref.at[e, pl.ds(i * rows, rows)], sem.at[i]
-                )
+                pltpu.make_async_copy(obuf.at[:, wide], out_ref.at[e, :, wide], sem.at[i])
             )
             copies[-1].start()
         for copy in copies:
@@ -585,13 +588,15 @@
                 pl.BlockSpec((None, m, features), lambda e, j: (e, 0, 0)),
                 pl.BlockSpec((1, features, bn), lambda e, j: (e, 0, j)),
                 pl.BlockSpec((1, features, bn), lambda e, j: (e, 0, j)),
-                pl.BlockSpec((1, bn, features), lambda e, j: (e, j, 0)),
+                hbm,
             ],
             out_specs=hbm,
             scratch_shapes=[
-                pltpu.VMEM((m, features), F32),
+                pltpu.VMEM((ff // bn, m, bn), BF16),
+                pltpu.VMEM((ff, features), BF16),
                 pltpu.VMEM((m, features), BF16),
                 pltpu.SemaphoreType.DMA((pieces,)),
+                pltpu.SemaphoreType.DMA,
             ],
             compiler_params=vmem(48),
             cost_estimate=cost(2 << 30, 8 * MIB),

time: 201 us -> 201 us (level)
  no operation moved by 1% of the time
where the time goes in v5:
time: 201 us; the launch traced here: 200 us
  waiting for transfers between devices  95.9 us (48%)
  Pallas kernels  38.1 us (19%)
  starting transfers between devices  37.4 us (19%)
  blocking collectives  21.1 us (10%)
  local copies, waits for them, and re-layouts  7.01 us (3%)
    ppermute x1, waiting for transfers between devices, layer(): meta_far = lax.ppermute(meta, 'half', mirror)  23.8 us
    ppermute x1, waiting for transfers between devices, gather_rows(): lax.ppermute(lax.dynamic_slice_in_dim(w, odd * part, part, 0), 'dp', over)  22.8 us
    all_to_all x1, blocking collectives, exchange(): return lax.all_to_all(v, group, split_axis=0, concat_axis=0, tiled=True)  21.1 us
    all_to_all x3, waiting for transfers between devices, exchange(): return lax.all_to_all(v, group, split_axis=0, concat_axis=0, tiled=True)  20.1 us
    ppermute x1, waiting for transfers between devices, layer(): other = lax.ppermute(part, 'half', mirror)  20.1 us
    all_to_all x3, starting transfers between devices, exchange(): return lax.all_to_all(v, group, split_axis=0, concat_axis=0, tiled=True)  11.8 us
    pallas_call x2, Pallas kernels, serve(): pl.pallas_call(expert_kernel, out_shape=jax.ShapeDtypeStruct((own, m, fea...  8.74 us
    ppermute x1, waiting for transfers between devices, gather_rows(): ya = lax.ppermute(xa, 'sub', flip)  8.59 us
  transfers between devices with their start and end apart: 16, of which 7 were waited for; matrix products, arithmetic and copies ran while one was open for 1% of the time, Pallas kernels for 13%

profile of v5, /device:TPU:0, one launch (start us, length us, event | category | flops | bytes accessed | tf_op | source)
XLA Modules:
  0.0 199.9 jit_solution(15153374409576732103)
XLA Ops:
  0.0 0.0 copy-start.8
  0.0 0.0 copy-start.10
  0.0 1.5 tails.1
  1.5 4.9 %collective-permute-start.1 = (bf16[8,4096]{1,0:T(8,128)(2,1)}, bf16[8,4096]{1,0:T(8,128)(2,1)S(1)}, u32[]{:S(2)}, u32[]{:S(2)}) collective-permute-start(bf16[8,4096]{1,0:T(8,128)(2,1)} %tails.1), channel_id=1, source_target_pairs={{0,4},{4,8},{8,12},{12,16},{16,20},{20,24},{24,28},{1,5},{5,9},{9,... | collective-permute-start | bytes 196616 | tf_op jit(solution)/shard_map/ppermute | solution.py:478
  6.4 1.3 slice.3
  7.7 1.6 collective-permute-start.5
  9.3 0.0 collective-permute-start.2
  9.3 0.0 collective-permute-done.1.tail_ref
  9.4 2.8 %states.1 = bf16[8,264,128]{2,1,0:T(8,128)(2,1)} custom-call(bf16[32,128]{1,0:T(8,128)(2,1)S(1)} %bitcast.54, f32[1,32]{1,0:T(1,128)S(1)} %bitcast.58, f32[1,32]{1,0:T(1,128)S(1)} %bitcast.60, bf16[8,4096]{1,0:T(8,128)(2,1)S(1)} %collective-permute-done.1.tail_ref, bf16[4,2048]{1,0:T(4,128)(2,1)S(1)} %copy-done.8, bf16[4,1024]{1,0:T(4,128)(2,1)S(1)} %copy-done.10, ...), custom_call_target="tpu_custom_call" | custom-call | flops 1073741824 | bytes 4194304 | tf_op jit(solution)/shard_map/states/pallas_call | solution.py:479
  12.2 0.0 copy-start.16
  12.2 6.0 %all-to-all-start = ((bf16[8,264,128]{2,1,0:T(8,128)(2,1)}), bf16[8,264,128]{2,1,0:T(8,128)(2,1)S(1)}, u32[]{:S(2)}, u32[]{:S(2)}) async-start(bf16[8,264,128]{2,1,0:T(8,128)(2,1)} %states.1), calls=%async_computation | async-start | bytes 1081344 | tf_op jit(solution)/shard_map/all_to_all | solution.py:492
  18.2 1.1 constant_dynamic-slice_fusion
  19.3 1.6 collective-permute-start.3
  20.8 22.8 %collective-permute-done.3.refs_2_ = bf16[128,2048]{1,0:T(8,128)(2,1)S(1)} collective-permute-done((bf16[128,2048]{1,0:T(8,128)(2,1)S(1)}, bf16[128,2048]{1,0:T(8,128)(2,1)S(1)}, u32[]{:S(2)}, u32[]{:S(2)}) %collective-permute-start.3) | collective-permute-done | bytes 524320 | tf_op jit(solution)/shard_map/ppermute | solution.py:415
  43.7 1.5 collective-permute-start.4
  45.2 0.0 collective-permute-done.5.refs_4_
  45.2 0.0 collective-permute-start.8
  45.2 0.0 all-to-all-done.in_ref
  45.2 0.9 prefix.1
  46.1 4.8 %all-to-all-start.1 = ((bf16[8,256,128]{2,1,0:T(8,128)(2,1)}), bf16[8,256,128]{2,1,0:T(8,128)(2,1)S(1)}, u32[]{:S(2)}, u32[]{:S(2)}) async-start(bf16[8,256,128]{2,1,0:T(8,128)(2,1)} %prefix.1), calls=%async_computation.1 | async-start | bytes 1048576 | tf_op jit(solution)/shard_map/all_to_all | solution.py:522
  50.9 0.2 collective-permute-start.6
  51.2 8.6 %collective-permute-done.4.refs_3_ = bf16[128,2048]{1,0:T(8,128)(2,1)} collective-permute-done((bf16[128,2048]{1,0:T(8,128)(2,1)S(1)}, bf16[128,2048]{1,0:T(8,128)(2,1)}, u32[]{:S(2)}, u32[]{:S(2)}) %collective-permute-start.4) | collective-permute-done | bytes 524320 | tf_op jit(solution)/shard_map/ppermute | solution.py:418
  59.8 0.0 collective-permute-start.7
  59.8 0.1 pad.2.clone
  59.9 0.1 stack.40.order_ref
  59.9 0.1 maximum_maximum_fusion.meta_ref
  60.0 0.0 copy-done.11
  60.0 3.9 %within.1 = (f32[128,2048]{1,0:T(8,128)}, f32[32,128]{1,0:T(8,128)}, bf16[128,1024]{1,0:T(8,128)(2,1)}) custom-call(bf16[32,128]{1,0:T(8,128)(2,1)S(1)} %bitcast.55, f32[1,32]{1,0:T(1,128)S(1)} %bitcast.59, f32[1,32]{1,0:T(1,128)S(1)} %bitcast.61, f32[1,32]{1,0:T(1,128)S(1)} %bitcast.62, bf16[8,4096]{1,0:T(8,128)(2,1)S(1)} %collective-permute-done.1.tail_ref, ...), custom_call_target="tpu_custom_call" | custom-call | flops 2147483648 | bytes 8388608 | tf_op jit(solution)/shard_map/within/pallas_call | solution.py:493
  63.9 1.7 warm.1
  65.6 0.0 collective-permute-done.6.refs_5_
  65.6 0.0 collective-permute-done.7.refs_6_
  65.6 0.5 all-to-all-done.1
  66.1 0.0 collective-permute-done.8.refs_7_
  66.1 0.0 collective-permute-done.2.refs_1_
  66.1 0.0 copy-done.13
  66.1 0.0 copy-done.17
  66.1 7.1 %mix.1 = (bf16[128,2048]{1,0:T(8,128)(2,1)}, bf16[128,2048]{1,0:T(8,128)(2,1)}, bf16[256,2048]{1,0:T(8,128)(2,1)}) custom-call(s32[10]{0:T(128)S(1)} %stack.40.order_ref, f32[1,2048]{1,0:T(1,128)S(1)} %bitcast.56, f32[1,2048]{1,0:T(1,128)S(1)} %bitcast.57, f32[8,128]{1,0:T(8,128)S(1)} %maximum_maximum_fusion.meta_ref, f32[32,128]{1,0:T(8,128)S(1)} %copy-done.17, ...), custom_call_target="tpu_custom_call" | custom-call | flops 3221225472 | bytes 16777216 | tf_op jit(solution)/shard_map/mix/pallas_call | solution.py:538
  73.3 2.6 %collective-permute-start.9 = (bf16[128,2048]{1,0:T(8,128)(2,1)}, bf16[128,2048]{1,0:T(8,128)(2,1)S(1)}, u32[]{:S(2)}, u32[]{:S(2)}) collective-permute-start(bf16[128,2048]{1,0:T(8,128)(2,1)} %get-tuple-element.27.x_in), channel_id=1, source_target_pairs={{0,16},{16,0},{1,17},{17,1},{2,18},{18,2},{3,19},{19,3},{4,20},{20... | collective-permute-start | bytes 1572872 | tf_op jit(solution)/shard_map/ppermute | solution.py:567
  75.9 0.4 collective-permute-start
  76.3 23.8 %collective-permute-done.far_ref = f32[8,128]{1,0:T(8,128)S(1)} collective-permute-done((f32[8,128]{1,0:T(8,128)S(1)}, f32[8,128]{1,0:T(8,128)S(1)}, u32[]{:S(2)}, u32[]{:S(2)}) %collective-permute-start) | collective-permute-done | bytes 4128 | tf_op jit(solution)/shard_map/ppermute | solution.py:460
  100.1 1.3 plan.1
  101.4 0.0 collective-permute-done.9.x_in
  101.4 1.8 relay.1
  103.3 0.0 copy-start
  103.3 21.1 %all_to_all.30 = bf16[16,16,2048]{2,1,0:T(8,128)(2,1)} all-to-all(bf16[16,16,2048]{2,1,0:T(8,128)(2,1)} %bitcast.63), channel_id=1, replica_groups=mesh['half'=2,'sub'=4,'dp'=4] {'sub','dp'}, dimensions={0} | all-to-all | bytes 2097152 | tf_op jit(solution)/shard_map/all_to_all | solution.py:572
  124.3 3.7 %all-to-all-start.2 = ((bf16[16,16,2048]{2,1,0:T(8,128)(2,1)}), bf16[16,16,2048]{2,1,0:T(8,128)(2,1)S(1)}, u32[]{:S(2)}, u32[]{:S(2)}) async-start(bf16[16,16,2048]{2,1,0:T(8,128)(2,1)} %bitcast.64), calls=%async_computation.2 | async-start | bytes 2097152 | tf_op jit(solution)/shard_map/all_to_all | solution.py:572
  128.0 1.2 copy-done.4
  129.2 4.4 %experts.3 = bf16[1,256,2048]{2,1,0:T(8,128)(2,1)S(1)} custom-call(bf16[1,256,2048]{2,1,0:T(8,128)(2,1)S(1)} %bitcast.44, bf16[1,2048,512]{2,1,0:T(8,128)(2,1)S(1)} %copy-done, bf16[1,2048,512]{2,1,0:T(8,128)(2,1)} %wu_ref.3, bf16[1,512,2048]{2,1,0:T(8,128)(2,1)} %wd_ref.3), custom_call_target="tpu_custom_call" | custom-call | flops 2147483648 | bytes 8388608 | tf_op jit(solution)/shard_map/experts/pallas_call | solution.py:583
  133.6 0.0 copy-start.2
  133.6 1.0 copy-done.2
  134.6 9.5 %all-to-all-done.2 = bf16[16,16,2048]{2,1,0:T(8,128)(2,1)S(1)} async-done(((bf16[16,16,2048]{2,1,0:T(8,128)(2,1)}), bf16[16,16,2048]{2,1,0:T(8,128)(2,1)S(1)}, u32[]{:S(2)}, u32[]{:S(2)}) %all-to-all-start.2) | async-done | bytes 1048608 | tf_op jit(solution)/shard_map/all_to_all | solution.py:572
  144.1 4.5 %all-to-all-start.5 = ((bf16[16,16,2048]{2,1,0:T(8,128)(2,1)}), bf16[16,16,2048]{2,1,0:T(8,128)(2,1)}, u32[]{:S(2)}, u32[]{:S(2)}) async-start(bf16[16,16,2048]{2,1,0:T(8,128)(2,1)} %bitcast.43), calls=%async_computation.5 | async-start | bytes 2097152 | tf_op jit(solution)/shard_map/all_to_all | solution.py:572
  148.6 4.4 %experts.2 = bf16[1,256,2048]{2,1,0:T(8,128)(2,1)S(1)} custom-call(bf16[1,256,2048]{2,1,0:T(8,128)(2,1)S(1)} %bitcast.42, bf16[1,2048,512]{2,1,0:T(8,128)(2,1)S(1)} %copy-done, bf16[1,2048,512]{2,1,0:T(8,128)(2,1)} %wu_ref.3, bf16[1,512,2048]{2,1,0:T(8,128)(2,1)} %wd_ref.3), custom_call_target="tpu_custom_call" | custom-call | flops 2147483648 | bytes 8388608 | tf_op jit(solution)/shard_map/experts/pallas_call | solution.py:583
  153.0 1.0 copy-done.1
  154.0 10.6 %all-to-all-done.5 = bf16[16,16,2048]{2,1,0:T(8,128)(2,1)} async-done(((bf16[16,16,2048]{2,1,0:T(8,128)(2,1)}), bf16[16,16,2048]{2,1,0:T(8,128)(2,1)}, u32[]{:S(2)}, u32[]{:S(2)}) %all-to-all-start.5) | async-done | bytes 1048608 | tf_op jit(solution)/shard_map/all_to_all | solution.py:572
  164.6 3.7 %all-to-all-start.3 = ((bf16[16,16,2048]{2,1,0:T(8,128)(2,1)}), bf16[16,16,2048]{2,1,0:T(8,128)(2,1)S(1)}, u32[]{:S(2)}, u32[]{:S(2)}) async-start(bf16[16,16,2048]{2,1,0:T(8,128)(2,1)} %bitcast.41), calls=%async_computation.3 | async-start | bytes 2097152 | tf_op jit(solution)/shard_map/all_to_all | solution.py:572
  168.2 2.5 %part.1 = bf16[128,2048]{1,0:T(8,128)(2,1)} custom-call(bf16[2,128,256]{2,1,0:T(8,128)(2,1)S(1)} %get-tuple-element.29.shares_ref, bf16[256,2048]{1,0:T(8,128)(2,1)} %bitcast.35.got_ref), custom_call_target="tpu_custom_call" | custom-call | flops 536870912 | bytes 3145728 | tf_op jit(solution)/shard_map/part/pallas_call | solution.py:655
  170.7 1.9 collective-permute-start.10
  172.6 4.6 %shared.1.base_ref = f32[128,2048]{1,0:T(8,128)} custom-call(bf16[128,2048]{1,0:T(8,128)(2,1)} %get-tuple-element.27.x_in, bf16[128,2048]{1,0:T(8,128)(2,1)} %get-tuple-element.28.mixed_in, bf16[2048,512]{1,0:T(8,128)(2,1)} %wg_in.1, bf16[2048,512]{1,0:T(8,128)(2,1)} %wu_in.1, bf16[512,2048]{1,0:T(8,128)(2,1)} %wd_in.1), custom_call_target="tpu_custom_call" | custom-call | flops 1073741824 | bytes 8388608 | tf_op jit(solution)/shard_map/shared/pallas_call | solution.py:610
  177.2 20.1 %collective-permute-done.10.other_ref = bf16[128,2048]{1,0:T(8,128)(2,1)S(1)} collective-permute-done((bf16[128,2048]{1,0:T(8,128)(2,1)}, bf16[128,2048]{1,0:T(8,128)(2,1)S(1)}, u32[]{:S(2)}, u32[]{:S(2)}) %collective-permute-start.10) | collective-permute-done | bytes 524320 | tf_op jit(solution)/shard_map/ppermute | solution.py:665
  197.3 1.2 copy-done.3
  198.5 0.1 sum.1.base_ref
  198.6 0.0 all-to-all-done.3
  198.6 1.2 combine.1
  (32 shorter events, 0.1 us)
Async XLA Ops:
  0.0 9.3 %copy-start.5 = (bf16[1,128,2048]{2,1,0:T(8,128)(2,1)S(1)}, bf16[1,128,2048]{2,1,0:T(8,128)(2,1)}, u32[]{:S(2)}) copy-start(bf16[1,128,2048]{2,1,0:T(8,128)(2,1)} %param.24) | copy-start | bytes 1572868
  0.0 9.3 %copy-start.6 = (bf16[1,128,1024]{2,1,0:T(8,128)(2,1)S(1)}, bf16[1,128,1024]{2,1,0:T(8,128)(2,1)}, u32[]{:S(2)}) copy-start(bf16[1,128,1024]{2,1,0:T(8,128)(2,1)} %param.26) | copy-start | bytes 786436
  0.0 9.3 %copy-start.9 = (bf16[1,128,32]{1,2,0:T(8,128)(2,1)S(1)}, bf16[1,128,32]{1,2,0:T(8,128)(2,1)}, u32[]{:S(2)}) copy-start(bf16[1,128,32]{1,2,0:T(8,128)(2,1)} %param.28) | copy-start | bytes 24580
  0.0 9.3 %copy-start.14 = (f32[32]{0:T(128)S(1)}, f32[32]{0:T(128)}, u32[]{:S(2)}) copy-start(f32[32]{0:T(128)} %param.32) | copy-start | bytes 388
  0.0 9.3 %copy-start.15 = (f32[32]{0:T(128)S(1)}, f32[32]{0:T(128)}, u32[]{:S(2)}) copy-start(f32[32]{0:T(128)} %param.33) | copy-start | bytes 388
  0.0 9.3 %copy-start.8 = (bf16[4,2048]{1,0:T(4,128)(2,1)S(1)}, bf16[4,2048]{1,0:T(4,128)(2,1)}, u32[]{:S(2)}) copy-start(bf16[4,2048]{1,0:T(4,128)(2,1)} %wx_ref.3) | copy-start | bytes 49156
  0.0 9.3 %copy-start.10 = (bf16[4,1024]{1,0:T(4,128)(2,1)S(1)}, bf16[4,1024]{1,0:T(4,128)(2,1)}, u32[]{:S(2)}) copy-start(bf16[4,1024]{1,0:T(4,128)(2,1)} %wb_ref.3) | copy-start | bytes 24580
  1.5 7.8 %collective-permute-start.1 = (bf16[8,4096]{1,0:T(8,128)(2,1)}, bf16[8,4096]{1,0:T(8,128)(2,1)S(1)}, u32[]{:S(2)}, u32[]{:S(2)}) collective-permute-start(bf16[8,4096]{1,0:T(8,128)(2,1)} %tails.1), channel_id=1, source_target_pairs={{0,4},{4,8},{8,12},{12,16},{16,20},{20,24},{24,28},{1,5},{5,9},{9,... | collective-permute-start | bytes 196616 | tf_op jit(solution)/shard_map/ppermute | solution.py:478
  7.7 37.4 %collective-permute-start.5 = (bf16[256,2048]{1,0:T(8,128)(2,1)S(1)}, bf16[256,2048]{1,0:T(8,128)(2,1)}, u32[]{:S(2)}, u32[]{:S(2)}) collective-permute-start(bf16[256,2048]{1,0:T(8,128)(2,1)S(1)} %slice.3), channel_id=1, source_target_pairs={{0,2},{1,3},{2,0},{3,1},{4,6},{5,7},{6,4},{7,5},{8,10},{9,11},{10,... | collective-permute-start | bytes 3145736 | tf_op jit(solution)/shard_map/ppermute | solution.py:417
  9.3 56.8 %collective-permute-start.2 = (bf16[512,2048]{1,0:T(8,128)(2,1)}, bf16[512,2048]{1,0:T(8,128)(2,1)}, u32[]{:S(2)}, u32[]{:S(2)}) collective-permute-start(bf16[512,2048]{1,0:T(8,128)(2,1)} %refs_0_.1), channel_id=1, source_target_pairs={{0,1},{1,0},{2,3},{3,2},{4,5},{5,4},{6,7},{7,6},{8,9},{9,8},{10,11... | collective-permute-start | bytes 6291464 | tf_op jit(solution)/shard_map/ppermute | solution.py:419
  12.1 47.6 %copy-start.18 = (s32[1,128,2]{1,2,0:T(2,128)S(1)}, s32[1,128,2]{1,2,0:T(2,128)}, u32[]{:S(2)}) copy-start(s32[1,128,2]{1,2,0:T(2,128)} %param.44) | copy-start | bytes 3076
  12.1 47.8 %copy-start.19 = (f32[1,128,2]{1,2,0:T(2,128)S(1)}, f32[1,128,2]{1,2,0:T(2,128)}, u32[]{:S(2)}) copy-start(f32[1,128,2]{1,2,0:T(2,128)} %param.45) | copy-start | bytes 3076
  12.1 47.9 %copy-start.7 = (bf16[1,128,1024]{2,1,0:T(8,128)(2,1)S(1)}, bf16[1,128,1024]{2,1,0:T(8,128)(2,1)}, u32[]{:S(2)}) copy-start(bf16[1,128,1024]{2,1,0:T(8,128)(2,1)} %param.27) | copy-start | bytes 786436
  12.1 47.9 %copy-start.11 = (bf16[4,1024]{1,0:T(4,128)(2,1)S(1)}, bf16[4,1024]{1,0:T(4,128)(2,1)}, u32[]{:S(2)}) copy-start(bf16[4,1024]{1,0:T(4,128)(2,1)} %wc_ref.1) | copy-start | bytes 24580
  12.2 47.9 %copy-start.16 = (f32[32]{0:T(128)S(1)}, f32[32]{0:T(128)}, u32[]{:S(2)}) copy-start(f32[32]{0:T(128)} %param.34) | copy-start | bytes 388
  12.2 33.0 %all-to-all-start = ((bf16[8,264,128]{2,1,0:T(8,128)(2,1)}), bf16[8,264,128]{2,1,0:T(8,128)(2,1)S(1)}, u32[]{:S(2)}, u32[]{:S(2)}) async-start(bf16[8,264,128]{2,1,0:T(8,128)(2,1)} %states.1), calls=%async_computation | async-start | bytes 1081344 | tf_op jit(solution)/shard_map/all_to_all | solution.py:492
  19.3 24.4 %collective-permute-start.3 = (bf16[128,2048]{1,0:T(8,128)(2,1)S(1)}, bf16[128,2048]{1,0:T(8,128)(2,1)S(1)}, u32[]{:S(2)}, u32[]{:S(2)}) collective-permute-start(bf16[128,2048]{1,0:T(8,128)(2,1)S(1)} %constant_dynamic-slice_fusion), channel_id=1, source_target_pairs={{0,2},{1,3},{2,0},{3,1},{4,6},{5,7},{6,4},{7,5},{8,10},{9,11},{10,... | collective-permute-start | bytes 1572872 | tf_op jit(solution)/shard_map/ppermute | solution.py:415
  43.7 20.2 %copy-start.20 = (bf16[128,2048]{1,0:T(8,128)(2,1)}, bf16[128,2048]{1,0:T(8,128)(2,1)S(1)}, u32[]{:S(2)}) copy-start(bf16[128,2048]{1,0:T(8,128)(2,1)S(1)} %collective-permute-done.3.refs_2_) | copy-start | bytes 1572868
  43.7 16.1 %collective-permute-start.4 = (bf16[128,2048]{1,0:T(8,128)(2,1)S(1)}, bf16[128,2048]{1,0:T(8,128)(2,1)}, u32[]{:S(2)}, u32[]{:S(2)}) collective-permute-start(bf16[128,2048]{1,0:T(8,128)(2,1)S(1)} %collective-permute-done.3.refs_2_), channel_id=1, source_target_pairs={{0,4},{4,0},{8,12},{12,8},{1,5},{5,1},{9,13},{13,9},{2,6},{6,2},{1... | collective-permute-start | bytes 1572872 | tf_op jit(solution)/shard_map/ppermute | solution.py:418
  45.2 20.9 %collective-permute-start.8 = (bf16[256,2048]{1,0:T(8,128)(2,1)}, bf16[256,2048]{1,0:T(8,128)(2,1)}, u32[]{:S(2)}, u32[]{:S(2)}) collective-permute-start(bf16[256,2048]{1,0:T(8,128)(2,1)} %collective-permute-done.5.refs_4_), channel_id=1, source_target_pairs={{0,1},{1,0},{2,3},{3,2},{4,5},{5,4},{6,7},{7,6},{8,9},{9,8},{10,11... | collective-permute-start | bytes 3145736 | tf_op jit(solution)/shard_map/ppermute | solution.py:422
  46.1 20.0 %all-to-all-start.1 = ((bf16[8,256,128]{2,1,0:T(8,128)(2,1)}), bf16[8,256,128]{2,1,0:T(8,128)(2,1)S(1)}, u32[]{:S(2)}, u32[]{:S(2)}) async-start(bf16[8,256,128]{2,1,0:T(8,128)(2,1)} %prefix.1), calls=%async_computation.1 | async-start | bytes 1048576 | tf_op jit(solution)/shard_map/all_to_all | solution.py:522
  50.9 14.7 %collective-permute-start.6 = (bf16[128,2048]{1,0:T(8,128)(2,1)S(1)}, bf16[128,2048]{1,0:T(8,128)(2,1)}, u32[]{:S(2)}, u32[]{:S(2)}) collective-permute-start(bf16[128,2048]{1,0:T(8,128)(2,1)S(1)} %collective-permute-done.3.refs_2_), channel_id=1, source_target_pairs={{0,1},{1,0},{2,3},{3,2},{4,5},{5,4},{6,7},{7,6},{8,9},{9,8},{10,11... | collective-permute-start | bytes 1572872 | tf_op jit(solution)/shard_map/ppermute | solution.py:420
  59.8 5.8 %collective-permute-start.7 = (bf16[128,2048]{1,0:T(8,128)(2,1)}, bf16[128,2048]{1,0:T(8,128)(2,1)}, u32[]{:S(2)}, u32[]{:S(2)}) collective-permute-start(bf16[128,2048]{1,0:T(8,128)(2,1)} %collective-permute-done.4.refs_3_), channel_id=1, source_target_pairs={{0,1},{1,0},{2,3},{3,2},{4,5},{5,4},{6,7},{7,6},{8,9},{9,8},{10,11... | collective-permute-start | bytes 1572872 | tf_op jit(solution)/shard_map/ppermute | solution.py:421
  63.9 2.2 %copy-start.12 = (f32[2048]{0:T(1024)S(1)}, f32[2048]{0:T(1024)}, u32[]{:S(2)}) copy-start(f32[2048]{0:T(1024)} %param.35) | copy-start | bytes 24580
  63.9 2.2 %copy-start.13 = (f32[2048]{0:T(1024)S(1)}, f32[2048]{0:T(1024)}, u32[]{:S(2)}) copy-start(f32[2048]{0:T(1024)} %param.37) | copy-start | bytes 24580
  63.9 2.2 %copy-start.17 = (f32[32,128]{1,0:T(8,128)S(1)}, f32[32,128]{1,0:T(8,128)}, u32[]{:S(2)}) copy-start(f32[32,128]{1,0:T(8,128)} %get-tuple-element.19.factor_ref) | copy-start | bytes 49156
  73.3 28.1 %collective-permute-start.9 = (bf16[128,2048]{1,0:T(8,128)(2,1)}, bf16[128,2048]{1,0:T(8,128)(2,1)S(1)}, u32[]{:S(2)}, u32[]{:S(2)}) collective-permute-start(bf16[128,2048]{1,0:T(8,128)(2,1)} %get-tuple-element.27.x_in), channel_id=1, source_target_pairs={{0,16},{16,0},{1,17},{17,1},{2,18},{18,2},{3,19},{19,3},{4,20},{20... | collective-permute-start | bytes 1572872 | tf_op jit(solution)/shard_map/ppermute | solution.py:567
  75.9 24.2 %collective-permute-start = (f32[8,128]{1,0:T(8,128)S(1)}, f32[8,128]{1,0:T(8,128)S(1)}, u32[]{:S(2)}, u32[]{:S(2)}) collective-permute-start(f32[8,128]{1,0:T(8,128)S(1)} %maximum_maximum_fusion.meta_ref), channel_id=1, source_target_pairs={{0,16},{16,0},{1,17},{17,1},{2,18},{18,2},{3,19},{19,3},{4,20},{20... | collective-permute-start | bytes 12296 | tf_op jit(solution)/shard_map/ppermute | solution.py:460
  103.3 24.7 %copy-start = (bf16[1,2048,512]{2,1,0:T(8,128)(2,1)S(1)}, bf16[1,2048,512]{2,1,0:T(8,128)(2,1)}, u32[]{:S(2)}) copy-start(bf16[1,2048,512]{2,1,0:T(8,128)(2,1)} %wg_ref.3) | copy-start | bytes 6291460
  124.3 19.8 %all-to-all-start.2 = ((bf16[16,16,2048]{2,1,0:T(8,128)(2,1)}), bf16[16,16,2048]{2,1,0:T(8,128)(2,1)S(1)}, u32[]{:S(2)}, u32[]{:S(2)}) async-start(bf16[16,16,2048]{2,1,0:T(8,128)(2,1)} %bitcast.64), calls=%async_computation.2 | async-start | bytes 2097152 | tf_op jit(solution)/shard_map/all_to_all | solution.py:572
  128.0 1.2 copy-start.4
  133.6 1.0 copy-start.2
  144.1 20.5 %all-to-all-start.5 = ((bf16[16,16,2048]{2,1,0:T(8,128)(2,1)}), bf16[16,16,2048]{2,1,0:T(8,128)(2,1)}, u32[]{:S(2)}, u32[]{:S(2)}) async-start(bf16[16,16,2048]{2,1,0:T(8,128)(2,1)} %bitcast.43), calls=%async_computation.5 | async-start | bytes 2097152 | tf_op jit(solution)/shard_map/all_to_all | solution.py:572
  153.0 1.0 copy-start.1
  164.6 34.1 %all-to-all-start.3 = ((bf16[16,16,2048]{2,1,0:T(8,128)(2,1)}), bf16[16,16,2048]{2,1,0:T(8,128)(2,1)S(1)}, u32[]{:S(2)}, u32[]{:S(2)}) async-start(bf16[16,16,2048]{2,1,0:T(8,128)(2,1)} %bitcast.41), calls=%async_computation.3 | async-start | bytes 2097152 | tf_op jit(solution)/shard_map/all_to_all | solution.py:572
  170.7 26.6 %collective-permute-start.10 = (bf16[128,2048]{1,0:T(8,128)(2,1)}, bf16[128,2048]{1,0:T(8,128)(2,1)S(1)}, u32[]{:S(2)}, u32[]{:S(2)}) collective-permute-start(bf16[128,2048]{1,0:T(8,128)(2,1)} %part.1), channel_id=1, source_target_pairs={{0,16},{16,0},{1,17},{17,1},{2,18},{18,2},{3,19},{19,3},{4,20},{20... | collective-permute-start | bytes 1572872 | tf_op jit(solution)/shard_map/ppermute | solution.py:665
  197.3 1.2 copy-start.3
